TPU v7x, 32 devices: a whole 2x2x4 slice. The times are simulated.
32 devices in a mesh: sp: 8 (over z, y), dp: 4 (over x, core).
Axes of the slice: x: 2, y: 2, z: 4, core: 2. Of those that a mesh axis runs over, the one named last changes fastest.
Arguments:
- u_pre: bfloat16 [4, 8192, 2048], P('dp', 'sp'), may hold values from -6 to 6
- v_pre: bfloat16 [4, 8192, 2048], P('dp', 'sp'), may hold values from -6 to 6
- d_out: bfloat16 [4, 8192, 2048], P('dp', 'sp'), may hold values from -6 to 6
- w_mix: bfloat16 [16, 128, 128], replicated, may hold values from -0.5 to 0.5
- mix_bias: float32 [16, 128], replicated, may hold values from 0.1 to 1.9
- norm_gain: float32 [16, 128], replicated, may hold values from 0.1 to 1.9
- norm_shift: float32 [16, 128], replicated, may hold values from -3 to 3
- w_out: bfloat16 [2048, 2048], P('dp'), may hold values from -0.125 to 0.125
Outputs:
- grad_u: bfloat16 [4, 8192, 2048], P('dp', 'sp')
- grad_v: bfloat16 [4, 8192, 2048], P('dp', 'sp')
- grad_w_out: float32 [2048, 2048], P('dp')
- grad_w_mix: float32 [16, 128, 128], replicated
- grad_mix_bias: float32 [16, 128], replicated
- grad_gain: float32 [16, 128], replicated
- grad_shift: float32 [16, 128], replicated
All inputs are finite; a program needn't handle non-finite values.
Results may differ from a plain program's by a relative error of at most 0.012.
Values may be sent and summed in bfloat16 or wider, within the bound.
No kernel may reach another device: no remote copies, remote signals or barrier semaphores. Data moves between devices by JAX's collectives and lax.ppermute only.
A program may use at most 192 MiB of HBM per device.

v0:
```python
import jax
import jax.numpy as jnp
from jax import lax
from jax.sharding import PartitionSpec as P

EPS = 1e-05


def mechanism(grad_s, u_pre, v_pre, w_mix, mix_bias, gain, shift):
    items, length, width = grad_s.shape
    groups, span = (w_mix.shape[0], w_mix.shape[1])
    chans = width // groups
    shape = (items, length // span, span, groups, chans)
    u_val = u_pre.astype(jnp.float32).reshape(shape)
    v_val = v_pre.astype(jnp.float32).reshape(shape)
    cotan = grad_s.astype(jnp.float32).reshape(shape)
    upper, u_back = jax.vjp(jax.nn.gelu, u_val)
    gated, v_back = jax.vjp(jax.nn.gelu, v_val)
    centre = gated - jnp.mean(gated, axis=-1, keepdims=True)
    inverse = lax.rsqrt(jnp.mean(centre * centre, axis=-1, keepdims=True) + EPS)
    scaled = centre * inverse
    normed = (scaled * gain + shift).astype(jnp.bfloat16)
    lower = jnp.tril(jnp.ones((span, span), dtype=bool))
    w_low = jnp.where(lower[None], w_mix, jnp.zeros_like(w_mix))
    mixed = jnp.einsum("gts,insgc->intgc", w_low, normed, preferred_element_type=jnp.float32)
    mixed = mixed + jnp.transpose(mix_bias)[:, :, None]
    gated_out = (upper * mixed).astype(jnp.bfloat16)
    d_mixed = cotan * upper
    d_mixed_b = d_mixed.astype(jnp.bfloat16)
    grad_u = u_back(cotan * mixed)[0].astype(jnp.bfloat16).reshape(items, length, width)
    grad_bias = jnp.transpose(jnp.sum(d_mixed, axis=(0, 1, 4)))
    grad_w = jnp.einsum("intgc,insgc->gts", d_mixed_b, normed, preferred_element_type=jnp.float32)
    grad_w = jnp.where(lower[None], grad_w, jnp.zeros_like(grad_w))
    d_normed = jnp.einsum("gts,intgc->insgc", w_low, d_mixed_b, preferred_element_type=jnp.float32)
    grad_gain = jnp.sum(d_normed * scaled, axis=(0, 1, 2))
    grad_shift = jnp.sum(d_normed, axis=(0, 1, 2))
    d_scaled = d_normed * gain
    d_gated = inverse * (
        d_scaled
        - jnp.mean(d_scaled, axis=-1, keepdims=True)
        - scaled * jnp.mean(d_scaled * scaled, axis=-1, keepdims=True)
    )
    grad_v = v_back(d_gated)[0].astype(jnp.bfloat16).reshape(items, length, width)
    return (
        grad_u,
        grad_v,
        gated_out.reshape(items, length, width),
        grad_w,
        grad_bias,
        grad_gain,
        grad_shift,
    )


def on_device(u_pre, v_pre, d_out, w_mix, mix_bias, norm_gain, norm_shift, w_out):
    grad_s = lax.dot_general(
        d_out,
        lax.all_gather(w_out, "dp", axis=0, tiled=True),
        (((2,), (1,)), ((), ())),
        preferred_element_type=jnp.float32,
    ).astype(jnp.bfloat16)
    grad_u, grad_v, gated_out, grad_w, grad_bias, grad_gain, grad_shift = mechanism(
        grad_s, u_pre, v_pre, w_mix, mix_bias, norm_gain, norm_shift
    )
    grad_w, grad_bias, grad_gain, grad_shift = lax.psum(
        (grad_w, grad_bias, grad_gain, grad_shift), ("sp", "dp")
    )
    width = gated_out.shape[2]
    flat_d = d_out.reshape(-1, d_out.shape[2])
    flat_s = gated_out.reshape(-1, width)
    num_sp = lax.axis_size("sp")
    num_dp = lax.axis_size("dp")
    piece_rows = width // (num_sp * num_dp)
    reordered = (
        flat_s.reshape(-1, num_dp, num_sp, piece_rows).transpose(0, 2, 1, 3).reshape(-1, width)
    )
    summed = lax.psum_scatter(
        lax.dot_general(
            reordered, flat_d, (((0,), (0,)), ((), ())), preferred_element_type=jnp.float32
        ),
        ("sp", "dp"),
        scatter_dimension=0,
        tiled=True,
    )
    grad_w_out = lax.all_gather(summed, "sp", axis=0, tiled=True)
    return (grad_u, grad_v, grad_w_out, grad_w, grad_bias, grad_gain, grad_shift)


def solution(mesh):
    return jax.shard_map(
        on_device,
        mesh=mesh,
        in_specs=(
            P("dp", "sp", None),
            P("dp", "sp", None),
            P("dp", "sp", None),
            P(),
            P(),
            P(),
            P(),
            P("dp", None),
        ),
        out_specs=(P("dp", "sp", None), P("dp", "sp", None), P("dp", None), P(), P(), P(), P()),
        check_vma=False,
    )
```

profile of v0, /device:TPU:0, one launch (start us, length us, event | category | flops | bytes accessed | tf_op | source)
XLA Modules:
  0.0 546.6 jit_solution(12029540268014962513)
XLA Ops:
  7.2 0.0 all-gather.3.cloned.1.call-start
  7.2 0.7 all-gather.3.cloned.1.call-update
  7.9 0.0 reduce-scatter.2.cloned.1.call-start
  7.9 3.2 convert_bitcast_fusion
  11.2 5.2 copy.68
  16.4 9.7 %copy.45 = f32[1,8,128,16,128]{2,4,1,3,0:T(8,128)} copy(f32[1,8,128,16,128]{4,3,0,2,1:T(8,128)} %bitcast.90) | data formatting | bytes 16777216 | tf_op jit(solution)/shard_map/reshape | solution.py:14
  26.1 3.2 convert_bitcast_fusion.1
  29.3 5.2 copy.66
  34.5 8.7 %copy.39 = f32[1,8,128,16,128]{2,4,1,3,0:T(8,128)} copy(f32[1,8,128,16,128]{4,3,0,2,1:T(8,128)} %bitcast.94) | data formatting | bytes 16777216 | tf_op jit(solution)/shard_map/reshape | solution.py:15
  43.3 0.0 copy-start.1
  43.3 0.0 copy-start.5
  43.3 0.0 copy-start.6
  43.3 5.9 %fusion.52 = f32[8,128,16]{1,0,2:T(8,128)S(1)} fusion(f32[1,8,128,16,128]{2,4,1,3,0:T(8,128)} %copy.39), kind=kLoop, calls=%fused_computation.77 | loop fusion | flops 18857984 | bytes 8454144 | tf_op jit(solution)/shard_map/reduce_sum | solution.py:19
  49.2 0.0 copy-done
  49.2 3.7 multiply_reduce_fusion.2
  53.0 6.5 %fusion.35 = bf16[8,128,16,128]{3,1,0,2:T(8,128)(2,1)} fusion(f32[8,128,16,128]{3,2,1,0:T(8,128)S(1)} %bitcast.95, f32[16,128]{1,0:T(8,128)S(1)} %copy-done.6, f32[16,128]{1,0:T(8,128)S(1)} %copy-done.5, f32[8,128,16]{1,0,2:T(8,128)S(1)} %add_rsqrt_fusion, f32[8,128,16]{1,0,2:T(8,128)S(1)} %broadcast_multiply_fusion.2), kind=kLoop, calls=%fused_computation.52 | loop fusion | flops 27262976 | bytes 12730368 | tf_op jit(solution)/shard_map/convert_element_type | solution.py:22
  59.5 11.1 %all-gather.3.cloned.1.call-done = bf16[2048,2048]{1,0:T(8,128)(2,1)} async-done(((bf16[512,2048]{1,0:T(8,128)(2,1)}), bf16[2048,2048]{1,0:T(8,128)(2,1)}) %all-gather.3.cloned.1.call-update) | async-done | bytes 8388624 | tf_op jit(solution)/shard_map/all_gather | solution.py:58
  70.5 12.7 %convert_bitcast_fusion.2 = f32[128,8,16,128]{3,1,2,0:T(8,128)S(1)} fusion(bf16[2048,2048]{1,0:T(8,128)(2,1)} %all-gather.3.cloned.1.call-done, bf16[1,1024,2048]{2,1,0:T(8,128)(2,1)} %param.10), kind=kOutput, calls=%fused_computation.51 | convolution fusion | flops 8594128896 | bytes 20971520 | tf_op jit(solution)/shard_map/dot_general | solution.py:56
  83.3 5.2 copy.65
  88.5 8.8 %copy.41 = f32[1,8,128,16,128]{2,4,1,3,0:T(8,128)} copy(f32[1,8,128,16,128]{4,3,2,1,0:T(8,128)} %bitcast.92) | data formatting | bytes 16777216 | tf_op jit(solution)/shard_map/reshape | solution.py:16
  97.3 0.0 copy-done.9
  97.3 14.1 %multiply_convert_fusion = (bf16[1,8,128,16,128]{2,4,1,3,0:T(8,128)(2,1)S(1)}, bf16[1,8,128,16,128]{2,4,1,3,0:T(8,128)(2,1)}, f32[128,16]{0,1:T(8,128)S(1)}) fusion(f32[128,16]{0,1:T(8,128)S(1)} %bitcast.99, f32[1,8,128,16,128]{2,4,1,3,0:T(8,128)} %copy.45, f32[1,8,128,16,128]{2,4,1,3,0:T(8,128)} %copy.41, bf16[8,128,16,128]{3,1,0,2:T(8,128)(2,1)} %fusion.35, ...), kind=kOutput, calls=%fused_computation.46 | convolution fusion | flops 593754112 | bytes 29917184 | tf_op jit(solution)/shard_map/gts,insgc->intgc/dot_general | solution.py:25
  111.4 5.6 %copy.58 = bf16[1,8,128,16,128]{2,1,4,3,0:T(8,128)(2,1)} copy(bf16[1,8,128,16,128]{2,4,1,3,0:T(8,128)(2,1)S(1)} %get-tuple-element.14) | data formatting | bytes 8388608 | tf_op jit(solution)/shard_map/convert_element_type | solution.py:27
  117.0 7.3 %reshape_reshape_reshape.3 = bf16[1024,4,8,64]{0,3,2,1:T(8,128)(2,1)} reshape(bf16[1,8,128,16,128]{2,1,4,3,0:T(8,128)(2,1)} %copy.58) | data formatting | bytes 8388608 | tf_op jit(solution)/shard_map/reshape;reshape;reshape | solution.py:75
  124.3 2.9 copy.59
  127.2 0.6 copy-done.7
  127.8 11.7 %fusion.37 = f32[2048,2048]{1,0:T(8,128)} fusion(bf16[1024,2048]{0,1:T(8,128)(2,1)S(1)} %bitcast.97, bf16[1,1024,2048]{2,1,0:T(8,128)(2,1)S(1)} %copy-done.7), kind=kOutput, calls=%fused_computation.57 | convolution fusion | flops 8589934592 | bytes 25165824 | tf_op jit(solution)/shard_map/dot_general | solution.py:78
  139.5 0.0 reduce-scatter.2.cloned.1.call-update
  139.5 0.0 all-gather.5.cloned.1.call-start
  139.5 183.0 %reduce-scatter.2.cloned.1.call-done = f32[64,2048]{1,0:T(8,128)} async-done(((f32[2048,2048]{1,0:T(8,128)}), f32[64,2048]{1,0:T(8,128)}) %reduce-scatter.2.cloned.1.call-update) | async-done | bytes 524304 | tf_op jit(solution)/shard_map/reduce_scatter | solution.py:77
  322.5 0.0 all-gather.5.cloned.1.call-update
  322.6 0.0 all-reduce.3.cloned.1.call-start
  322.6 0.0 copy-start.3
  322.6 10.4 %fusion.33 = bf16[8,128,16,128]{3,1,0,2:T(8,128)(2,1)S(1)} fusion(f32[8,128,16,128]{3,2,1,0:T(8,128)} %bitcast.93, f32[8,128,16,128]{3,2,1,0:T(8,128)} %bitcast.91), kind=kLoop, calls=%fused_computation.39 | loop fusion | flops 20971520 | bytes 20971520 | tf_op jit(solution)/shard_map/convert_element_type | solution.py:29
  333.0 0.0 copy-start.2
  333.1 2.0 copy-done.2
  335.1 2.2 fusion.43
  337.3 11.4 %fusion.34 = (f32[16,128]{1,0:T(8,128)S(1)}, f32[8,128,16]{1,0,2:T(8,128)S(1)}, f32[8,128,16]{1,0,2:T(8,128)S(1)}, f32[16,128]{1,0:T(8,128)S(1)}, f32[16,8,128,128]{3,2,1,0:T(8,128)}) fusion(f32[8,128,16]{1,0,2:T(8,128)S(1)} %add_rsqrt_fusion, f32[8,128,16]{1,0,2:T(8,128)S(1)} %broadcast_multiply_fusion.2, f32[1,8,128,16,128]{2,4,1,3,0:T(8,128)} %copy.39, ...), kind=kOutput, calls=%fused_computation.44 | convolution fusion | flops 572747776 | bytes 21798912 | tf_op jit(solution)/shard_map/gts,intgc->insgc/dot_general | solution.py:34
  348.7 0.0 all-reduce.3.cloned.1.call-update
  348.8 12.3 %fusion.6 = bf16[1,8,128,16,128]{2,4,1,3,0:T(8,128)(2,1)} fusion(f32[1,8,128,16,128]{2,4,1,3,0:T(8,128)} %copy.39, f32[16,8,128,128]{3,2,1,0:T(8,128)} %get-tuple-element.17, f32[8,128,16]{1,0,2:T(8,128)S(1)} %get-tuple-element.18, f32[8,128,16]{1,0,2:T(8,128)S(1)} %get-tuple-element.19, f32[16,128]{1,0:T(8,128)S(1)} %copy-done.5, ...), kind=kLoop, calls=%fused_computation.12 | loop fusion | flops 58720256 | bytes 21241856 | tf_op jit(solution)/shard_map/convert_element_type | solution.py:43
  361.0 6.7 %copy.47 = bf16[1,8,128,16,128]{4,3,2,1,0:T(8,128)(2,1)} copy(bf16[1,8,128,16,128]{2,4,1,3,0:T(8,128)(2,1)} %get-tuple-element.15) | data formatting | bytes 8388608 | tf_op jit(solution)/shard_map/convert_element_type | solution.py:30
  367.7 7.3 %reshape.458 = bf16[1,1024,2048]{2,1,0:T(8,128)(2,1)} reshape(bf16[1,8,128,16,128]{4,3,2,1,0:T(8,128)(2,1)} %copy.47) | data formatting | bytes 8388608 | tf_op jit(solution)/shard_map/reshape | solution.py:30
  375.0 6.7 %copy.56 = bf16[1,8,128,16,128]{4,3,2,1,0:T(8,128)(2,1)} copy(bf16[1,8,128,16,128]{2,4,1,3,0:T(8,128)(2,1)} %fusion.6) | data formatting | bytes 8388608 | tf_op jit(solution)/shard_map/convert_element_type | solution.py:43
  381.7 7.3 %reshape.461 = bf16[1,1024,2048]{2,1,0:T(8,128)(2,1)} reshape(bf16[1,8,128,16,128]{4,3,2,1,0:T(8,128)(2,1)} %copy.56) | data formatting | bytes 8388608 | tf_op jit(solution)/shard_map/reshape | solution.py:43
  389.0 42.5 %all-reduce = (f32[16,128]{1,0:T(8,128)}, f32[16,128]{1,0:T(8,128)}, f32[16,128]{1,0:T(8,128)}) all-reduce(f32[16,128]{1,0:T(8,128)S(1)} %bitcast.98, f32[16,128]{1,0:T(8,128)S(1)} %get-tuple-element.7, f32[16,128]{1,0:T(8,128)S(1)} %get-tuple-element.10), channel_id=1, replica_groups=mesh['sp'=8,'dp'=4] {'sp','dp'}, use_global_device_ids=true, to_apply=%region_7.8 | all-reduce | flops 6144 | bytes 49152 | tf_op jit(solution)/shard_map/psum | solution.py:65
  431.6 102.5 %all-reduce.3.cloned.1.call-done = f32[16,128,128]{2,1,0:T(8,128)} async-done(((f32[16,128,128]{2,1,0:T(8,128)}), f32[16,128,128]{2,1,0:T(8,128)}) %all-reduce.3.cloned.1.call-update) | async-done | bytes 1048592 | tf_op jit(solution)/shard_map/psum | solution.py:65
  534.1 4.8 copy.78
  538.9 1.0 copy.79
  (16 shorter events, 0.1 us)
Async XLA Ops:
  7.2 63.4 %all-gather.3.cloned.1.call-start = ((), (), s32[]{:S(2)}) async-start(), calls=%async_computation.1 | async-start | bytes 10485760 | tf_op jit(solution)/shard_map/all_gather | solution.py:58
  7.9 314.6 %reduce-scatter.2.cloned.1.call-start = ((), (), s32[]{:S(2)}) async-start(), calls=%async_computation.2 | async-start | bytes 17301504 | tf_op jit(solution)/shard_map/reduce_scatter | solution.py:77
  43.3 5.9 %copy-start = (f32[1,8,128,16,128]{2,4,1,3,0:T(8,128)S(1)}, f32[1,8,128,16,128]{2,4,1,3,0:T(8,128)}, u32[]{:S(2)}) copy-start(f32[1,8,128,16,128]{2,4,1,3,0:T(8,128)} %copy.39) | copy-start | bytes 25165828
  43.3 9.7 %copy-start.1 = (f32[128,8,16,128]{3,2,1,0:T(8,128)S(1)}, f32[128,8,16,128]{3,2,1,0:T(8,128)}, u32[]{:S(2)}) copy-start(f32[128,8,16,128]{3,2,1,0:T(8,128)} %copy.66) | copy-start | bytes 25165828
  43.3 9.7 %copy-start.5 = (f32[16,128]{1,0:T(8,128)S(1)}, f32[16,128]{1,0:T(8,128)}, u32[]{:S(2)}) copy-start(f32[16,128]{1,0:T(8,128)} %param.13) | copy-start | bytes 24580
  43.3 9.7 %copy-start.6 = (f32[16,128]{1,0:T(8,128)S(1)}, f32[16,128]{1,0:T(8,128)}, u32[]{:S(2)}) copy-start(f32[16,128]{1,0:T(8,128)} %param.14) | copy-start | bytes 24580
  88.5 8.8 %copy-start.8 = (bf16[16,128,128]{2,1,0:T(8,128)(2,1)S(1)}, bf16[16,128,128]{2,1,0:T(8,128)(2,1)}, u32[]{:S(2)}) copy-start(bf16[16,128,128]{2,1,0:T(8,128)(2,1)} %param.11) | copy-start | bytes 1572868
  88.5 8.8 %copy-start.9 = (f32[16,128]{1,0:T(8,128)S(1)}, f32[16,128]{1,0:T(8,128)}, u32[]{:S(2)}) copy-start(f32[16,128]{1,0:T(8,128)} %param.12) | copy-start | bytes 24580
  124.3 3.4 copy-start.7
  139.5 292.1 %all-gather.5.cloned.1.call-start = ((), (), s32[]{:S(2)}) async-start(), calls=%async_computation.3 | async-start | bytes 4718592 | tf_op jit(solution)/shard_map/all_gather | solution.py:85
  322.6 211.5 %all-reduce.3.cloned.1.call-start = ((), (), s32[]{:S(2)}) async-start(), calls=%async_computation.4 | async-start | bytes 2097152 | tf_op jit(solution)/shard_map/psum | solution.py:65
  322.6 12.5 %copy-start.3 = (bf16[8,128,16,128]{3,1,0,2:T(8,128)(2,1)S(1)}, bf16[8,128,16,128]{3,1,0,2:T(8,128)(2,1)}, u32[]{:S(2)}) copy-start(bf16[8,128,16,128]{3,1,0,2:T(8,128)(2,1)} %fusion.35) | copy-start | bytes 12582916
  333.0 2.0 copy-start.2
  534.1 4.8 copy-start.4
Sparse Core Ops, SparseCore 0:
  9.5 60.9 all-gather.2
  139.6 182.8 reduce-scatter.1
  324.7 74.5 all-gather.4
  404.8 129.1 all-reduce.2
where the time goes:
time: 551 us; the launch traced here: 547 us
  waiting for transfers between devices  297 us (54%)
  local copies, waits for them, and re-layouts  95 us (17%)
  matrix products  52.2 us (9%)
  other arithmetic  45.2 us (8%)
  blocking collectives  42.5 us (8%)
  between operations  14.2 us (3%)
    reduce_scatter x1, waiting for transfers between devices, on_device(): lax.psum_scatter(lax.dot_general(reordered, flat_d, (((0,), (0,)), ((), (...  183 us
    psum x1, waiting for transfers between devices, on_device(): lax.psum((grad_w, grad_bias, grad_gain, grad_shift), ('sp', 'dp'))  102 us
    psum x1, blocking collectives, on_device(): lax.psum((grad_w, grad_bias, grad_gain, grad_shift), ('sp', 'dp'))  42.5 us
    unnamed x25, local copies, waits for them, and re-layouts  24 us
    dot_general x1, matrix products, mechanism(): jnp.einsum('gts,insgc->intgc', w_low, normed, preferred_element_type=jnp....  14.1 us
    dot_general x1, matrix products, on_device(): lax.dot_general(d_out, lax.all_gather(w_out, 'dp', axis=0, tiled=True), (...  12.7 us
    convert_element_type x1, other arithmetic, mechanism(): v_back(d_gated)[0].astype(jnp.bfloat16).reshape(items, length, width)  12.3 us
    dot_general x1, matrix products, on_device(): lax.dot_general(reordered, flat_d, (((0,), (0,)), ((), ())), preferred_el...  11.7 us
  transfers between devices with their start and end apart: 4, of which 3 were waited for; matrix products, arithmetic and copies ran while one was open for 21% of the time, Pallas kernels for 0%

commit v1 on v0

v1 whole, which is shorter than its diff:
```python
import functools

import jax
import jax.numpy as jnp
from jax import lax
from jax.experimental import pallas as pl
from jax.experimental.pallas import tpu as pltpu
from jax.sharding import PartitionSpec as P

EPS = 1e-05
K0 = 0.7978845608028654
K1 = 0.044715
AXES = ("sp", "dp")
bf16 = jnp.bfloat16
f32 = jnp.float32


def swap(value, bit_sp, bit_dp):
    num_sp, num_dp = lax.axis_size("sp"), lax.axis_size("dp")
    pairs = [
        (s * num_dp + d, (s ^ bit_sp) * num_dp + (d ^ bit_dp))
        for s in range(num_sp)
        for d in range(num_dp)
    ]
    return lax.ppermute(value, AXES, pairs)


def dot(a, b, dims):
    return lax.dot_general(a, b, (dims, ((), ())), preferred_element_type=f32)


def forward_kernel(cfg, sc, u, v, d_out, w_low, bias, gain, shift, *rest):
    span, chans, per, piece, inner, fused = cfg
    if fused:
        recv, s1, k1, s2, k2, upper_o, m1_o, scaled_o, w1_o, gated = rest
    else:
        part, upper_o, m1_o, scaled_o, w1_o, gated = rest
    blocks = u.shape[0] // span
    cols = []
    for g in range(per):
        row = jnp.broadcast_to(bias[g], (chans, span))
        cols.append(jnp.transpose(row))

    def step(b, carry):
        rows = pl.ds(pl.multiple_of(b * span, span), span)
        for g in range(per):
            lanes = slice(g * chans, (g + 1) * chans)
            a = u[rows, lanes].astype(f32)
            c = v[rows, lanes].astype(f32)
            c2 = c * c
            tv = jnp.tanh(c * (K0 + (K0 * K1) * c2))
            hv = 0.5 + 0.5 * tv
            gate = c * hv
            dv = hv + (c * (0.5 - 0.5 * tv * tv)) * (K0 + (3.0 * K0 * K1) * c2)
            centre = gate - jnp.mean(gate, axis=1, keepdims=True)
            inv = lax.rsqrt(jnp.mean(centre * centre, axis=1, keepdims=True) + EPS)
            scaled = centre * inv
            normed = (scaled * gain[g] + shift[g]).astype(bf16)
            mixed = dot(w_low[g], normed, ((1,), (0,))) + cols[g]
            a2 = a * a
            tu = jnp.tanh(a * (K0 + (K0 * K1) * a2))
            hu = 0.5 + 0.5 * tu
            up = a * hu
            du = hu + (a * (0.5 - 0.5 * tu * tu)) * (K0 + (3.0 * K0 * K1) * a2)
            gated[rows, lanes] = (up * mixed).astype(bf16)
            upper_o[rows, lanes] = up.astype(bf16)
            m1_o[rows, lanes] = (mixed * du).astype(bf16)
            scaled_o[rows, lanes] = scaled.astype(bf16)
            w1_o[rows, lanes] = (dv * inv).astype(bf16)
        return carry

    lax.fori_loop(0, blocks, step, 0)
    if not fused:
        part[0] = dot(gated[...], d_out[...], ((0,), (0,))).astype(bf16)
        return
    half = d_out.shape[1] // 2
    count = per * chans // piece
    for side, (send, keep) in enumerate(((s1, k1), (s2, k2))):
        lanes = slice(side * half, (side + 1) * half)
        total = dot(gated[...], d_out[:, lanes], ((0,), (0,)))
        for p in range(count):
            rows = slice(p * piece, (p + 1) * piece)
            value = (total[rows] + recv[0, rows, lanes].astype(f32)).astype(bf16)
            rel = jnp.bitwise_xor(p, sc[1] % inner)
            low, high = rel % 2, rel // 2
            if side == 0:
                flag, at = low, high
            else:
                flag, at = high % 2, (high // 2) * 2 + low
            where = pl.ds(pl.multiple_of(at * piece, piece), piece)

            @pl.when(flag == 1)
            def _():
                send[0, where, :] = value

            @pl.when(flag == 0)
            def _():
                keep[0, where, :] = value


def forward(sc, u, v, d_out, w_low, bias, gain, shift, recv):
    num_sp, num_dp = lax.axis_size("sp"), lax.axis_size("dp")
    length, width = u.shape
    groups, span, _ = w_low.shape
    chans = width // groups
    rows = width // num_dp
    per = 2
    chunk = per * chans
    steps = rows // chunk
    count = num_dp // 2
    piece = rows // num_sp
    inner = chunk // piece
    fused = recv is not None
    first = num_dp - (2 if fused else 1)

    def at(i, j, sc):
        return jnp.bitwise_xor(first - 2 * i, sc[0]) * steps + j

    wide = pl.BlockSpec((length, chunk), lambda i, j, sc: (0, at(i, j, sc)))
    vec = pl.BlockSpec((per, 1, span), lambda i, j, sc: (at(i, j, sc), 0, 0))
    in_specs = [
        wide,
        wide,
        pl.BlockSpec(d_out.shape, lambda i, j, sc: (0, 0), pipeline_mode=pl.Buffered(1)),
        pl.BlockSpec((per, span, span), lambda i, j, sc: (at(i, j, sc), 0, 0)),
        vec,
        vec,
        vec,
    ]
    args = [u, v, d_out, w_low, bias, gain, shift]
    save = pl.BlockSpec((length, chunk), lambda i, j, sc: (0, i * steps + j))
    save_shape = jax.ShapeDtypeStruct((length, count * rows), bf16)
    depth = d_out.shape[1]
    if fused:
        in_specs.append(pl.BlockSpec((1, chunk, depth), lambda i, j, sc: (i, j, 0)))
        args.append(recv)
        spec = pl.BlockSpec(
            (1, chunk // 2, depth // 2),
            lambda i, j, sc: (i, jnp.bitwise_xor(j, sc[1] // inner), 0),
        )
        heads = [spec] * 4
        shapes = [jax.ShapeDtypeStruct((count, rows // 2, depth // 2), bf16)] * 4
    else:
        heads = [pl.BlockSpec((1, chunk, depth), lambda i, j, sc: (i, j, 0))]
        shapes = [jax.ShapeDtypeStruct((count, rows, depth), bf16)]
    return pl.pallas_call(
        functools.partial(forward_kernel, (span, chans, per, piece, inner, fused)),
        grid_spec=pltpu.PrefetchScalarGridSpec(
            num_scalar_prefetch=1,
            grid=(count, steps),
            in_specs=in_specs,
            out_specs=heads + [save] * 4,
            scratch_shapes=[pltpu.VMEM((length, chunk), bf16)],
        ),
        out_shape=shapes + [save_shape] * 4,
        name="forward_own" if fused else "forward_other",
    )(sc, *args)


def backward_kernel(cfg, sc, d_out, w, upper, m1, scaled_i, w1, w_up, gain, shift, *rest):
    span, chans, per = cfg
    gu, gv, small, grad = rest[-4:]
    blocks = upper.shape[0] // span
    grad[...] = dot(d_out[...], w[...], ((1,), (1,))).astype(bf16)

    def step(b, carry):
        rows = pl.ds(pl.multiple_of(b * span, span), span)
        out = []
        for g in range(per):
            acc_w, acc_b, acc_g, acc_s = carry[4 * g : 4 * g + 4]
            lanes = slice(g * chans, (g + 1) * chans)
            cot = grad[rows, lanes].astype(f32)
            gu[rows, lanes] = (cot * m1[rows, lanes].astype(f32)).astype(bf16)
            dm = cot * upper[rows, lanes].astype(f32)
            dmb = dm.astype(bf16)
            scaled = scaled_i[rows, lanes].astype(f32)
            normed = (scaled * gain[g] + shift[g]).astype(bf16)
            acc_w = acc_w + dot(dmb, normed, ((1,), (1,)))
            dn = dot(w_up[g], dmb, ((1,), (0,)))
            e = dn * gain[g]
            mean_e = jnp.mean(e, axis=1, keepdims=True)
            mean_s = jnp.mean(e * scaled, axis=1, keepdims=True)
            gv[rows, lanes] = (
                w1[rows, lanes].astype(f32) * (e - mean_e - scaled * mean_s)
            ).astype(bf16)
            out += [acc_w, acc_b + dm, acc_g + dn * scaled, acc_s + dn]
        return tuple(out)

    zero = jnp.zeros((span, chans), f32)
    done = lax.fori_loop(0, blocks, step, (zero,) * (4 * per))
    row = lax.broadcasted_iota(jnp.int32, (span, span), 0)
    col = lax.broadcasted_iota(jnp.int32, (span, span), 1)
    lines = []
    for g in range(per):
        lines.append(jnp.sum(jnp.transpose(done[4 * g + 1]), axis=0, keepdims=True))
        lines.append(jnp.sum(done[4 * g + 2], axis=0, keepdims=True))
        lines.append(jnp.sum(done[4 * g + 3], axis=0, keepdims=True))
    even, odd = done[0], done[4]
    diag = jnp.sum(jnp.where(row == col, odd, 0.0), axis=0, keepdims=True)
    small[0, :span] = jnp.where(row >= col, even, jnp.transpose(odd))
    pad = jnp.zeros((small.shape[1] - span - 7, span), f32)
    small[0, span:] = jnp.concatenate(lines + [diag, pad], axis=0)


SMALL_ROWS = 144


def backward(sc, rel, index, d_out, w, saves, w_up, gain, shift, carried):
    num_dp = lax.axis_size("dp")
    length, depth = d_out.shape
    groups, span, _ = w_up.shape
    rows = w.shape[0]
    width = rows * num_dp
    chans = width // groups
    per = 2
    chunk = per * chans
    steps = rows // chunk

    def at(j, sc):
        return jnp.bitwise_xor(rel, sc[0]) * steps + j

    save = pl.BlockSpec((length, chunk), lambda j, sc: (0, index * steps + j))
    vec = pl.BlockSpec((per, 1, span), lambda j, sc: (at(j, sc), 0, 0))
    in_specs = [
        pl.BlockSpec(d_out.shape, lambda j, sc: (0, 0), pipeline_mode=pl.Buffered(1)),
        pl.BlockSpec((chunk, depth), lambda j, sc: (j, 0)),
        save,
        save,
        save,
        save,
        pl.BlockSpec((per, span, span), lambda j, sc: (at(j, sc), 0, 0)),
        vec,
        vec,
    ]
    args = [d_out, w, *saves, w_up, gain, shift]
    aliases = {}
    if carried is not None:
        for k, value in enumerate(carried):
            aliases[1 + len(args)] = k
            in_specs.append(pl.BlockSpec(memory_space=pl.ANY))
            args.append(value)
    out = pl.BlockSpec((length, chunk), lambda j, sc: (0, at(j, sc)))
    shape = jax.ShapeDtypeStruct((length, width), bf16)
    return pl.pallas_call(
        functools.partial(backward_kernel, (span, chans, per)),
        grid_spec=pltpu.PrefetchScalarGridSpec(
            num_scalar_prefetch=1,
            grid=(steps,),
            in_specs=in_specs,
            out_specs=[
                out,
                out,
                pl.BlockSpec((1, SMALL_ROWS, span), lambda j, sc: (at(j, sc), 0, 0)),
            ],
            scratch_shapes=[pltpu.VMEM((length, chunk), bf16)],
        ),
        out_shape=[
            shape,
            shape,
            jax.ShapeDtypeStruct((groups // per, SMALL_ROWS, span), f32),
        ],
        input_output_aliases=aliases,
        name=f"backward_{rel}",
    )(sc, *args)


def assemble_kernel(sc, a, b, out):
    half = a.shape[-1]
    out[:, :half] = a[0].astype(f32)
    out[:, half:] = b[0].astype(f32)


def assemble(sc, first, second, order_a, order_b, rows):
    pieces, piece, half = first.shape

    def place(order):
        def index(p, sc):
            rel = jnp.bitwise_xor(p, sc[1])
            at = 0
            for bit in order:
                at = at * 2 + jnp.bitwise_and(rel // bit, 1)
            return (at, 0, 0)

        return index

    return pl.pallas_call(
        assemble_kernel,
        grid_spec=pltpu.PrefetchScalarGridSpec(
            num_scalar_prefetch=1,
            grid=(pieces,),
            in_specs=[
                pl.BlockSpec((1, piece, half), place(order_a)),
                pl.BlockSpec((1, piece, half), place(order_b)),
            ],
            out_specs=pl.BlockSpec((piece, 2 * half), lambda p, sc: (p, 0)),
        ),
        out_shape=jax.ShapeDtypeStruct((rows, 2 * half), f32),
        name="assemble",
    )(sc, first, second)


def bits_of(count):
    return [1 << k for k in range(count.bit_length() - 1)]


def add(a, b):
    return (a.astype(f32) + b.astype(f32)).astype(a.dtype)


def reduce_projection(sc, s1, k1, s2, k2, piece):
    num_sp, num_dp = lax.axis_size("sp"), lax.axis_size("dp")
    sp_bits = bits_of(num_sp)
    bit_a, bit_b, others = sp_bits[0], sp_bits[1], sp_bits[2:]
    count, _, half = k1.shape
    rest = num_sp // 4
    k1 = add(k1, swap(s1, bit_a, 0)).reshape(count, rest, 2, piece, half)
    k2 = add(k2, swap(s2, bit_b, 0)).reshape(count, rest, 2, piece, half)
    r1 = swap(k1[:, :, 1], bit_b, 0)
    r2 = swap(k2[:, :, 1], bit_a, 0)
    both = jnp.stack([add(k1[:, :, 0], r1), add(k2[:, :, 0], r2)], axis=1)
    for bit in reversed(bits_of(num_dp)[1:]):
        middle = both.shape[0] // 2
        both = add(both[middle:], swap(both[:middle], 0, bit))
    both = both[0]
    for k, bit in enumerate(others):
        shape = both.shape
        split = (2, rest >> (k + 1), 2, 1 << k, piece, half)
        got = jnp.flip(swap(both, bit, 0).reshape(split), axis=2).reshape(shape)
        both = add(both, got)
    a, b = both[0], both[1]
    a = jnp.concatenate([a, swap(a, bit_a, 0)], axis=0)
    b = jnp.concatenate([b, swap(b, bit_b, 0)], axis=0)
    a = jnp.concatenate([a, swap(a, bit_b, 0)], axis=0)
    b = jnp.concatenate([b, swap(b, bit_a, 0)], axis=0)
    high = list(reversed(others))
    return assemble(sc, a, b, [bit_b, bit_a] + high, [bit_a, bit_b] + high, num_sp * piece)


def reduce_small(value):
    steps = [(0, bit) for bit in bits_of(lax.axis_size("dp"))]
    steps += [(bit, 0) for bit in bits_of(lax.axis_size("sp"))]
    shape = value.shape
    value = value.reshape(-1, shape[-1])
    done = []
    for bit_sp, bit_dp in steps[:4]:
        if bit_dp:
            mine = jnp.bitwise_and(lax.axis_index("dp") // bit_dp, 1)
        else:
            mine = jnp.bitwise_and(lax.axis_index("sp") // bit_sp, 1)
        half = value.shape[0] // 2
        keep = lax.dynamic_slice_in_dim(value, mine * half, half)
        send = lax.dynamic_slice_in_dim(value, (1 - mine) * half, half)
        value = keep + swap(send, bit_sp, bit_dp)
        done.append((bit_sp, bit_dp, mine))
    for bit_sp, bit_dp in steps[4:]:
        value = value + swap(value, bit_sp, bit_dp)
    for bit_sp, bit_dp, mine in reversed(done):
        other = swap(value, bit_sp, bit_dp)
        first = jnp.where(mine == 0, value, other)
        second = jnp.where(mine == 0, other, value)
        value = jnp.concatenate([first, second], axis=0)
    return value.reshape(shape)


def on_device(u_pre, v_pre, d_out, w_mix, mix_bias, norm_gain, norm_shift, w_out):
    num_sp, num_dp = lax.axis_size("sp"), lax.axis_size("dp")
    shape = u_pre.shape
    width = shape[2]
    groups, span, _ = w_mix.shape
    u, v = u_pre.reshape(-1, width), v_pre.reshape(-1, width)
    d = d_out.reshape(-1, d_out.shape[2])
    sc = jnp.stack([lax.axis_index("dp"), lax.axis_index("sp")]).astype(jnp.int32)
    lower = jnp.tril(jnp.ones((span, span), dtype=bool))
    w_low = jnp.where(lower[None], w_mix, jnp.zeros_like(w_mix))
    w_up = jnp.swapaxes(w_low, 1, 2)
    bias, gain, shift = (a[:, None, :] for a in (mix_bias, norm_gain, norm_shift))

    weights = {0: w_out}
    for rel in range(2, num_dp, 2):
        top = 1 << (rel.bit_length() - 1)
        weights[rel] = swap(weights[rel - top], 0, top)
    for rel in range(0, num_dp, 2):
        weights[rel + 1] = swap(weights[rel], 0, 1)

    part, *saves_other = forward(sc, u, v, d, w_low, bias, gain, shift, None)
    recv = swap(part, 0, 1)
    s1, k1, s2, k2, *saves_own = forward(sc, u, v, d, w_low, bias, gain, shift, recv)
    carried = None
    order = [1, 0] + list(range(2, num_dp))
    for rel in order:
        saves = saves_own if rel % 2 == 0 else saves_other
        index = num_dp // 2 - 1 - rel // 2
        carried = backward(
            sc, rel, index, d, weights[rel], saves, w_up, gain, shift, carried
        )
    grad_u, grad_v, small = carried
    grad_w_out = reduce_projection(sc, s1, k1, s2, k2, width // num_dp // num_sp)
    small = reduce_small(small)
    body, lines = small[:, :span], small[:, span:]
    diag = jnp.where(jnp.eye(span, dtype=bool)[None], lines[:, 6][:, None, :], 0.0)
    strict = jnp.tril(jnp.ones((span, span), dtype=bool), -1)[None]
    even = jnp.where(lower[None], body, 0.0)
    odd = jnp.where(strict, jnp.swapaxes(body, 1, 2), diag)
    grad_w = jnp.stack([even, odd], axis=1).reshape(groups, span, span)
    lines = lines[:, :6].reshape(groups, 3, span)
    return (
        grad_u.reshape(shape),
        grad_v.reshape(shape),
        grad_w_out,
        grad_w,
        lines[:, 0],
        lines[:, 1],
        lines[:, 2],
    )


def solution(mesh):
    return jax.shard_map(
        on_device,
        mesh=mesh,
        in_specs=(
            P("dp", "sp", None),
            P("dp", "sp", None),
            P("dp", "sp", None),
            P(),
            P(),
            P(),
            P(),
            P("dp", None),
        ),
        out_specs=(P("dp", "sp", None), P("dp", "sp", None), P("dp", None), P(), P(), P(), P()),
        check_vma=False,
    )
```

time: 551 us -> 291 us (0.53)
  waiting for transfers between devices: 297 us -> 133 us
  Pallas kernels: 0 us -> 110 us
  local copies, waits for them, and re-layouts: 95 us -> 6.54 us
  matrix products: 52.2 us -> 0 us
  blocking collectives: 42.5 us -> 0 us
  other arithmetic: 45.2 us -> 12.1 us
  starting transfers between devices: 0.16 us -> 27.8 us
  between operations: 14.2 us -> 0.95 us
    reduce_scatter x1 -> x0, waiting for transfers between devices: 183 us -> none  [on_device(): lax.psum_scatter(lax.dot_general(reordered, flat_d, (((0,), (0,)), ((), (...]
    ppermute x0 -> x23, waiting for transfers between devices: none -> 133 us  [swap(): return lax.ppermute(value, AXES, pairs)]
    pallas_call x0 -> x7, Pallas kernels: none -> 110 us  [the longest x4 54.2 us: backward(): pl.pallas_call(functools.partial(backward_kernel, (span, chans, per)), gr...]
    psum x1 -> x0, waiting for transfers between devices: 102 us -> none  [on_device(): lax.psum((grad_w, grad_bias, grad_gain, grad_shift), ('sp', 'dp'))]
    dot_general x5 -> x0, matrix products: 52.2 us -> none  [the longest x1 14.1 us: mechanism(): jnp.einsum('gts,insgc->intgc', w_low, normed, preferred_element_type=jnp....]
    psum x1 -> x0, blocking collectives: 42.5 us -> none  [on_device(): lax.psum((grad_w, grad_bias, grad_gain, grad_shift), ('sp', 'dp'))]
    reshape x5 -> x1, local copies, waits for them, and re-layouts: 41.9 us -> 0.01 us  [on_device(): lines = lines[:, :6].reshape(groups, 3, span)]
    ppermute x0 -> x23, starting transfers between devices: none -> 27.8 us  [swap(): return lax.ppermute(value, AXES, pairs)]
  transfers between devices with their start and end apart: 4 -> 23, of which waited for: 3 -> 14; matrix products, arithmetic and copies ran while one was open for 21% -> 3% of each run, Pallas kernels for 0% -> 23%
where the time goes in v1:
time: 291 us
  waiting for transfers between devices  133 us (46%)
  Pallas kernels  110 us (38%)
  starting transfers between devices  27.8 us (10%)
  other arithmetic  12.1 us (4%)
  local copies, waits for them, and re-layouts  6.54 us (2%)
    ppermute x23, waiting for transfers between devices, swap(): return lax.ppermute(value, AXES, pairs)  133 us
    pallas_call x4, Pallas kernels, backward(): pl.pallas_call(functools.partial(backward_kernel, (span, chans, per)), gr...  54.2 us
    pallas_call x2, Pallas kernels, forward(): pl.pallas_call(functools.partial(forward_kernel, (span, chans, per, piece...  48.8 us
    ppermute x23, starting transfers between devices, swap(): return lax.ppermute(value, AXES, pairs)  27.8 us
    pallas_call x1, Pallas kernels, assemble(): pl.pallas_call(assemble_kernel, grid_spec=pltpu.PrefetchScalarGridSpec(nu...  6.92 us
  transfers between devices with their start and end apart: 23, of which 14 were waited for; matrix products, arithmetic and copies ran while one was open for 3% of the time, Pallas kernels for 23%

profile of v1, /device:TPU:0, one launch (start us, length us, event | category | flops | bytes accessed | tf_op | source)
XLA Modules:
  0.0 290.6 jit_solution(4798583277599592906)
XLA Ops:
  0.7 1.3 copy.30
  2.0 1.0 copy.31.w_low
  3.0 0.6 pad_add_fusion.sc
  3.6 22.9 %forward_other.1 = (bf16[2,512,2048]{2,1,0:T(8,128)(2,1)}, bf16[1024,1024]{1,0:T(8,128)(2,1)}, bf16[1024,1024]{1,0:T(8,128)(2,1)}, bf16[1024,1024]{1,0:T(8,128)(2,1)}, bf16[1024,1024]{1,0:T(8,128)(2,1)}) custom-call(s32[2]{0:T(128)} %pad_add_fusion.sc, bf16[1024,2048]{1,0:T(8,128)(2,1)} %bitcast.69, bf16[1024,2048]{1,0:T(8,128)(2,1)} %bitcast.71, ...), custom_call_target="tpu_custom_call" | custom-call | tf_op jit(solution)/shard_map/forward_other/pallas_call | solution.py:146
  27.1 2.6 collective-permute-start
  29.8 46.2 %collective-permute-done.w = bf16[512,2048]{1,0:T(8,128)(2,1)} collective-permute-done((bf16[512,2048]{1,0:T(8,128)(2,1)S(1)}, bf16[512,2048]{1,0:T(8,128)(2,1)}, u32[]{:S(2)}, u32[]{:S(2)}) %collective-permute-start) | collective-permute-done | bytes 2097184 | tf_op jit(solution)/shard_map/ppermute | solution.py:25
  76.0 0.8 fusion.8.w_up
  76.8 13.4 %backward_1.1 = (bf16[1024,2048]{1,0:T(8,128)(2,1)}, bf16[1024,2048]{1,0:T(8,128)(2,1)}, f32[8,144,128]{2,1,0:T(8,128)}) custom-call(s32[2]{0:T(128)} %pad_add_fusion.sc, bf16[1024,2048]{1,0:T(8,128)(2,1)} %bitcast.62, bf16[512,2048]{1,0:T(8,128)(2,1)} %collective-permute-done.3.w, bf16[1024,1024]{1,0:T(8,128)(2,1)} %get-tuple-element.32.upper, ...), custom_call_target="tpu_custom_call" | custom-call | tf_op jit(solution)/shard_map/backward_1/pallas_call | solution.py:244
  90.2 25.9 %forward_own.1 = (bf16[2,256,1024]{2,1,0:T(8,128)(2,1)}, bf16[2,256,1024]{2,1,0:T(8,128)(2,1)}, bf16[2,256,1024]{2,1,0:T(8,128)(2,1)}, bf16[2,256,1024]{2,1,0:T(...) custom-call(s32[2]{0:T(128)} %pad_add_fusion.sc, ...), custom_call_target="tpu_custom_call" | custom-call | tf_op jit(solution)/shard_map/forward_own/pallas_call | solution.py:146
  116.1 13.4 %backward_0.1 = (bf16[1024,2048]{1,0:T(8,128)(2,1)}, bf16[1024,2048]{1,0:T(8,128)(2,1)}, f32[8,144,128]{2,1,0:T(8,128)}) custom-call(s32[2]{0:T(128)} %pad_add_fusion.sc, bf16[1024,2048]{1,0:T(8,128)(2,1)} %bitcast.64, bf16[512,2048]{1,0:T(8,128)(2,1)} %w.1, ...), custom_call_target="tpu_custom_call", output_to_operand_aliasing={{0}: (10, {}), {1}: (11, {}), {2}: (12, {})} | custom-call | tf_op jit(solution)/shard_map/backward_0/pallas_call | solution.py:244
  129.5 13.7 %backward_2.1 = (bf16[1024,2048]{1,0:T(8,128)(2,1)}, bf16[1024,2048]{1,0:T(8,128)(2,1)}, f32[8,144,128]{2,1,0:T(8,128)}) custom-call(s32[2]{0:T(128)} %pad_add_fusion.sc, bf16[1024,2048]{1,0:T(8,128)(2,1)} %bitcast.65, bf16[512,2048]{1,0:T(8,128)(2,1)} %collective-permute-done.w, ...), custom_call_target="tpu_custom_call", output_to_operand_aliasing={{0}: (10, {}), {1}: (11, {}), {2}: (12, {})} | custom-call | tf_op jit(solution)/shard_map/backward_2/pallas_call | solution.py:244
  143.2 13.7 %backward_3.1 = (bf16[1024,2048]{1,0:T(8,128)(2,1)}, bf16[1024,2048]{1,0:T(8,128)(2,1)}, f32[8,144,128]{2,1,0:T(8,128)}) custom-call(s32[2]{0:T(128)} %pad_add_fusion.sc, bf16[1024,2048]{1,0:T(8,128)(2,1)} %bitcast.66, bf16[512,2048]{1,0:T(8,128)(2,1)} %collective-permute-done.1.w, ...), custom_call_target="tpu_custom_call", output_to_operand_aliasing={{0}: (10, {}), {1}: (11, {}), {2}: (12, {})} | custom-call | tf_op jit(solution)/shard_map/backward_3/pallas_call | solution.py:244
  156.9 1.1 constant_dynamic-slice_fusion.3
  158.6 1.2 collective-permute-done.14
  159.8 1.0 dynamic-slice_add_fusion
  160.8 1.8 collective-permute-start.15
  162.6 4.4 %collective-permute-done.15 = f32[288,128]{1,0:T(8,128)S(1)} collective-permute-done((f32[288,128]{1,0:T(8,128)S(1)}, f32[288,128]{1,0:T(8,128)S(1)}, u32[]{:S(2)}, u32[]{:S(2)}) %collective-permute-start.15) | collective-permute-done | bytes 147488 | tf_op jit(solution)/shard_map/ppermute | solution.py:25
  167.0 1.8 collective-permute-start.16
  169.1 2.9 collective-permute-done.16
  172.0 2.1 collective-permute-start.17
  174.2 2.2 collective-permute-done.17
  176.5 3.0 %collective-permute-start.18 = (f32[72,128]{1,0:T(8,128)S(1)}, f32[72,128]{1,0:T(8,128)S(1)}, u32[]{:S(2)}, u32[]{:S(2)}) collective-permute-start(f32[72,128]{1,0:T(8,128)S(1)} %dynamic-slice_add_fusion.3), channel_id=1, source_target_pairs={{0,16},{1,17},{2,18},{3,19},{4,20},{5,21},{6,22},{7,23},{8,24},{9,... | collective-permute-start | bytes 110600 | tf_op jit(solution)/shard_map/ppermute | solution.py:25
  179.5 16.4 %collective-permute-done.18 = f32[72,128]{1,0:T(8,128)S(1)} collective-permute-done((f32[72,128]{1,0:T(8,128)S(1)}, f32[72,128]{1,0:T(8,128)S(1)}, u32[]{:S(2)}, u32[]{:S(2)}) %collective-permute-start.18) | collective-permute-done | bytes 36896 | tf_op jit(solution)/shard_map/ppermute | solution.py:25
  195.9 5.0 %collective-permute-start.19 = (f32[72,128]{1,0:T(8,128)S(1)}, f32[72,128]{1,0:T(8,128)S(1)}, u32[]{:S(2)}, u32[]{:S(2)}) collective-permute-start(f32[72,128]{1,0:T(8,128)S(1)} %add.88), channel_id=1, source_target_pairs={{0,8},{1,9},{2,10},{3,11},{4,12},{5,13},{6,14},{7,15},{8,0},{9,1},... | collective-permute-start | bytes 110600 | tf_op jit(solution)/shard_map/ppermute | solution.py:25
  200.9 2.2 collective-permute-done.19
  203.1 1.7 collective-permute-start.20
  205.3 2.1 collective-permute-start.5
  207.4 1.6 add_convert_fusion
  209.0 0.8 slice_bitcast_fusion
  210.4 0.9 broadcast_select_fusion.6
  211.3 3.3 %collective-permute-done.5 = bf16[2,2,64,1024]{3,2,1,0:T(8,128)(2,1)S(1)} collective-permute-done((bf16[2,2,64,1024]{3,2,1,0:T(8,128)(2,1)S(1)}, bf16[2,2,64,1024]{3,2,1,0:T(8,128)(2,1)S(1)}, u32[]{:S(2)}, u32[]{:S(2)}) %collective-permute-start.5) | collective-permute-done | bytes 524320 | tf_op jit(solution)/shard_map/ppermute | solution.py:25
  214.8 4.6 %collective-permute-done.7 = bf16[2,2,64,1024]{3,2,1,0:T(8,128)(2,1)} collective-permute-done((bf16[2,2,64,1024]{3,2,1,0:T(8,128)(2,1)}, bf16[2,2,64,1024]{3,2,1,0:T(8,128)(2,1)}, u32[]{:S(2)}, u32[]{:S(2)}) %collective-permute-start.7) | collective-permute-done | bytes 524320 | tf_op jit(solution)/shard_map/ppermute | solution.py:25
  219.4 1.2 fusion.4
  220.7 1.6 collective-permute-start.8
  222.2 0.6 collective-permute-start.21
  222.8 8.8 %collective-permute-done.21 = f32[288,128]{1,0:T(8,128)S(1)} collective-permute-done((f32[288,128]{1,0:T(8,128)S(1)}, f32[288,128]{1,0:T(8,128)S(1)}, u32[]{:S(2)}, u32[]{:S(2)}) %collective-permute-start.21) | collective-permute-done | bytes 147488 | tf_op jit(solution)/shard_map/ppermute | solution.py:25
  232.4 0.9 collective-permute-done.22
  233.3 25.1 %collective-permute-done.9 = bf16[2,2,64,1024]{3,2,1,0:T(8,128)(2,1)S(1)} collective-permute-done((bf16[2,2,64,1024]{3,2,1,0:T(8,128)(2,1)S(1)}, bf16[2,2,64,1024]{3,2,1,0:T(8,128)(2,1)S(1)}, u32[]{:S(2)}, u32[]{:S(2)}) %collective-permute-start.9) | collective-permute-done | bytes 524320 | tf_op jit(solution)/shard_map/ppermute | solution.py:25
  259.1 0.6 collective-permute-start.10
  259.9 6.8 %collective-permute-done.12 = bf16[2,64,1024]{2,1,0:T(8,128)(2,1)S(1)} collective-permute-done((bf16[2,64,1024]{2,1,0:T(8,128)(2,1)S(1)}, bf16[2,64,1024]{2,1,0:T(8,128)(2,1)S(1)}, u32[]{:S(2)}, u32[]{:S(2)}) %collective-permute-start.12) | collective-permute-done | bytes 262176 | tf_op jit(solution)/shard_map/ppermute | solution.py:25
  266.7 0.6 collective-permute-start.13
  267.3 1.6 collective-permute-start.11
  269.0 1.3 copy.38
  270.4 0.6 fusion.7
  271.0 8.5 %collective-permute-done.13 = bf16[4,64,1024]{2,1,0:T(8,128)(2,1)} collective-permute-done((bf16[4,64,1024]{2,1,0:T(8,128)(2,1)S(1)}, bf16[4,64,1024]{2,1,0:T(8,128)(2,1)}, u32[]{:S(2)}, u32[]{:S(2)}) %collective-permute-start.13) | collective-permute-done | bytes 524320 | tf_op jit(solution)/shard_map/ppermute | solution.py:25
  279.5 2.1 pad_maximum_fusion.1.b
  281.6 2.1 pad_maximum_fusion.a
  283.7 6.9 %assemble.1 = f32[512,2048]{1,0:T(8,128)} custom-call(s32[2]{0:T(128)} %pad_add_fusion.sc, bf16[8,64,1024]{2,1,0:T(8,128)(2,1)} %pad_maximum_fusion.a, bf16[8,64,1024]{2,1,0:T(8,128)(2,1)} %pad_maximum_fusion.1.b), custom_call_target="tpu_custom_call" | custom-call | tf_op jit(solution)/shard_map/assemble/pallas_call | solution.py:286
  (60 shorter events, 4.8 us)
Async XLA Ops:
  3.6 23.5 %copy-start = (bf16[512,2048]{1,0:T(8,128)(2,1)S(1)}, bf16[512,2048]{1,0:T(8,128)(2,1)}, u32[]{:S(2)}) copy-start(bf16[512,2048]{1,0:T(8,128)(2,1)} %w.1) | copy-start | bytes 6291460
  26.5 63.7 %collective-permute-start.2 = (bf16[2,512,2048]{2,1,0:T(8,128)(2,1)}, bf16[2,512,2048]{2,1,0:T(8,128)(2,1)}, u32[]{:S(2)}, u32[]{:S(2)}) collective-permute-start(bf16[2,512,2048]{2,1,0:T(8,128)(2,1)} %get-tuple-element.36), channel_id=1, source_target_pairs={{0,1},{1,0},{2,3},{3,2},{4,5},{5,4},{6,7},{7,6},{8,9},{9,8},{10,11... | collective-permute-start | bytes 12582920 | tf_op jit(solution)/shard_map/ppermute | solution.py:25
  27.1 48.9 %collective-permute-start = (bf16[512,2048]{1,0:T(8,128)(2,1)S(1)}, bf16[512,2048]{1,0:T(8,128)(2,1)}, u32[]{:S(2)}, u32[]{:S(2)}) collective-permute-start(bf16[512,2048]{1,0:T(8,128)(2,1)S(1)} %copy-done), channel_id=1, source_target_pairs={{0,2},{1,3},{2,0},{3,1},{4,6},{5,7},{6,4},{7,5},{8,10},{9,11},{10,... | collective-permute-start | bytes 6291464 | tf_op jit(solution)/shard_map/ppermute | solution.py:25
  29.7 47.2 %collective-permute-start.3 = (bf16[512,2048]{1,0:T(8,128)(2,1)S(1)}, bf16[512,2048]{1,0:T(8,128)(2,1)}, u32[]{:S(2)}, u32[]{:S(2)}) collective-permute-start(bf16[512,2048]{1,0:T(8,128)(2,1)S(1)} %copy-done), channel_id=1, source_target_pairs={{0,1},{1,0},{2,3},{3,2},{4,5},{5,4},{6,7},{7,6},{8,9},{9,8},{10,11... | collective-permute-start | bytes 6291464 | tf_op jit(solution)/shard_map/ppermute | solution.py:25
  76.0 67.2 %collective-permute-start.1 = (bf16[512,2048]{1,0:T(8,128)(2,1)}, bf16[512,2048]{1,0:T(8,128)(2,1)}, u32[]{:S(2)}, u32[]{:S(2)}) collective-permute-start(bf16[512,2048]{1,0:T(8,128)(2,1)} %collective-permute-done.w), channel_id=1, source_target_pairs={{0,1},{1,0},{2,3},{3,2},{4,5},{5,4},{6,7},{7,6},{8,9},{9,8},{10,11... | collective-permute-start | bytes 6291464 | tf_op jit(solution)/shard_map/ppermute | solution.py:25
  156.9 47.9 %copy-start.2 = (bf16[2,256,1024]{2,1,0:T(8,128)(2,1)S(1)}, bf16[2,256,1024]{2,1,0:T(8,128)(2,1)}, u32[]{:S(2)}) copy-start(bf16[2,256,1024]{2,1,0:T(8,128)(2,1)} %get-tuple-element.52) | copy-start | bytes 3145732
  158.0 1.8 collective-permute-start.14
  160.8 6.2 %collective-permute-start.15 = (f32[288,128]{1,0:T(8,128)S(1)}, f32[288,128]{1,0:T(8,128)S(1)}, u32[]{:S(2)}, u32[]{:S(2)}) collective-permute-start(f32[288,128]{1,0:T(8,128)S(1)} %constant_dynamic-slice_fusion.2), channel_id=1, source_target_pairs={{0,2},{1,3},{2,0},{3,1},{4,6},{5,7},{6,4},{7,5},{8,10},{9,11},{10,... | collective-permute-start | bytes 442376 | tf_op jit(solution)/shard_map/ppermute | solution.py:25
  167.0 5.0 %collective-permute-start.16 = (f32[144,128]{1,0:T(8,128)S(1)}, f32[144,128]{1,0:T(8,128)S(1)}, u32[]{:S(2)}, u32[]{:S(2)}) collective-permute-start(f32[144,128]{1,0:T(8,128)S(1)} %constant_dynamic-slice_fusion.1), channel_id=1, source_target_pairs={{0,4},{1,5},{2,6},{3,7},{4,0},{5,1},{6,2},{7,3},{8,12},{9,13},{10,... | collective-permute-start | bytes 221192 | tf_op jit(solution)/shard_map/ppermute | solution.py:25
  168.9 36.0 %collective-permute-start.4 = (bf16[2,256,1024]{2,1,0:T(8,128)(2,1)}, bf16[2,256,1024]{2,1,0:T(8,128)(2,1)S(1)}, u32[]{:S(2)}, u32[]{:S(2)}) collective-permute-start(bf16[2,256,1024]{2,1,0:T(8,128)(2,1)} %get-tuple-element.53), channel_id=1, source_target_pairs={{0,4},{1,5},{2,6},{3,7},{4,0},{5,1},{6,2},{7,3},{8,12},{9,13},{10,... | collective-permute-start | bytes 3145736 | tf_op jit(solution)/shard_map/ppermute | solution.py:25
  172.0 4.5 %collective-permute-start.17 = (f32[72,128]{1,0:T(8,128)S(1)}, f32[72,128]{1,0:T(8,128)S(1)}, u32[]{:S(2)}, u32[]{:S(2)}) collective-permute-start(f32[72,128]{1,0:T(8,128)S(1)} %constant_dynamic-slice_fusion), channel_id=1, source_target_pairs={{0,8},{1,9},{2,10},{3,11},{4,12},{5,13},{6,14},{7,15},{8,0},{9,1},... | collective-permute-start | bytes 110600 | tf_op jit(solution)/shard_map/ppermute | solution.py:25
  174.2 33.3 %collective-permute-start.6 = (bf16[2,256,1024]{2,1,0:T(8,128)(2,1)}, bf16[2,256,1024]{2,1,0:T(8,128)(2,1)}, u32[]{:S(2)}, u32[]{:S(2)}) collective-permute-start(bf16[2,256,1024]{2,1,0:T(8,128)(2,1)} %get-tuple-element.55), channel_id=1, source_target_pairs={{0,8},{1,9},{2,10},{3,11},{4,12},{5,13},{6,14},{7,15},{8,0},{9,1},... | collective-permute-start | bytes 3145736 | tf_op jit(solution)/shard_map/ppermute | solution.py:25
  176.5 19.4 %collective-permute-start.18 = (f32[72,128]{1,0:T(8,128)S(1)}, f32[72,128]{1,0:T(8,128)S(1)}, u32[]{:S(2)}, u32[]{:S(2)}) collective-permute-start(f32[72,128]{1,0:T(8,128)S(1)} %dynamic-slice_add_fusion.3), channel_id=1, source_target_pairs={{0,16},{1,17},{2,18},{3,19},{4,20},{5,21},{6,22},{7,23},{8,24},{9,... | collective-permute-start | bytes 110600 | tf_op jit(solution)/shard_map/ppermute | solution.py:25
  195.9 7.2 %collective-permute-start.19 = (f32[72,128]{1,0:T(8,128)S(1)}, f32[72,128]{1,0:T(8,128)S(1)}, u32[]{:S(2)}, u32[]{:S(2)}) collective-permute-start(f32[72,128]{1,0:T(8,128)S(1)} %add.88), channel_id=1, source_target_pairs={{0,8},{1,9},{2,10},{3,11},{4,12},{5,13},{6,14},{7,15},{8,0},{9,1},... | collective-permute-start | bytes 110600 | tf_op jit(solution)/shard_map/ppermute | solution.py:25
  203.1 7.3 %collective-permute-start.20 = (f32[144,128]{1,0:T(8,128)S(1)}, f32[144,128]{1,0:T(8,128)}, u32[]{:S(2)}, u32[]{:S(2)}) collective-permute-start(f32[144,128]{1,0:T(8,128)S(1)} %pad_maximum_fusion.9), channel_id=1, source_target_pairs={{0,4},{1,5},{2,6},{3,7},{4,0},{5,1},{6,2},{7,3},{8,12},{9,13},{10,... | collective-permute-start | bytes 221192 | tf_op jit(solution)/shard_map/ppermute | solution.py:25
  204.8 2.6 copy-start.1
  205.3 9.2 %collective-permute-start.5 = (bf16[2,2,64,1024]{3,2,1,0:T(8,128)(2,1)S(1)}, bf16[2,2,64,1024]{3,2,1,0:T(8,128)(2,1)S(1)}, u32[]{:S(2)}, u32[]{:S(2)}) collective-permute-start(bf16[2,2,64,1024]{3,2,1,0:T(8,128)(2,1)S(1)} %slice_bitcast_fusion.2), channel_id=1, source_target_pairs={{0,8},{1,9},{2,10},{3,11},{4,12},{5,13},{6,14},{7,15},{8,0},{9,1},... | collective-permute-start | bytes 1572872 | tf_op jit(solution)/shard_map/ppermute | solution.py:25
  209.9 9.5 %collective-permute-start.7 = (bf16[2,2,64,1024]{3,2,1,0:T(8,128)(2,1)}, bf16[2,2,64,1024]{3,2,1,0:T(8,128)(2,1)}, u32[]{:S(2)}, u32[]{:S(2)}) collective-permute-start(bf16[2,2,64,1024]{3,2,1,0:T(8,128)(2,1)} %slice_bitcast_fusion), channel_id=1, source_target_pairs={{0,4},{1,5},{2,6},{3,7},{4,0},{5,1},{6,2},{7,3},{8,12},{9,13},{10,... | collective-permute-start | bytes 1572872 | tf_op jit(solution)/shard_map/ppermute | solution.py:25
  220.7 11.1 %collective-permute-start.8 = (bf16[1,2,2,64,1024]{4,3,2,1,0:T(8,128)(2,1)S(1)}, bf16[1,2,2,64,1024]{4,3,2,1,0:T(8,128)(2,1)S(1)}, u32[]{:S(2)}, u32[]{:S(2)}) collective-permute-start(bf16[1,2,2,64,1024]{4,3,2,1,0:T(8,128)(2,1)S(1)} %pad_maximum_fusion.4), channel_id=1, source_target_pairs={{0,2},{1,3},{2,0},{3,1},{4,6},{5,7},{6,4},{7,5},{8,10},{9,11},{10,... | collective-permute-start | bytes 1572872 | tf_op jit(solution)/shard_map/ppermute | solution.py:25
  222.2 9.4 %collective-permute-start.21 = (f32[288,128]{1,0:T(8,128)S(1)}, f32[288,128]{1,0:T(8,128)S(1)}, u32[]{:S(2)}, u32[]{:S(2)}) collective-permute-start(f32[288,128]{1,0:T(8,128)S(1)} %pad_maximum_fusion.8), channel_id=1, source_target_pairs={{0,2},{1,3},{2,0},{3,1},{4,6},{5,7},{6,4},{7,5},{8,10},{9,11},{10,... | collective-permute-start | bytes 442376 | tf_op jit(solution)/shard_map/ppermute | solution.py:25
  231.7 1.6 collective-permute-start.22
  231.9 26.5 %collective-permute-start.9 = (bf16[2,2,64,1024]{3,2,1,0:T(8,128)(2,1)S(1)}, bf16[2,2,64,1024]{3,2,1,0:T(8,128)(2,1)S(1)}, u32[]{:S(2)}, u32[]{:S(2)}) collective-permute-start(bf16[2,2,64,1024]{3,2,1,0:T(8,128)(2,1)S(1)} %fusion.2), channel_id=1, source_target_pairs={{0,16},{1,17},{2,18},{3,19},{4,20},{5,21},{6,22},{7,23},{8,24},{9,... | collective-permute-start | bytes 1572872 | tf_op jit(solution)/shard_map/ppermute | solution.py:25
  258.7 7.9 %collective-permute-start.12 = (bf16[2,64,1024]{2,1,0:T(8,128)(2,1)S(1)}, bf16[2,64,1024]{2,1,0:T(8,128)(2,1)S(1)}, u32[]{:S(2)}, u32[]{:S(2)}) collective-permute-start(bf16[2,64,1024]{2,1,0:T(8,128)(2,1)S(1)} %get-tuple-element.59), channel_id=1, source_target_pairs={{0,8},{1,9},{2,10},{3,11},{4,12},{5,13},{6,14},{7,15},{8,0},{9,1},... | collective-permute-start | bytes 786440 | tf_op jit(solution)/shard_map/ppermute | solution.py:25
  259.1 8.2 %collective-permute-start.10 = (bf16[2,64,1024]{2,1,0:T(8,128)(2,1)S(1)}, bf16[2,64,1024]{2,1,0:T(8,128)(2,1)S(1)}, u32[]{:S(2)}, u32[]{:S(2)}) collective-permute-start(bf16[2,64,1024]{2,1,0:T(8,128)(2,1)S(1)} %get-tuple-element.60), channel_id=1, source_target_pairs={{0,4},{1,5},{2,6},{3,7},{4,0},{5,1},{6,2},{7,3},{8,12},{9,13},{10,... | collective-permute-start | bytes 786440 | tf_op jit(solution)/shard_map/ppermute | solution.py:25
  266.7 12.8 %collective-permute-start.13 = (bf16[4,64,1024]{2,1,0:T(8,128)(2,1)S(1)}, bf16[4,64,1024]{2,1,0:T(8,128)(2,1)}, u32[]{:S(2)}, u32[]{:S(2)}) collective-permute-start(bf16[4,64,1024]{2,1,0:T(8,128)(2,1)S(1)} %pad_maximum_fusion.6), channel_id=1, source_target_pairs={{0,4},{1,5},{2,6},{3,7},{4,0},{5,1},{6,2},{7,3},{8,12},{9,13},{10,... | collective-permute-start | bytes 1572872 | tf_op jit(solution)/shard_map/ppermute | solution.py:25
  267.3 14.3 %collective-permute-start.11 = (bf16[4,64,1024]{2,1,0:T(8,128)(2,1)S(1)}, bf16[4,64,1024]{2,1,0:T(8,128)(2,1)}, u32[]{:S(2)}, u32[]{:S(2)}) collective-permute-start(bf16[4,64,1024]{2,1,0:T(8,128)(2,1)S(1)} %pad_maximum_fusion.5), channel_id=1, source_target_pairs={{0,8},{1,9},{2,10},{3,11},{4,12},{5,13},{6,14},{7,15},{8,0},{9,1},... | collective-permute-start | bytes 1572872 | tf_op jit(solution)/shard_map/ppermute | solution.py:25

commit v2 on v1

v2 whole, which is shorter than its diff:
```python
import functools

import jax
import jax.numpy as jnp
from jax import lax
from jax.experimental import pallas as pl
from jax.experimental.pallas import tpu as pltpu
from jax.sharding import PartitionSpec as P


EPS = 1e-05
K0 = 0.7978845608028654
K1 = 0.044715
VMEM = 18 << 20
AXES = ("sp", "dp")
bf16 = jnp.bfloat16
f32 = jnp.float32


def swap(value, bit_sp, bit_dp):
    num_sp, num_dp = lax.axis_size("sp"), lax.axis_size("dp")
    pairs = [
        (s * num_dp + d, (s ^ bit_sp) * num_dp + (d ^ bit_dp))
        for s in range(num_sp)
        for d in range(num_dp)
    ]
    return lax.ppermute(value, AXES, pairs)


def dot(a, b, dims):
    return lax.dot_general(a, b, (dims, ((), ())), preferred_element_type=f32)


def forward_kernel(cfg, sc, u, v, d_out, w_mix, bias, gain, shift, *rest):
    span, chans, per, piece, inner, fused = cfg
    if fused:
        recv, s1, k1, s2, k2, upper_o, m1_o, scaled_o, w1_o, gated, wide = rest
    else:
        part, upper_o, m1_o, scaled_o, w1_o, gated, wide = rest
    blocks = u.shape[0] // span

    row = lax.broadcasted_iota(jnp.int32, (span, span), 0)
    col = lax.broadcasted_iota(jnp.int32, (span, span), 1)
    for g in range(per):
        lanes = slice(g * chans, (g + 1) * chans)
        for b in range(blocks):
            rows = slice(b * span, (b + 1) * span)
            c = v[rows, lanes].astype(f32)
            c2 = c * c
            tv = jnp.tanh(c * (K0 + (K0 * K1) * c2))
            hv = 0.5 + 0.5 * tv
            gate = c * hv
            dv = hv + (c * (0.5 - 0.5 * tv * tv)) * (K0 + (3.0 * K0 * K1) * c2)
            centre = gate - jnp.mean(gate, axis=1, keepdims=True)
            var = jnp.mean(centre * centre, axis=1, keepdims=True)
            inv = lax.rsqrt(var + EPS)
            scaled = centre * inv
            wide[:, b * chans : (b + 1) * chans] = (scaled * gain[g] + shift[g]).astype(bf16)
            scaled_o[rows, lanes] = scaled.astype(bf16)
            w1_o[rows, lanes] = (dv * inv).astype(bf16)
        w_low = jnp.where(row >= col, w_mix[g], jnp.zeros_like(w_mix[g]))
        mixed_all = dot(w_low, wide[...], ((1,), (0,)))
        offset = jnp.transpose(jnp.broadcast_to(bias[g], (chans, span)))
        for b in range(blocks):
            rows = slice(b * span, (b + 1) * span)
            a = u[rows, lanes].astype(f32)
            mixed = mixed_all[:, b * chans : (b + 1) * chans] + offset
            a2 = a * a
            tu = jnp.tanh(a * (K0 + (K0 * K1) * a2))
            hu = 0.5 + 0.5 * tu
            up = a * hu
            du = hu + (a * (0.5 - 0.5 * tu * tu)) * (K0 + (3.0 * K0 * K1) * a2)
            gated[rows, lanes] = (up * mixed).astype(bf16)
            upper_o[rows, lanes] = up.astype(bf16)
            m1_o[rows, lanes] = (mixed * du).astype(bf16)
    if not fused:
        part[0] = dot(gated[...], d_out[...], ((0,), (0,))).astype(bf16)
        return
    half = d_out.shape[1] // 2
    count = per * chans // piece
    for side, (send, keep) in enumerate(((s1, k1), (s2, k2))):
        lanes = slice(side * half, (side + 1) * half)
        total = dot(gated[...], d_out[:, lanes], ((0,), (0,)))
        for p in range(count):
            rows = slice(p * piece, (p + 1) * piece)
            value = (total[rows] + recv[0, rows, lanes].astype(f32)).astype(bf16)
            rel = jnp.bitwise_xor(p, sc[1] % inner)
            low, high = rel % 2, rel // 2
            if side == 0:
                flag, at = low, high
            else:
                flag, at = high % 2, (high // 2) * 2 + low
            where = pl.ds(pl.multiple_of(at * piece, piece), piece)

            @pl.when(flag == 1)
            def _():
                send[0, where, :] = value

            @pl.when(flag == 0)
            def _():
                keep[0, where, :] = value


def forward(sc, first, count, u, v, d_out, w_mix, bias, gain, shift, recv):
    num_sp, num_dp = lax.axis_size("sp"), lax.axis_size("dp")
    length, width = u.shape
    groups, span, _ = w_mix.shape
    chans = width // groups
    rows = width // num_dp
    per = 2
    chunk = per * chans
    steps = rows // chunk
    piece = rows // num_sp
    inner = chunk // piece
    fused = recv is not None

    def at(i, j, sc):
        return jnp.bitwise_xor(first - 2 * i, sc[0]) * steps + j

    wide = pl.BlockSpec((length, chunk), lambda i, j, sc: (0, at(i, j, sc)))
    vec = pl.BlockSpec((per, 1, span), lambda i, j, sc: (at(i, j, sc), 0, 0))
    in_specs = [
        wide,
        wide,
        pl.BlockSpec(memory_space=pltpu.VMEM),
        pl.BlockSpec((per, span, span), lambda i, j, sc: (at(i, j, sc), 0, 0)),
        vec,
        vec,
        vec,
    ]
    args = [u, v, d_out, w_mix, bias, gain, shift]
    save = pl.BlockSpec((length, chunk), lambda i, j, sc: (0, i * steps + j))
    save_shape = jax.ShapeDtypeStruct((length, count * rows), bf16)
    depth = d_out.shape[1]
    if fused:
        in_specs.append(pl.BlockSpec((1, chunk, depth), lambda i, j, sc: (i, j, 0)))
        args.append(recv)
        spec = pl.BlockSpec(
            (1, chunk // 2, depth // 2),
            lambda i, j, sc: (i, jnp.bitwise_xor(j, sc[1] // inner), 0),
        )
        heads = [spec] * 4
        shapes = [jax.ShapeDtypeStruct((count, rows // 2, depth // 2), bf16)] * 4
    else:
        heads = [pl.BlockSpec((1, chunk, depth), lambda i, j, sc: (i, j, 0))]
        shapes = [jax.ShapeDtypeStruct((count, rows, depth), bf16)]
    return pl.pallas_call(
        functools.partial(forward_kernel, (span, chans, per, piece, inner, fused)),
        grid_spec=pltpu.PrefetchScalarGridSpec(
            num_scalar_prefetch=1,
            grid=(count, steps),
            in_specs=in_specs,
            out_specs=heads + [save] * 4,
            scratch_shapes=[
                pltpu.VMEM((length, chunk), bf16),
                pltpu.VMEM((span, length // span * chans), bf16),
            ],
        ),
        out_shape=shapes + [save_shape] * 4,
        cost_estimate=pl.CostEstimate(
            flops=2 * length * rows * count * depth, transcendentals=0, bytes_accessed=0
        ),
        compiler_params=pltpu.CompilerParams(vmem_limit_bytes=VMEM),
    )(sc, *args)


LINES = 16


def encode(ref, at, square, lines):
    span = square.shape[0]
    high = lines.astype(bf16)
    ref[at, :span] = square.astype(bf16)
    ref[at, span : span + LINES] = high
    ref[at, span + LINES :] = (lines - high.astype(f32)).astype(bf16)


def decode(ref, at):
    span = ref.shape[1] - 2 * LINES
    high = ref[at, span : span + LINES].astype(f32)
    return ref[at, :span].astype(f32), high + ref[at, span + LINES :].astype(f32)


def backward_kernel(cfg, sc, d_out, w, upper, m1, scaled_i, w1, w_mix, gain, shift, *rest):
    span, chans, per = cfg
    gu, gv, small, grad, dm_all, nm_all = rest[-6:]
    blocks = upper.shape[0] // span
    row = lax.broadcasted_iota(jnp.int32, (span, span), 0)
    col = lax.broadcasted_iota(jnp.int32, (span, span), 1)
    w_low = [jnp.where(row >= col, w_mix[g], jnp.zeros_like(w_mix[g])) for g in range(per)]
    nm_all[:, span:, :] = jnp.ones((per, span, nm_all.shape[2]), bf16)
    parts = 2
    acc = [None] * per
    acc_g = [jnp.zeros((8, chans), f32)] * per
    acc_s = [jnp.zeros((8, chans), f32)] * per
    size = blocks // parts
    for h in range(parts):
        grad[h * size * span : (h + 1) * size * span] = dot(d_out[h * size * span : (h + 1) * size * span], w[...], ((1,), (1,))).astype(bf16)
    for h in range(parts):
        wide = slice(h * size * chans, (h + 1) * size * chans)
        for g in range(per):
            lanes = slice(g * chans, (g + 1) * chans)
            for b in range(h * size, (h + 1) * size):
                rows = slice(b * span, (b + 1) * span)
                at = slice(b * chans, (b + 1) * chans)
                cot = grad[rows, lanes].astype(f32)
                gu[rows, lanes] = (cot * m1[rows, lanes].astype(f32)).astype(bf16)
                dm_all[g, :, at] = (cot * upper[rows, lanes].astype(f32)).astype(bf16)
                scaled = scaled_i[rows, lanes].astype(f32)
                nm_all[g, :span, at] = (scaled * gain[g] + shift[g]).astype(bf16)
            both = dot(dm_all[g, :, wide], nm_all[g, :, wide], ((1,), (1,)))
            acc[g] = both if h == 0 else acc[g] + both
            dn_all = dot(w_low[g], dm_all[g, :, wide], ((0,), (0,)))
            for b in range(h * size, (h + 1) * size):
                rows = slice(b * span, (b + 1) * span)
                k = b - h * size
                dn = dn_all[:, k * chans : (k + 1) * chans]
                scaled = scaled_i[rows, lanes].astype(f32)
                prod = dn * scaled
                acc_g[g] = acc_g[g] + jnp.sum(prod.reshape(-1, 8, chans), axis=0)
                acc_s[g] = acc_s[g] + jnp.sum(dn.reshape(-1, 8, chans), axis=0)
                e = dn * gain[g]
                mean_e = jnp.mean(e, axis=1, keepdims=True)
                mean_s = jnp.mean(prod * gain[g], axis=1, keepdims=True)
                gv[rows, lanes] = (
                    w1[rows, lanes].astype(f32) * (e - mean_e - scaled * mean_s)
                ).astype(bf16)
    lines, mats = [], []
    for g in range(per):
        mats.append(acc[g][:, :span])
        lines.append(jnp.transpose(acc[g][:, span:])[:1])
        lines.append(jnp.sum(acc_g[g], axis=0, keepdims=True))
        lines.append(jnp.sum(acc_s[g], axis=0, keepdims=True))
    even, odd = mats
    diag = jnp.sum(jnp.where(row == col, odd, 0.0), axis=0, keepdims=True)
    square = jnp.where(row >= col, even, jnp.transpose(odd))
    pad = jnp.zeros((LINES - 7, span), f32)
    lines = jnp.concatenate(lines + [diag, pad], axis=0)
    encode(small, 0, square, lines)


def backward(sc, rel, index, d_out, w, saves, w_mix, gain, shift, carried):
    num_dp = lax.axis_size("dp")
    length, depth = d_out.shape
    groups, span, _ = w_mix.shape
    rows = w.shape[0]
    width = rows * num_dp
    chans = width // groups
    per = 2
    chunk = per * chans
    steps = rows // chunk

    def at(j, sc):
        return jnp.bitwise_xor(rel, sc[0]) * steps + j

    save = pl.BlockSpec((length, chunk), lambda j, sc: (0, index * steps + j))
    vec = pl.BlockSpec((per, 1, span), lambda j, sc: (at(j, sc), 0, 0))
    in_specs = [
        pl.BlockSpec(memory_space=pltpu.VMEM),
        pl.BlockSpec((chunk, depth), lambda j, sc: (j, 0)),
        save,
        save,
        save,
        save,
        pl.BlockSpec((per, span, span), lambda j, sc: (at(j, sc), 0, 0)),
        vec,
        vec,
    ]
    args = [d_out, w, *saves, w_mix, gain, shift]
    aliases = {}
    if carried is not None:
        for k, value in enumerate(carried):
            aliases[1 + len(args)] = k
            in_specs.append(pl.BlockSpec(memory_space=pl.ANY))
            args.append(value)
    out = pl.BlockSpec((length, chunk), lambda j, sc: (0, at(j, sc)))
    shape = jax.ShapeDtypeStruct((length, width), bf16)
    return pl.pallas_call(
        functools.partial(backward_kernel, (span, chans, per)),
        grid_spec=pltpu.PrefetchScalarGridSpec(
            num_scalar_prefetch=1,
            grid=(steps,),
            in_specs=in_specs,
            out_specs=[
                out,
                out,
                pl.BlockSpec((1, span + 2 * LINES, span), lambda j, sc: (j, 0, 0)),
            ],
            scratch_shapes=[
                pltpu.VMEM((length, chunk), bf16),
                pltpu.VMEM((per, span, length // span * chans), bf16),
                pltpu.VMEM((per, 2 * span, length // span * chans), bf16),
            ],
        ),
        out_shape=[
            shape,
            shape,
            jax.ShapeDtypeStruct((steps, span + 2 * LINES, span), bf16),
        ],
        input_output_aliases=aliases,
        cost_estimate=pl.CostEstimate(
            flops=2 * length * rows * depth, transcendentals=0, bytes_accessed=0
        ),
        compiler_params=pltpu.CompilerParams(vmem_limit_bytes=VMEM),
    )(sc, *args)


def add(a, b):
    return (a.astype(f32) + b.astype(f32)).astype(bf16)


def split_kernel(k1, r1, k2, r2, send1, keep1, send2, keep2):
    for k, r, send, keep in ((k1, r1, send1, keep1), (k2, r2, send2, keep2)):
        for i in range(k.shape[0]):
            for j in range(k.shape[1]):
                send[i, j] = add(k[i, j, 1], r[i, j, 1])
                keep[i, j] = add(k[i, j, 0], r[i, j, 0])


def join_kernel(k1, r1, k2, r2, out):
    out[:, 0] = add(k1[...], r1[...])
    out[:, 1] = add(k2[...], r2[...])


def join_more_kernel(k1, r1, k2, r2, more, out):
    for side, (k, r) in enumerate(((k1, r1), (k2, r2))):
        total = k[...].astype(f32) + r[...].astype(f32)
        out[:, side] = (total + more[:, side].astype(f32)).astype(bf16)


def merge_kernel(mine, got, out):
    for i in range(mine.shape[0]):
        square, lines = decode(mine, i)
        more, extra = decode(got, i)
        encode(out, i, square + more, lines + extra)


def unpack_kernel(sc, *refs):
    *blocks, grad_w, bias, gain, shift = refs
    steps = blocks[0].shape[0]
    span = blocks[0].shape[2]
    row = lax.broadcasted_iota(jnp.int32, (span, span), 0)
    col = lax.broadcasted_iota(jnp.int32, (span, span), 1)
    for rel, block in enumerate(blocks):
        base = jnp.bitwise_xor(rel, sc[0]) * (2 * steps)
        for j in range(steps):
            square, lines = decode(block, j)
            even = jnp.where(row >= col, square, 0.0)
            odd = jnp.where(row > col, jnp.transpose(square), 0.0)
            odd = jnp.where(row == col, jnp.broadcast_to(lines[6:7], (span, span)), odd)
            for g, value in enumerate((even, odd)):
                at = base + 2 * j + g
                grad_w[at] = value
                for k, ref in enumerate((bias, gain, shift)):
                    ref[pl.ds(at, 1), :] = lines[3 * g + k : 3 * g + k + 1]


def unpack(sc, blocks, groups):
    span = blocks[0].shape[2]
    whole = pl.BlockSpec(memory_space=pltpu.VMEM)
    line = jax.ShapeDtypeStruct((groups, span), f32)
    return pl.pallas_call(
        unpack_kernel,
        in_specs=[pl.BlockSpec(memory_space=pltpu.SMEM)] + [whole] * len(blocks),
        out_specs=[whole] * 4,
        out_shape=[jax.ShapeDtypeStruct((groups, span, span), f32), line, line, line],
        compiler_params=pltpu.CompilerParams(vmem_limit_bytes=VMEM),
        name="unpack",
    )(sc, *blocks)


def flip_kernel(step, value, got, *outs):
    for side in range(value.shape[0]):
        for j in range(value.shape[1]):
            sums = add(value[side, j], got[side, j ^ step])
            if len(outs) == 1:
                outs[0][side, j] = sums
            else:
                outs[side][j] = sums


def local(body, shapes, *args):
    return pl.pallas_call(
        body,
        out_shape=[jax.ShapeDtypeStruct(shape, bf16) for shape in shapes],
        in_specs=[pl.BlockSpec(memory_space=pltpu.VMEM)] * len(args),
        out_specs=[pl.BlockSpec(memory_space=pltpu.VMEM)] * len(shapes),
        compiler_params=pltpu.CompilerParams(vmem_limit_bytes=VMEM),
    )(*args)


def assemble_kernel(sc, *refs):
    *parts, out = refs
    half = parts[0].shape[-1]
    piece = parts[0].shape[1]
    for side in range(2):
        for low in range(4):
            at = jnp.bitwise_xor(low, jnp.bitwise_and(sc[1], 3)) * piece
            rows = pl.ds(pl.multiple_of(at, piece), piece)
            lanes = slice(side * half, (side + 1) * half)
            out[rows, lanes] = parts[4 * side + low][0].astype(f32)


def assemble(sc, parts):
    rest, piece, half = parts[0].shape
    spec = pl.BlockSpec((1, piece, half), lambda h, sc: (jnp.bitwise_xor(h, sc[1] // 4), 0, 0))
    return pl.pallas_call(
        assemble_kernel,
        grid_spec=pltpu.PrefetchScalarGridSpec(
            num_scalar_prefetch=1,
            grid=(rest,),
            in_specs=[spec] * 8,
            out_specs=pl.BlockSpec((4 * piece, 2 * half), lambda h, sc: (h, 0)),
        ),
        out_shape=jax.ShapeDtypeStruct((rest * 4 * piece, 2 * half), f32),
        name="assemble",
    )(sc, *parts)


def bits_of(count):
    return [1 << k for k in range(count.bit_length() - 1)]


def reduce_small(packed):
    sp_bits, dp_bits = bits_of(lax.axis_size("sp")), bits_of(lax.axis_size("dp"))
    for bit in [dp_bits[0]] + list(reversed(dp_bits[1:])):
        for rel in [r for r in packed if r & bit]:
            got = swap(packed.pop(rel), 0, bit)
            mine = packed[rel ^ bit]
            packed[rel ^ bit] = local(merge_kernel, [mine.shape], mine, got)[0]
    value = packed[0]
    for bit in sp_bits:
        value = local(merge_kernel, [value.shape], value, swap(value, bit, 0))[0]
    blocks = {0: value}
    for bit in dp_bits[1:] + [dp_bits[0]]:
        for rel in list(blocks):
            blocks[rel | bit] = swap(blocks[rel], 0, bit)
    return [blocks[rel] for rel in range(len(blocks))]


def program(u_pre, v_pre, d_out, w_mix, mix_bias, norm_gain, norm_shift, w_out):
    num_sp, num_dp = lax.axis_size("sp"), lax.axis_size("dp")
    shape = u_pre.shape
    width = shape[2]
    groups, _, _ = w_mix.shape
    u, v = u_pre.reshape(-1, width), v_pre.reshape(-1, width)
    d = d_out.reshape(-1, d_out.shape[2])
    sc = jnp.stack([lax.axis_index("dp"), lax.axis_index("sp")]).astype(jnp.int32)
    bias, gain, shift = (a[:, None, :] for a in (mix_bias, norm_gain, norm_shift))
    u, v, w_mix, bias, gain, shift = (
        pltpu.with_memory_space_constraint(a, pltpu.HBM) for a in (u, v, w_mix, bias, gain, shift)
    )

    sp_bits, dp_bits = bits_of(num_sp), bits_of(num_dp)
    bit_a, bit_b, others = sp_bits[0], sp_bits[1], sp_bits[2:]
    piece = width // num_dp // num_sp
    depth = d.shape[1]
    half = depth // 2
    rest = num_sp // 4
    count = num_dp // 4
    weights = {0: w_out, 1: swap(w_out, 0, 1)}
    for rel in range(2, num_dp, 2):
        top = 1 << (rel.bit_length() - 1)
        weights[rel] = swap(weights[rel - top], 0, top)
    for rel in range(2, num_dp, 2):
        weights[rel + 1] = swap(weights[rel], 0, 1)

    saves, heads = {}, {}

    def front(rel, recv):
        out = forward(sc, rel, count, u, v, d, w_mix, bias, gain, shift, recv)
        kept = out[-4:]
        for i in range(count):
            saves[rel - 2 * i] = (kept, i)
        heads[rel] = out[:-4]

    packed = {}

    def back(rel, carried):
        kept, i = saves[rel]
        *carried, packed[rel] = backward(
            sc, rel, i, d, weights[rel], kept, w_mix, gain, shift, carried
        )
        return carried

    top, low = num_dp - 1, num_dp // 2 - 1
    front(top, None)
    recv_a = swap(heads[top][0], 0, 1)
    front(low, None)
    recv_b = swap(heads[low][0], 0, 1)
    front(top - 1, recv_a)
    s1a, k1a, s2a, k2a = heads[top - 1]
    r1a, r2a = swap(s1a, bit_a, 0), swap(s2a, bit_b, 0)
    front(low - 1, recv_b)
    s1b, k1b, s2b, k2b = heads[low - 1]
    r1b, r2b = swap(s1b, bit_a, 0), swap(s2b, bit_b, 0)
    shaped = (count, rest, 2, piece, half)
    done = (count, rest, piece, half)

    def split(*arrays):
        return local(split_kernel, [done] * 4, *(x.reshape(shaped) for x in arrays))

    carried = back(1, None)
    t1a, k1a, t2a, k2a = split(k1a, r1a, k2a, r2a)
    r1a, r2a = swap(t1a, bit_b, 0), swap(t2a, bit_a, 0)
    carried = back(2, carried)
    t1b, k1b, t2b, k2b = split(k1b, r1b, k2b, r2b)
    r1b, r2b = swap(t1b, bit_b, 0), swap(t2b, bit_a, 0)
    stacked = (count, 2, rest, piece, half)
    send = local(join_kernel, [stacked], k1a, r1a, k2a, r2a)[0]
    both_r = swap(send, 0, dp_bits[-1])
    carried = back(3, carried)
    both = local(join_more_kernel, [stacked], k1b, r1b, k2b, r2b, both_r)[0]
    for bit in reversed(dp_bits[1:-1]):
        middle = both.shape[0] // 2
        both = add(both[middle:], swap(both[:middle], 0, bit))
    both = both[0]
    for k, bit in enumerate(others):
        got = swap(both, bit, 0)
        if k == len(others) - 1:
            shapes = [(rest, piece, half)] * 2
            for rel in list(range(4, num_dp)) + [0]:
                carried = back(rel, carried)
        else:
            shapes = [both.shape]
        out = local(functools.partial(flip_kernel, 1 << k), shapes, both, got)
        both = out[0]
    a, b = out
    grad_u, grad_v = carried
    a1, b2 = swap(a, bit_a, 0), swap(b, bit_b, 0)
    a2, b1 = swap(a, bit_b, 0), swap(b, bit_a, 0)
    a3, b3 = swap(a1, bit_b, 0), swap(b2, bit_a, 0)
    grad_w_out = assemble(sc, [a, a1, a2, a3, b, b1, b2, b3])
    grads = unpack(sc, reduce_small(packed), groups)
    return (grad_u.reshape(shape), grad_v.reshape(shape), grad_w_out, *grads)


def solution(mesh):
    return jax.shard_map(
        program,
        mesh=mesh,
        in_specs=(
            P("dp", "sp", None),
            P("dp", "sp", None),
            P("dp", "sp", None),
            P(),
            P(),
            P(),
            P(),
            P("dp", None),
        ),
        out_specs=(P("dp", "sp", None), P("dp", "sp", None), P("dp", None), P(), P(), P(), P()),
        check_vma=False,
    )
```

time: 291 us -> 185 us (0.64)
  waiting for transfers between devices: 133 us -> 79.8 us
  Pallas kernels: 110 us -> 72.8 us
  other arithmetic: 12.1 us -> 0.07 us
    ppermute x23 -> x30, waiting for transfers between devices: 133 us -> 79.8 us  [swap(): return lax.ppermute(value, AXES, pairs)]
    pallas_call x4, Pallas kernels: 54.2 us -> 29.6 us  [backward(): pl.pallas_call(functools.partial(backward_kernel, (span, chans, per)), gr...]
    pallas_call x2 -> x4, Pallas kernels: 48.8 us -> 36.2 us  [forward(): pl.pallas_call(functools.partial(forward_kernel, (span, chans, per, piece...]
    concatenate x8 -> x0, other arithmetic: 4.41 us -> none  [the longest x1 2.13 us: reduce_projection(): a = jnp.concatenate([a, swap(a, bit_b, 0)], axis=0)]
    ppermute x23 -> x30, starting transfers between devices: 27.8 us -> 27.6 us  [swap(): return lax.ppermute(value, AXES, pairs)]
  transfers between devices with their start and end apart: 23 -> 30, of which waited for: 14 -> 11; matrix products, arithmetic and copies ran while one was open for 3% -> 0% of each run, Pallas kernels for 23% -> 38%
where the time goes in v2:
time: 185 us
  waiting for transfers between devices  79.8 us (43%)
  Pallas kernels  72.8 us (39%)
  starting transfers between devices  27.6 us (15%)
  local copies, waits for them, and re-layouts  3.67 us (2%)
    ppermute x30, waiting for transfers between devices, swap(): return lax.ppermute(value, AXES, pairs)  79.8 us
    pallas_call x4, Pallas kernels, forward(): pl.pallas_call(functools.partial(forward_kernel, (span, chans, per, piece...  36.2 us
    pallas_call x4, Pallas kernels, backward(): pl.pallas_call(functools.partial(backward_kernel, (span, chans, per)), gr...  29.6 us
    ppermute x30, starting transfers between devices, swap(): return lax.ppermute(value, AXES, pairs)  27.6 us
    pallas_call x1, Pallas kernels, assemble(): pl.pallas_call(assemble_kernel, grid_spec=pltpu.PrefetchScalarGridSpec(nu...  4.16 us
  transfers between devices with their start and end apart: 30, of which 11 were waited for; matrix products, arithmetic and copies ran while one was open for 0% of the time, Pallas kernels for 38%

profile of v2, /device:TPU:0, one launch (start us, length us, event | category | flops | bytes accessed | tf_op | source)
XLA Modules:
  0.0 184.8 jit_solution(11520459250677381018)
XLA Ops:
  0.6 3.0 %collective-permute-start.1 = (bf16[512,2048]{1,0:T(8,128)(2,1)}, bf16[512,2048]{1,0:T(8,128)(2,1)S(1)}, u32[]{:S(2)}, u32[]{:S(2)}) collective-permute-start(bf16[512,2048]{1,0:T(8,128)(2,1)} %w.1), channel_id=1, source_target_pairs={{0,2},{1,3},{2,0},{3,1},{4,6},{5,7},{6,4},{7,5},{8,10},{9,11},{10,... | collective-permute-start | bytes 6291464 | tf_op jit(solution)/shard_map/ppermute | solution.py:27
  3.7 2.2 %copy-done = bf16[1,1024,2048]{2,1,0:T(8,128)(2,1)S(1)} copy-done((bf16[1,1024,2048]{2,1,0:T(8,128)(2,1)S(1)}, bf16[1,1024,2048]{2,1,0:T(8,128)(2,1)}, u32[]{:S(2)}) %copy-start) | copy-done | bytes 4194328
  5.9 8.5 %shard_map.137 = (bf16[1,512,2048]{2,1,0:T(8,128)(2,1)S(1)}, bf16[1024,512]{1,0:T(8,128)(2,1)S(1)}, bf16[1024,512]{1,0:T(8,128)(2,1)S(1)}, bf16[1024,512]{1,0:T(8,128)(2,1)S(1)}, bf16[1024,512]{1,0:T(8,128)(2,1)S(1)}) custom-call(s32[2]{0:T(128)S(1)} %pad_add_fusion.sc, bf16[1024,2048]{1,0:T(8,128)(2,1)} %bitcast.37, bf16[1024,2048]{1,0:T(8,128)(2,1)} %bitcast.41, ...), custom_call_target="tpu_custom_call" | custom-call | flops 2147483648 | tf_op jit(solution)/shard_map/pallas_call | solution.py:147
  14.5 8.5 %shard_map.135 = (bf16[1,512,2048]{2,1,0:T(8,128)(2,1)S(1)}, bf16[1024,512]{1,0:T(8,128)(2,1)S(1)}, bf16[1024,512]{1,0:T(8,128)(2,1)S(1)}, bf16[1024,512]{1,0:T(8,128)(2,1)S(1)}, bf16[1024,512]{1,0:T(8,128)(2,1)S(1)}) custom-call(s32[2]{0:T(128)S(1)} %pad_add_fusion.sc, bf16[1024,2048]{1,0:T(8,128)(2,1)} %bitcast.38, bf16[1024,2048]{1,0:T(8,128)(2,1)} %bitcast.42, ...), custom_call_target="tpu_custom_call" | custom-call | flops 2147483648 | tf_op jit(solution)/shard_map/pallas_call | solution.py:147
  23.0 0.5 collective-permute-start
  23.7 25.8 %collective-permute-done.1.w = bf16[512,2048]{1,0:T(8,128)(2,1)S(1)} collective-permute-done((bf16[512,2048]{1,0:T(8,128)(2,1)}, bf16[512,2048]{1,0:T(8,128)(2,1)S(1)}, u32[]{:S(2)}, u32[]{:S(2)}) %collective-permute-start.1) | collective-permute-done | bytes 2097184 | tf_op jit(solution)/shard_map/ppermute | solution.py:27
  49.5 9.7 %shard_map.138 = (bf16[1,256,1024]{2,1,0:T(8,128)(2,1)S(1)}, bf16[1,256,1024]{2,1,0:T(8,128)(2,1)S(1)}, bf16[1,256,1024]{2,1,0:T(8,128)(2,1)S(1)}, bf16[1,256,10...) custom-call(s32[2]{0:T(128)S(1)} %pad_add_fusion.sc, ...), custom_call_target="tpu_custom_call" | custom-call | flops 2147483648 | tf_op jit(solution)/shard_map/pallas_call | solution.py:147
  59.2 1.8 collective-permute-start.9
  61.0 1.6 collective-permute-start.10
  62.6 11.0 %collective-permute-done.9 = bf16[1,256,1024]{2,1,0:T(8,128)(2,1)S(1)} collective-permute-done((bf16[1,256,1024]{2,1,0:T(8,128)(2,1)S(1)}, bf16[1,256,1024]{2,1,0:T(8,128)(2,1)S(1)}, u32[]{:S(2)}, u32[]{:S(2)}) %collective-permute-start.9) | collective-permute-done | bytes 524320 | tf_op jit(solution)/shard_map/ppermute | solution.py:27
  73.6 1.5 collective-permute-done.10
  75.1 0.2 shard_map.144
  75.3 1.6 collective-permute-start.11
  76.9 9.6 %shard_map.136 = (bf16[1,256,1024]{2,1,0:T(8,128)(2,1)S(1)}, bf16[1,256,1024]{2,1,0:T(8,128)(2,1)S(1)}, bf16[1,256,1024]{2,1,0:T(8,128)(2,1)S(1)}, bf16[1,256,10...) custom-call(s32[2]{0:T(128)S(1)} %pad_add_fusion.sc, ...), custom_call_target="tpu_custom_call" | custom-call | flops 2147483648 | tf_op jit(solution)/shard_map/pallas_call | solution.py:147
  86.5 0.6 collective-permute-start.5
  87.1 0.3 collective-permute-start.6
  87.4 1.7 collective-permute-start.12
  89.0 16.0 %collective-permute-done.12.r2 = bf16[1,2,64,1024]{3,2,1,0:T(8,128)(2,1)S(1)} collective-permute-done((bf16[1,2,64,1024]{3,2,1,0:T(8,128)(2,1)S(1)}, bf16[1,2,64,1024]{3,2,1,0:T(8,128)(2,1)S(1)}, u32[]{:S(2)}, u32[]{:S(2)}) %collective-permute-start.12) | collective-permute-done | bytes 262176 | tf_op jit(solution)/shard_map/ppermute | solution.py:27
  105.2 1.5 collective-permute-start.13
  107.0 0.5 collective-permute-start.7
  107.5 0.6 collective-permute-start.8
  108.1 5.3 %collective-permute-done.7.r1 = bf16[1,2,64,1024]{3,2,1,0:T(8,128)(2,1)S(1)} collective-permute-done((bf16[1,2,64,1024]{3,2,1,0:T(8,128)(2,1)S(1)}, bf16[1,2,64,1024]{3,2,1,0:T(8,128)(2,1)S(1)}, u32[]{:S(2)}, u32[]{:S(2)}) %collective-permute-start.7) | collective-permute-done | bytes 262176 | tf_op jit(solution)/shard_map/ppermute | solution.py:27
  113.4 0.5 collective-permute-done.8.r2
  113.9 3.4 %collective-permute-done.13.more = bf16[1,2,2,64,1024]{4,3,2,1,0:T(8,128)(2,1)S(1)} collective-permute-done((bf16[1,2,2,64,1024]{4,3,2,1,0:T(8,128)(2,1)S(1)}, bf16[1,2,2,64,1024]{4,3,2,1,0:T(8,128)(2,1)S(1)}, u32[]{:S(2)}, u32[]{:S(2)}) %collective-permute-start.13) | collective-permute-done | bytes 524320 | tf_op jit(solution)/shard_map/ppermute | solution.py:27
  117.5 2.7 %collective-permute-start.14 = (bf16[2,2,64,1024]{3,2,1,0:T(8,128)(2,1)S(1)}, bf16[2,2,64,1024]{3,2,1,0:T(8,128)(2,1)S(1)}, u32[]{:S(2)}, u32[]{:S(2)}) collective-permute-start(bf16[2,2,64,1024]{3,2,1,0:T(8,128)(2,1)S(1)} %bitcast.27), channel_id=1, source_target_pairs={{0,16},{1,17},{2,18},{3,19},{4,20},{5,21},{6,22},{7,23},{8,24},{9,... | collective-permute-start | bytes 1572872 | tf_op jit(solution)/shard_map/ppermute | solution.py:27
  120.2 7.4 %shard_map.139 = (bf16[1024,2048]{1,0:T(8,128)(2,1)}, bf16[1024,2048]{1,0:T(8,128)(2,1)}, bf16[2,160,128]{2,1,0:T(8,128)(2,1)S(1)}) custom-call(s32[2]{0:T(128)S(1)} %pad_add_fusion.sc, bf16[1024,2048]{1,0:T(8,128)(2,1)S(1)} %bitcast.23, bf16[512,2048]{1,0:T(8,128)(2,1)S(1)} %collective-permute-done.4.w, bf16[1024,512]{1,0:T(8,128)(2,1)S(1)} %get-tuple-element.73.upper, ...), custom_call_target="tpu_custom_call" | custom-call | flops 2147483648 | tf_op jit(solution)/shard_map/pallas_call | solution.py:278
  127.6 7.4 %shard_map.140 = (bf16[1024,2048]{1,0:T(8,128)(2,1)}, bf16[1024,2048]{1,0:T(8,128)(2,1)}, bf16[2,160,128]{2,1,0:T(8,128)(2,1)S(1)}) custom-call(s32[2]{0:T(128)S(1)} %pad_add_fusion.sc, bf16[1024,2048]{1,0:T(8,128)(2,1)S(1)} %bitcast.24, bf16[512,2048]{1,0:T(8,128)(2,1)S(1)} %collective-permute-done.1.w, ...), custom_call_target="tpu_custom_call", output_to_operand_aliasing={{0}: (10, {}), {1}: (11, {})} | custom-call | flops 2147483648 | tf_op jit(solution)/shard_map/pallas_call | solution.py:278
  135.0 7.4 %shard_map.141 = (bf16[1024,2048]{1,0:T(8,128)(2,1)}, bf16[1024,2048]{1,0:T(8,128)(2,1)}, bf16[2,160,128]{2,1,0:T(8,128)(2,1)S(1)}) custom-call(s32[2]{0:T(128)S(1)} %pad_add_fusion.sc, bf16[1024,2048]{1,0:T(8,128)(2,1)S(1)} %bitcast.25, bf16[512,2048]{1,0:T(8,128)(2,1)S(1)} %collective-permute-done.2.w, ...), custom_call_target="tpu_custom_call", output_to_operand_aliasing={{0}: (10, {}), {1}: (11, {})} | custom-call | flops 2147483648 | tf_op jit(solution)/shard_map/pallas_call | solution.py:278
  142.4 0.5 collective-permute-start.21
  143.1 0.7 collective-permute-start.15
  143.7 0.4 collective-permute-start.19
  144.2 1.6 collective-permute-start.23
  145.8 7.4 %shard_map.142 = (bf16[1024,2048]{1,0:T(8,128)(2,1)}, bf16[1024,2048]{1,0:T(8,128)(2,1)}, bf16[2,160,128]{2,1,0:T(8,128)(2,1)S(1)}) custom-call(s32[2]{0:T(128)S(1)} %pad_add_fusion.sc, bf16[1024,2048]{1,0:T(8,128)(2,1)S(1)} %bitcast.26, bf16[512,2048]{1,0:T(8,128)(2,1)S(1)} %copy-done.2, ...), custom_call_target="tpu_custom_call", output_to_operand_aliasing={{0}: (10, {}), {1}: (11, {})} | custom-call | flops 2147483648 | tf_op jit(solution)/shard_map/pallas_call | solution.py:278
  153.2 1.5 collective-permute-start.24
  154.8 1.6 collective-permute-start.16
  156.3 1.4 collective-permute-done.24.got
  157.8 1.6 collective-permute-start.25
  159.4 1.4 collective-permute-start.18
  160.8 0.5 collective-permute-start.17
  161.3 0.6 collective-permute-start.20
  161.9 4.7 %collective-permute-done.25.got = bf16[2,160,128]{2,1,0:T(8,128)(2,1)S(1)} collective-permute-done((bf16[2,160,128]{2,1,0:T(8,128)(2,1)S(1)}, bf16[2,160,128]{2,1,0:T(8,128)(2,1)S(1)}, u32[]{:S(2)}, u32[]{:S(2)}) %collective-permute-start.25) | collective-permute-done | bytes 81952 | tf_op jit(solution)/shard_map/ppermute | solution.py:27
  166.7 6.2 %collective-permute-done.26.got = bf16[2,160,128]{2,1,0:T(8,128)(2,1)S(1)} collective-permute-done((bf16[2,160,128]{2,1,0:T(8,128)(2,1)S(1)}, bf16[2,160,128]{2,1,0:T(8,128)(2,1)S(1)}, u32[]{:S(2)}, u32[]{:S(2)}) %collective-permute-start.26) | collective-permute-done | bytes 81952 | tf_op jit(solution)/shard_map/ppermute | solution.py:27
  172.9 0.6 collective-permute-start.28
  173.5 3.9 %collective-permute-done.28.refs_2_ = bf16[2,160,128]{2,1,0:T(8,128)(2,1)S(1)} collective-permute-done((bf16[2,160,128]{2,1,0:T(8,128)(2,1)S(1)}, bf16[2,160,128]{2,1,0:T(8,128)(2,1)S(1)}, u32[]{:S(2)}, u32[]{:S(2)}) %collective-permute-start.28) | collective-permute-done | bytes 81952 | tf_op jit(solution)/shard_map/ppermute | solution.py:27
  177.5 0.6 copy-done.10
  178.2 0.7 copy-done.12
  178.9 4.2 %assemble.1 = f32[512,2048]{1,0:T(8,128)} custom-call(s32[2]{0:T(128)} %copy-done.5, bf16[2,64,1024]{2,1,0:T(8,128)(2,1)} %copy-done.3, bf16[2,64,1024]{2,1,0:T(8,128)(2,1)} %copy-done.7, bf16[2,64,1024]{2,1,0:T(8,128)(2,1)} %copy-done.9, bf16[2,64,1024]{2,1,0:T(8,128)(2,1)} %copy-done.11, bf16[2,64,1024]{2,1,0:T(8,128)(2,1)} %copy-done.4, ...), custom_call_target="tpu_custom_call" | custom-call | tf_op jit(solution)/shard_map/assemble/pallas_call | solution.py:407
  183.1 1.7 unpack.1
  (60 shorter events, 1.4 us)
Async XLA Ops:
  0.6 48.9 %collective-permute-start.1 = (bf16[512,2048]{1,0:T(8,128)(2,1)}, bf16[512,2048]{1,0:T(8,128)(2,1)S(1)}, u32[]{:S(2)}, u32[]{:S(2)}) collective-permute-start(bf16[512,2048]{1,0:T(8,128)(2,1)} %w.1), channel_id=1, source_target_pairs={{0,2},{1,3},{2,0},{3,1},{4,6},{5,7},{6,4},{7,5},{8,10},{9,11},{10,... | collective-permute-start | bytes 6291464 | tf_op jit(solution)/shard_map/ppermute | solution.py:27
  3.7 142.0 %copy-start.5 = (s32[2]{0:T(128)}, s32[2]{0:T(128)S(1)}, u32[]{:S(2)}) copy-start(s32[2]{0:T(128)S(1)} %pad_add_fusion.sc) | copy-start | bytes 28
  3.7 2.2 %copy-start = (bf16[1,1024,2048]{2,1,0:T(8,128)(2,1)S(1)}, bf16[1,1024,2048]{2,1,0:T(8,128)(2,1)}, u32[]{:S(2)}) copy-start(bf16[1,1024,2048]{2,1,0:T(8,128)(2,1)} %param.10) | copy-start | bytes 12582916
  14.4 9.2 %copy-start.2 = (bf16[512,2048]{1,0:T(8,128)(2,1)S(1)}, bf16[512,2048]{1,0:T(8,128)(2,1)}, u32[]{:S(2)}) copy-start(bf16[512,2048]{1,0:T(8,128)(2,1)} %w.1) | copy-start | bytes 6291460
  14.4 35.1 %collective-permute-start.3 = (bf16[1,512,2048]{2,1,0:T(8,128)(2,1)S(1)}, bf16[1,512,2048]{2,1,0:T(8,128)(2,1)S(1)}, u32[]{:S(2)}, u32[]{:S(2)}) collective-permute-start(bf16[1,512,2048]{2,1,0:T(8,128)(2,1)S(1)} %get-tuple-element.68), channel_id=1, source_target_pairs={{0,1},{1,0},{2,3},{3,2},{4,5},{5,4},{6,7},{7,6},{8,9},{9,8},{10,11... | collective-permute-start | bytes 6291464 | tf_op jit(solution)/shard_map/ppermute | solution.py:27
  23.0 53.9 %collective-permute-start = (bf16[1,512,2048]{2,1,0:T(8,128)(2,1)S(1)}, bf16[1,512,2048]{2,1,0:T(8,128)(2,1)S(1)}, u32[]{:S(2)}, u32[]{:S(2)}) collective-permute-start(bf16[1,512,2048]{2,1,0:T(8,128)(2,1)S(1)} %get-tuple-element.59), channel_id=1, source_target_pairs={{0,1},{1,0},{2,3},{3,2},{4,5},{5,4},{6,7},{7,6},{8,9},{9,8},{10,11... | collective-permute-start | bytes 6291464 | tf_op jit(solution)/shard_map/ppermute | solution.py:27
  23.6 96.6 %collective-permute-start.4 = (bf16[512,2048]{1,0:T(8,128)(2,1)S(1)}, bf16[512,2048]{1,0:T(8,128)(2,1)S(1)}, u32[]{:S(2)}, u32[]{:S(2)}) collective-permute-start(bf16[512,2048]{1,0:T(8,128)(2,1)S(1)} %copy-done.2), channel_id=1, source_target_pairs={{0,1},{1,0},{2,3},{3,2},{4,5},{5,4},{6,7},{7,6},{8,9},{9,8},{10,11... | collective-permute-start | bytes 6291464 | tf_op jit(solution)/shard_map/ppermute | solution.py:27
  49.5 85.5 %collective-permute-start.2 = (bf16[512,2048]{1,0:T(8,128)(2,1)S(1)}, bf16[512,2048]{1,0:T(8,128)(2,1)S(1)}, u32[]{:S(2)}, u32[]{:S(2)}) collective-permute-start(bf16[512,2048]{1,0:T(8,128)(2,1)S(1)} %collective-permute-done.1.w), channel_id=1, source_target_pairs={{0,1},{1,0},{2,3},{3,2},{4,5},{5,4},{6,7},{7,6},{8,9},{9,8},{10,11... | collective-permute-start | bytes 6291464 | tf_op jit(solution)/shard_map/ppermute | solution.py:27
  49.5 27.4 %copy-start.1 = (bf16[1,1024,2048]{2,1,0:T(8,128)(2,1)S(1)}, bf16[1,1024,2048]{2,1,0:T(8,128)(2,1)}, u32[]{:S(2)}) copy-start(bf16[1,1024,2048]{2,1,0:T(8,128)(2,1)} %param.10) | copy-start | bytes 12582916
  59.2 14.4 %collective-permute-start.9 = (bf16[1,256,1024]{2,1,0:T(8,128)(2,1)S(1)}, bf16[1,256,1024]{2,1,0:T(8,128)(2,1)S(1)}, u32[]{:S(2)}, u32[]{:S(2)}) collective-permute-start(bf16[1,256,1024]{2,1,0:T(8,128)(2,1)S(1)} %get-tuple-element.94), channel_id=1, source_target_pairs={{0,4},{1,5},{2,6},{3,7},{4,0},{5,1},{6,2},{7,3},{8,12},{9,13},{10,... | collective-permute-start | bytes 1572872 | tf_op jit(solution)/shard_map/ppermute | solution.py:27
  61.0 14.0 %collective-permute-start.10 = (bf16[1,256,1024]{2,1,0:T(8,128)(2,1)S(1)}, bf16[1,256,1024]{2,1,0:T(8,128)(2,1)S(1)}, u32[]{:S(2)}, u32[]{:S(2)}) collective-permute-start(bf16[1,256,1024]{2,1,0:T(8,128)(2,1)S(1)} %get-tuple-element.96), channel_id=1, source_target_pairs={{0,8},{1,9},{2,10},{3,11},{4,12},{5,13},{6,14},{7,15},{8,0},{9,1},... | collective-permute-start | bytes 1572872 | tf_op jit(solution)/shard_map/ppermute | solution.py:27
  75.3 12.1 %collective-permute-start.11 = (bf16[1,2,64,1024]{3,2,1,0:T(8,128)(2,1)S(1)}, bf16[1,2,64,1024]{3,2,1,0:T(8,128)(2,1)S(1)}, u32[]{:S(2)}, u32[]{:S(2)}) collective-permute-start(bf16[1,2,64,1024]{3,2,1,0:T(8,128)(2,1)S(1)} %get-tuple-element.98), channel_id=1, source_target_pairs={{0,8},{1,9},{2,10},{3,11},{4,12},{5,13},{6,14},{7,15},{8,0},{9,1},... | collective-permute-start | bytes 786440 | tf_op jit(solution)/shard_map/ppermute | solution.py:27
  86.5 20.2 %collective-permute-start.5 = (bf16[1,256,1024]{2,1,0:T(8,128)(2,1)S(1)}, bf16[1,256,1024]{2,1,0:T(8,128)(2,1)S(1)}, u32[]{:S(2)}, u32[]{:S(2)}) collective-permute-start(bf16[1,256,1024]{2,1,0:T(8,128)(2,1)S(1)} %get-tuple-element.86), channel_id=1, source_target_pairs={{0,4},{1,5},{2,6},{3,7},{4,0},{5,1},{6,2},{7,3},{8,12},{9,13},{10,... | collective-permute-start | bytes 1572872 | tf_op jit(solution)/shard_map/ppermute | solution.py:27
  87.1 19.7 %collective-permute-start.6 = (bf16[1,256,1024]{2,1,0:T(8,128)(2,1)S(1)}, bf16[1,256,1024]{2,1,0:T(8,128)(2,1)S(1)}, u32[]{:S(2)}, u32[]{:S(2)}) collective-permute-start(bf16[1,256,1024]{2,1,0:T(8,128)(2,1)S(1)} %get-tuple-element.88), channel_id=1, source_target_pairs={{0,8},{1,9},{2,10},{3,11},{4,12},{5,13},{6,14},{7,15},{8,0},{9,1},... | collective-permute-start | bytes 1572872 | tf_op jit(solution)/shard_map/ppermute | solution.py:27
  87.4 17.7 %collective-permute-start.12 = (bf16[1,2,64,1024]{3,2,1,0:T(8,128)(2,1)S(1)}, bf16[1,2,64,1024]{3,2,1,0:T(8,128)(2,1)S(1)}, u32[]{:S(2)}, u32[]{:S(2)}) collective-permute-start(bf16[1,2,64,1024]{3,2,1,0:T(8,128)(2,1)S(1)} %get-tuple-element.100), channel_id=1, source_target_pairs={{0,4},{1,5},{2,6},{3,7},{4,0},{5,1},{6,2},{7,3},{8,12},{9,13},{10,... | collective-permute-start | bytes 786440 | tf_op jit(solution)/shard_map/ppermute | solution.py:27
  105.2 12.1 %collective-permute-start.13 = (bf16[1,2,2,64,1024]{4,3,2,1,0:T(8,128)(2,1)S(1)}, bf16[1,2,2,64,1024]{4,3,2,1,0:T(8,128)(2,1)S(1)}, u32[]{:S(2)}, u32[]{:S(2)}) collective-permute-start(bf16[1,2,2,64,1024]{4,3,2,1,0:T(8,128)(2,1)S(1)} %shard_map.145), channel_id=1, source_target_pairs={{0,2},{1,3},{2,0},{3,1},{4,6},{5,7},{6,4},{7,5},{8,10},{9,11},{10,... | collective-permute-start | bytes 1572872 | tf_op jit(solution)/shard_map/ppermute | solution.py:27
  107.0 6.4 %collective-permute-start.7 = (bf16[1,2,64,1024]{3,2,1,0:T(8,128)(2,1)S(1)}, bf16[1,2,64,1024]{3,2,1,0:T(8,128)(2,1)S(1)}, u32[]{:S(2)}, u32[]{:S(2)}) collective-permute-start(bf16[1,2,64,1024]{3,2,1,0:T(8,128)(2,1)S(1)} %get-tuple-element.90), channel_id=1, source_target_pairs={{0,8},{1,9},{2,10},{3,11},{4,12},{5,13},{6,14},{7,15},{8,0},{9,1},... | collective-permute-start | bytes 786440 | tf_op jit(solution)/shard_map/ppermute | solution.py:27
  107.5 6.4 %collective-permute-start.8 = (bf16[1,2,64,1024]{3,2,1,0:T(8,128)(2,1)S(1)}, bf16[1,2,64,1024]{3,2,1,0:T(8,128)(2,1)S(1)}, u32[]{:S(2)}, u32[]{:S(2)}) collective-permute-start(bf16[1,2,64,1024]{3,2,1,0:T(8,128)(2,1)S(1)} %get-tuple-element.92), channel_id=1, source_target_pairs={{0,4},{1,5},{2,6},{3,7},{4,0},{5,1},{6,2},{7,3},{8,12},{9,13},{10,... | collective-permute-start | bytes 786440 | tf_op jit(solution)/shard_map/ppermute | solution.py:27
  117.5 25.4 %collective-permute-start.14 = (bf16[2,2,64,1024]{3,2,1,0:T(8,128)(2,1)S(1)}, bf16[2,2,64,1024]{3,2,1,0:T(8,128)(2,1)S(1)}, u32[]{:S(2)}, u32[]{:S(2)}) collective-permute-start(bf16[2,2,64,1024]{3,2,1,0:T(8,128)(2,1)S(1)} %bitcast.27), channel_id=1, source_target_pairs={{0,16},{1,17},{2,18},{3,19},{4,20},{5,21},{6,22},{7,23},{8,24},{9,... | collective-permute-start | bytes 1572872 | tf_op jit(solution)/shard_map/ppermute | solution.py:27
  142.4 1.8 collective-permute-start.22
  142.4 10.8 %collective-permute-start.21 = (bf16[2,160,128]{2,1,0:T(8,128)(2,1)S(1)}, bf16[2,160,128]{2,1,0:T(8,128)(2,1)S(1)}, u32[]{:S(2)}, u32[]{:S(2)}) collective-permute-start(bf16[2,160,128]{2,1,0:T(8,128)(2,1)S(1)} %get-tuple-element.104), channel_id=1, source_target_pairs={{0,1},{1,0},{2,3},{3,2},{4,5},{5,4},{6,7},{7,6},{8,9},{9,8},{10,11... | collective-permute-start | bytes 245768 | tf_op jit(solution)/shard_map/ppermute | solution.py:27
  143.0 11.7 %copy-start.3 = (bf16[2,64,1024]{2,1,0:T(8,128)(2,1)}, bf16[2,64,1024]{2,1,0:T(8,128)(2,1)S(1)}, u32[]{:S(2)}) copy-start(bf16[2,64,1024]{2,1,0:T(8,128)(2,1)S(1)} %get-tuple-element.101.refs_0_) | copy-start | bytes 786436
  143.0 16.4 %copy-start.4 = (bf16[2,64,1024]{2,1,0:T(8,128)(2,1)}, bf16[2,64,1024]{2,1,0:T(8,128)(2,1)S(1)}, u32[]{:S(2)}) copy-start(bf16[2,64,1024]{2,1,0:T(8,128)(2,1)S(1)} %get-tuple-element.102.refs_4_) | copy-start | bytes 786436
  143.1 17.8 %collective-permute-start.15 = (bf16[2,64,1024]{2,1,0:T(8,128)(2,1)S(1)}, bf16[2,64,1024]{2,1,0:T(8,128)(2,1)S(1)}, u32[]{:S(2)}, u32[]{:S(2)}) collective-permute-start(bf16[2,64,1024]{2,1,0:T(8,128)(2,1)S(1)} %get-tuple-element.101.refs_0_), channel_id=1, source_target_pairs={{0,4},{1,5},{2,6},{3,7},{4,0},{5,1},{6,2},{7,3},{8,12},{9,13},{10,... | collective-permute-start | bytes 786440 | tf_op jit(solution)/shard_map/ppermute | solution.py:27
  143.7 17.6 %collective-permute-start.19 = (bf16[2,64,1024]{2,1,0:T(8,128)(2,1)S(1)}, bf16[2,64,1024]{2,1,0:T(8,128)(2,1)S(1)}, u32[]{:S(2)}, u32[]{:S(2)}) collective-permute-start(bf16[2,64,1024]{2,1,0:T(8,128)(2,1)S(1)} %get-tuple-element.102.refs_4_), channel_id=1, source_target_pairs={{0,8},{1,9},{2,10},{3,11},{4,12},{5,13},{6,14},{7,15},{8,0},{9,1},... | collective-permute-start | bytes 786440 | tf_op jit(solution)/shard_map/ppermute | solution.py:27
  144.2 9.0 %collective-permute-start.23 = (bf16[2,160,128]{2,1,0:T(8,128)(2,1)S(1)}, bf16[2,160,128]{2,1,0:T(8,128)(2,1)S(1)}, u32[]{:S(2)}, u32[]{:S(2)}) collective-permute-start(bf16[2,160,128]{2,1,0:T(8,128)(2,1)S(1)} %shard_map.149), channel_id=1, source_target_pairs={{0,2},{1,3},{2,0},{3,1},{4,6},{5,7},{6,4},{7,5},{8,10},{9,11},{10,... | collective-permute-start | bytes 245768 | tf_op jit(solution)/shard_map/ppermute | solution.py:27
  153.2 30.0 %copy-start.6 = (s32[2]{0:T(128)S(1)}, s32[2]{0:T(128)}, u32[]{:S(2)}) copy-start(s32[2]{0:T(128)} %copy-done.5) | copy-start | bytes 28
  153.2 4.5 %collective-permute-start.24 = (bf16[2,160,128]{2,1,0:T(8,128)(2,1)S(1)}, bf16[2,160,128]{2,1,0:T(8,128)(2,1)S(1)}, u32[]{:S(2)}, u32[]{:S(2)}) collective-permute-start(bf16[2,160,128]{2,1,0:T(8,128)(2,1)S(1)} %shard_map.150.mine), channel_id=1, source_target_pairs={{0,4},{1,5},{2,6},{3,7},{4,0},{5,1},{6,2},{7,3},{8,12},{9,13},{10,... | collective-permute-start | bytes 245768 | tf_op jit(solution)/shard_map/ppermute | solution.py:27
  154.8 18.7 %collective-permute-start.16 = (bf16[2,64,1024]{2,1,0:T(8,128)(2,1)S(1)}, bf16[2,64,1024]{2,1,0:T(8,128)(2,1)S(1)}, u32[]{:S(2)}, u32[]{:S(2)}) collective-permute-start(bf16[2,64,1024]{2,1,0:T(8,128)(2,1)S(1)} %get-tuple-element.101.refs_0_), channel_id=1, source_target_pairs={{0,8},{1,9},{2,10},{3,11},{4,12},{5,13},{6,14},{7,15},{8,0},{9,1},... | collective-permute-start | bytes 786440 | tf_op jit(solution)/shard_map/ppermute | solution.py:27
  157.8 8.8 %collective-permute-start.25 = (bf16[2,160,128]{2,1,0:T(8,128)(2,1)S(1)}, bf16[2,160,128]{2,1,0:T(8,128)(2,1)S(1)}, u32[]{:S(2)}, u32[]{:S(2)}) collective-permute-start(bf16[2,160,128]{2,1,0:T(8,128)(2,1)S(1)} %shard_map.151.mine), channel_id=1, source_target_pairs={{0,8},{1,9},{2,10},{3,11},{4,12},{5,13},{6,14},{7,15},{8,0},{9,1},... | collective-permute-start | bytes 245768 | tf_op jit(solution)/shard_map/ppermute | solution.py:27
  159.4 18.0 %collective-permute-start.18 = (bf16[2,64,1024]{2,1,0:T(8,128)(2,1)S(1)}, bf16[2,64,1024]{2,1,0:T(8,128)(2,1)S(1)}, u32[]{:S(2)}, u32[]{:S(2)}) collective-permute-start(bf16[2,64,1024]{2,1,0:T(8,128)(2,1)S(1)} %get-tuple-element.102.refs_4_), channel_id=1, source_target_pairs={{0,4},{1,5},{2,6},{3,7},{4,0},{5,1},{6,2},{7,3},{8,12},{9,13},{10,... | collective-permute-start | bytes 786440 | tf_op jit(solution)/shard_map/ppermute | solution.py:27
  160.8 16.6 %copy-start.7 = (bf16[2,64,1024]{2,1,0:T(8,128)(2,1)}, bf16[2,64,1024]{2,1,0:T(8,128)(2,1)S(1)}, u32[]{:S(2)}) copy-start(bf16[2,64,1024]{2,1,0:T(8,128)(2,1)S(1)} %collective-permute-done.15.refs_1_) | copy-start | bytes 786436
  160.8 16.6 %collective-permute-start.17 = (bf16[2,64,1024]{2,1,0:T(8,128)(2,1)S(1)}, bf16[2,64,1024]{2,1,0:T(8,128)(2,1)S(1)}, u32[]{:S(2)}, u32[]{:S(2)}) collective-permute-start(bf16[2,64,1024]{2,1,0:T(8,128)(2,1)S(1)} %collective-permute-done.15.refs_1_), channel_id=1, source_target_pairs={{0,8},{1,9},{2,10},{3,11},{4,12},{5,13},{6,14},{7,15},{8,0},{9,1},... | collective-permute-start | bytes 786440 | tf_op jit(solution)/shard_map/ppermute | solution.py:27
  161.3 16.1 %copy-start.8 = (bf16[2,64,1024]{2,1,0:T(8,128)(2,1)}, bf16[2,64,1024]{2,1,0:T(8,128)(2,1)S(1)}, u32[]{:S(2)}) copy-start(bf16[2,64,1024]{2,1,0:T(8,128)(2,1)S(1)} %collective-permute-done.19.refs_6_) | copy-start | bytes 786436
  161.3 16.1 %collective-permute-start.20 = (bf16[2,64,1024]{2,1,0:T(8,128)(2,1)S(1)}, bf16[2,64,1024]{2,1,0:T(8,128)(2,1)S(1)}, u32[]{:S(2)}, u32[]{:S(2)}) collective-permute-start(bf16[2,64,1024]{2,1,0:T(8,128)(2,1)S(1)} %collective-permute-done.19.refs_6_), channel_id=1, source_target_pairs={{0,4},{1,5},{2,6},{3,7},{4,0},{5,1},{6,2},{7,3},{8,12},{9,13},{10,... | collective-permute-start | bytes 786440 | tf_op jit(solution)/shard_map/ppermute | solution.py:27
  166.6 6.3 %collective-permute-start.26 = (bf16[2,160,128]{2,1,0:T(8,128)(2,1)S(1)}, bf16[2,160,128]{2,1,0:T(8,128)(2,1)S(1)}, u32[]{:S(2)}, u32[]{:S(2)}) collective-permute-start(bf16[2,160,128]{2,1,0:T(8,128)(2,1)S(1)} %shard_map.152.mine), channel_id=1, source_target_pairs={{0,16},{1,17},{2,18},{3,19},{4,20},{5,21},{6,22},{7,23},{8,24},{9,... | collective-permute-start | bytes 245768 | tf_op jit(solution)/shard_map/ppermute | solution.py:27
  172.9 4.5 %collective-permute-start.28 = (bf16[2,160,128]{2,1,0:T(8,128)(2,1)S(1)}, bf16[2,160,128]{2,1,0:T(8,128)(2,1)S(1)}, u32[]{:S(2)}, u32[]{:S(2)}) collective-permute-start(bf16[2,160,128]{2,1,0:T(8,128)(2,1)S(1)} %shard_map.153.refs_0_), channel_id=1, source_target_pairs={{0,2},{1,3},{2,0},{3,1},{4,6},{5,7},{6,4},{7,5},{8,10},{9,11},{10,... | collective-permute-start | bytes 245768 | tf_op jit(solution)/shard_map/ppermute | solution.py:27
  173.5 4.0 %copy-start.9 = (bf16[2,64,1024]{2,1,0:T(8,128)(2,1)}, bf16[2,64,1024]{2,1,0:T(8,128)(2,1)S(1)}, u32[]{:S(2)}) copy-start(bf16[2,64,1024]{2,1,0:T(8,128)(2,1)S(1)} %collective-permute-done.16.refs_2_) | copy-start | bytes 786436
  173.5 9.6 %collective-permute-start.27 = (bf16[2,160,128]{2,1,0:T(8,128)(2,1)S(1)}, bf16[2,160,128]{2,1,0:T(8,128)(2,1)S(1)}, u32[]{:S(2)}, u32[]{:S(2)}) collective-permute-start(bf16[2,160,128]{2,1,0:T(8,128)(2,1)S(1)} %shard_map.153.refs_0_), channel_id=1, source_target_pairs={{0,1},{1,0},{2,3},{3,2},{4,5},{5,4},{6,7},{7,6},{8,9},{9,8},{10,11... | collective-permute-start | bytes 245768 | tf_op jit(solution)/shard_map/ppermute | solution.py:27
  177.4 5.7 %collective-permute-start.29 = (bf16[2,160,128]{2,1,0:T(8,128)(2,1)S(1)}, bf16[2,160,128]{2,1,0:T(8,128)(2,1)S(1)}, u32[]{:S(2)}, u32[]{:S(2)}) collective-permute-start(bf16[2,160,128]{2,1,0:T(8,128)(2,1)S(1)} %collective-permute-done.28.refs_2_), channel_id=1, source_target_pairs={{0,1},{1,0},{2,3},{3,2},{4,5},{5,4},{6,7},{7,6},{8,9},{9,8},{10,11... | collective-permute-start | bytes 245768 | tf_op jit(solution)/shard_map/ppermute | solution.py:27
  177.4 0.7 copy-start.10
  177.4 0.8 copy-start.11
  178.2 0.7 copy-start.12

commit v3 on v2

--- a/solution.py
+++ b/solution.py
@@ -32,7 +32,8 @@
 
 
 def forward_kernel(cfg, sc, u, v, d_out, w_mix, bias, gain, shift, *rest):
-    span, chans, per, piece, inner, fused = cfg
+    span, chans, per, piece, inner, fused, resident, place = cfg
+    here = pl.program_id(0) * pl.num_programs(1) + pl.program_id(1)
     if fused:
         recv, s1, k1, s2, k2, upper_o, m1_o, scaled_o, w1_o, gated, wide = rest
     else:
@@ -43,47 +44,52 @@
     col = lax.broadcasted_iota(jnp.int32, (span, span), 1)
     for g in range(per):
         lanes = slice(g * chans, (g + 1) * chans)
+        source = lanes
+        if resident:
+            start = (place(pl.program_id(0), pl.program_id(1), sc) * per + g) * chans
+            source = pl.ds(pl.multiple_of(start, chans), chans)
         for b in range(blocks):
             rows = slice(b * span, (b + 1) * span)
-            c = v[rows, lanes].astype(f32)
+            c = v[rows, source].astype(f32)
             c2 = c * c
             tv = jnp.tanh(c * (K0 + (K0 * K1) * c2))
             hv = 0.5 + 0.5 * tv
             gate = c * hv
-            dv = hv + (c * (0.5 - 0.5 * tv * tv)) * (K0 + (3.0 * K0 * K1) * c2)
+            dv = hv + (gate * (1.0 - hv)) * (2.0 * K0 + (6.0 * K0 * K1) * c2)
             centre = gate - jnp.mean(gate, axis=1, keepdims=True)
             var = jnp.mean(centre * centre, axis=1, keepdims=True)
             inv = lax.rsqrt(var + EPS)
             scaled = centre * inv
             wide[:, b * chans : (b + 1) * chans] = (scaled * gain[g] + shift[g]).astype(bf16)
-            scaled_o[rows, lanes] = scaled.astype(bf16)
-            w1_o[rows, lanes] = (dv * inv).astype(bf16)
+            scaled_o[here, rows, lanes] = scaled.astype(bf16)
+            w1_o[here, rows, lanes] = (dv * inv).astype(bf16)
         w_low = jnp.where(row >= col, w_mix[g], jnp.zeros_like(w_mix[g]))
         mixed_all = dot(w_low, wide[...], ((1,), (0,)))
         offset = jnp.transpose(jnp.broadcast_to(bias[g], (chans, span)))
         for b in range(blocks):
             rows = slice(b * span, (b + 1) * span)
-            a = u[rows, lanes].astype(f32)
+            a = u[rows, source].astype(f32)
             mixed = mixed_all[:, b * chans : (b + 1) * chans] + offset
             a2 = a * a
             tu = jnp.tanh(a * (K0 + (K0 * K1) * a2))
             hu = 0.5 + 0.5 * tu
             up = a * hu
-            du = hu + (a * (0.5 - 0.5 * tu * tu)) * (K0 + (3.0 * K0 * K1) * a2)
+            du = hu + (up * (1.0 - hu)) * (2.0 * K0 + (6.0 * K0 * K1) * a2)
             gated[rows, lanes] = (up * mixed).astype(bf16)
-            upper_o[rows, lanes] = up.astype(bf16)
-            m1_o[rows, lanes] = (mixed * du).astype(bf16)
+            upper_o[here, rows, lanes] = up.astype(bf16)
+            m1_o[here, rows, lanes] = (mixed * du).astype(bf16)
     if not fused:
-        part[0] = dot(gated[...], d_out[...], ((0,), (0,))).astype(bf16)
+        part[here] = dot(gated[...], d_out[...], ((0,), (0,))).astype(bf16)
         return
     half = d_out.shape[1] // 2
     count = per * chans // piece
+    there = pl.program_id(0) * pl.num_programs(1) + jnp.bitwise_xor(pl.program_id(1), sc[1] // inner)
     for side, (send, keep) in enumerate(((s1, k1), (s2, k2))):
         lanes = slice(side * half, (side + 1) * half)
         total = dot(gated[...], d_out[:, lanes], ((0,), (0,)))
         for p in range(count):
             rows = slice(p * piece, (p + 1) * piece)
-            value = (total[rows] + recv[0, rows, lanes].astype(f32)).astype(bf16)
+            value = (total[rows] + recv[here, rows, lanes].astype(f32)).astype(bf16)
             rel = jnp.bitwise_xor(p, sc[1] % inner)
             low, high = rel % 2, rel // 2
             if side == 0:
@@ -94,14 +100,14 @@
 
             @pl.when(flag == 1)
             def _():
-                send[0, where, :] = value
+                send[there, where, :] = value
 
             @pl.when(flag == 0)
             def _():
-                keep[0, where, :] = value
-
-
-def forward(sc, first, count, u, v, d_out, w_mix, bias, gain, shift, recv):
+                keep[there, where, :] = value
+
+
+def forward(sc, first, count, resident, u, v, d_out, w_mix, bias, gain, shift, recv):
     num_sp, num_dp = lax.axis_size("sp"), lax.axis_size("dp")
     length, width = u.shape
     groups, span, _ = w_mix.shape
@@ -119,38 +125,35 @@
 
     wide = pl.BlockSpec((length, chunk), lambda i, j, sc: (0, at(i, j, sc)))
     vec = pl.BlockSpec((per, 1, span), lambda i, j, sc: (at(i, j, sc), 0, 0))
+    whole = pl.BlockSpec(memory_space=pltpu.VMEM)
     in_specs = [
-        wide,
-        wide,
-        pl.BlockSpec(memory_space=pltpu.VMEM),
+        whole if resident else wide,
+        whole if resident else wide,
+        whole,
         pl.BlockSpec((per, span, span), lambda i, j, sc: (at(i, j, sc), 0, 0)),
         vec,
         vec,
         vec,
     ]
     args = [u, v, d_out, w_mix, bias, gain, shift]
-    save = pl.BlockSpec((length, chunk), lambda i, j, sc: (0, i * steps + j))
-    save_shape = jax.ShapeDtypeStruct((length, count * rows), bf16)
+    blocks = count * steps
+    save_shape = jax.ShapeDtypeStruct((blocks, length, chunk), bf16)
     depth = d_out.shape[1]
     if fused:
-        in_specs.append(pl.BlockSpec((1, chunk, depth), lambda i, j, sc: (i, j, 0)))
-        args.append(recv)
-        spec = pl.BlockSpec(
-            (1, chunk // 2, depth // 2),
-            lambda i, j, sc: (i, jnp.bitwise_xor(j, sc[1] // inner), 0),
-        )
-        heads = [spec] * 4
-        shapes = [jax.ShapeDtypeStruct((count, rows // 2, depth // 2), bf16)] * 4
+        in_specs.append(whole)
+        args.append(recv.reshape(blocks, chunk, depth))
+        heads = [whole] * 4
+        shapes = [jax.ShapeDtypeStruct((blocks, chunk // 2, depth // 2), bf16)] * 4
     else:
-        heads = [pl.BlockSpec((1, chunk, depth), lambda i, j, sc: (i, j, 0))]
-        shapes = [jax.ShapeDtypeStruct((count, rows, depth), bf16)]
+        heads = [whole]
+        shapes = [jax.ShapeDtypeStruct((blocks, chunk, depth), bf16)]
     return pl.pallas_call(
-        functools.partial(forward_kernel, (span, chans, per, piece, inner, fused)),
+        functools.partial(forward_kernel, (span, chans, per, piece, inner, fused, resident, at)),
         grid_spec=pltpu.PrefetchScalarGridSpec(
             num_scalar_prefetch=1,
             grid=(count, steps),
             in_specs=in_specs,
-            out_specs=heads + [save] * 4,
+            out_specs=heads + [whole] * 4,
             scratch_shapes=[
                 pltpu.VMEM((length, chunk), bf16),
                 pltpu.VMEM((span, length // span * chans), bf16),
@@ -182,9 +185,11 @@
 
 
 def backward_kernel(cfg, sc, d_out, w, upper, m1, scaled_i, w1, w_mix, gain, shift, *rest):
-    span, chans, per = cfg
+    span, chans, per, base = cfg
+    here = pl.program_id(0)
+    save = base + here
     gu, gv, small, grad, dm_all, nm_all = rest[-6:]
-    blocks = upper.shape[0] // span
+    blocks = upper.shape[1] // span
     row = lax.broadcasted_iota(jnp.int32, (span, span), 0)
     col = lax.broadcasted_iota(jnp.int32, (span, span), 1)
     w_low = [jnp.where(row >= col, w_mix[g], jnp.zeros_like(w_mix[g])) for g in range(per)]
@@ -195,7 +200,7 @@
     acc_s = [jnp.zeros((8, chans), f32)] * per
     size = blocks // parts
     for h in range(parts):
-        grad[h * size * span : (h + 1) * size * span] = dot(d_out[h * size * span : (h + 1) * size * span], w[...], ((1,), (1,))).astype(bf16)
+        grad[h * size * span : (h + 1) * size * span] = dot(d_out[h * size * span : (h + 1) * size * span], w[here], ((1,), (1,))).astype(bf16)
     for h in range(parts):
         wide = slice(h * size * chans, (h + 1) * size * chans)
         for g in range(per):
@@ -204,9 +209,9 @@
                 rows = slice(b * span, (b + 1) * span)
                 at = slice(b * chans, (b + 1) * chans)
                 cot = grad[rows, lanes].astype(f32)
-                gu[rows, lanes] = (cot * m1[rows, lanes].astype(f32)).astype(bf16)
-                dm_all[g, :, at] = (cot * upper[rows, lanes].astype(f32)).astype(bf16)
-                scaled = scaled_i[rows, lanes].astype(f32)
+                gu[rows, lanes] = (cot * m1[save, rows, lanes].astype(f32)).astype(bf16)
+                dm_all[g, :, at] = (cot * upper[save, rows, lanes].astype(f32)).astype(bf16)
+                scaled = scaled_i[save, rows, lanes].astype(f32)
                 nm_all[g, :span, at] = (scaled * gain[g] + shift[g]).astype(bf16)
             both = dot(dm_all[g, :, wide], nm_all[g, :, wide], ((1,), (1,)))
             acc[g] = both if h == 0 else acc[g] + both
@@ -215,7 +220,7 @@
                 rows = slice(b * span, (b + 1) * span)
                 k = b - h * size
                 dn = dn_all[:, k * chans : (k + 1) * chans]
-                scaled = scaled_i[rows, lanes].astype(f32)
+                scaled = scaled_i[save, rows, lanes].astype(f32)
                 prod = dn * scaled
                 acc_g[g] = acc_g[g] + jnp.sum(prod.reshape(-1, 8, chans), axis=0)
                 acc_s[g] = acc_s[g] + jnp.sum(dn.reshape(-1, 8, chans), axis=0)
@@ -223,7 +228,7 @@
                 mean_e = jnp.mean(e, axis=1, keepdims=True)
                 mean_s = jnp.mean(prod * gain[g], axis=1, keepdims=True)
                 gv[rows, lanes] = (
-                    w1[rows, lanes].astype(f32) * (e - mean_e - scaled * mean_s)
+                    w1[save, rows, lanes].astype(f32) * (e - mean_e - scaled * mean_s)
                 ).astype(bf16)
     lines, mats = [], []
     for g in range(per):
@@ -236,7 +241,7 @@
     square = jnp.where(row >= col, even, jnp.transpose(odd))
     pad = jnp.zeros((LINES - 7, span), f32)
     lines = jnp.concatenate(lines + [diag, pad], axis=0)
-    encode(small, 0, square, lines)
+    encode(small, here, square, lines)
 
 
 def backward(sc, rel, index, d_out, w, saves, w_mix, gain, shift, carried):
@@ -253,20 +258,14 @@
     def at(j, sc):
         return jnp.bitwise_xor(rel, sc[0]) * steps + j
 
-    save = pl.BlockSpec((length, chunk), lambda j, sc: (0, index * steps + j))
+    whole = pl.BlockSpec(memory_space=pltpu.VMEM)
     vec = pl.BlockSpec((per, 1, span), lambda j, sc: (at(j, sc), 0, 0))
-    in_specs = [
-        pl.BlockSpec(memory_space=pltpu.VMEM),
-        pl.BlockSpec((chunk, depth), lambda j, sc: (j, 0)),
-        save,
-        save,
-        save,
-        save,
+    in_specs = [whole] * 6 + [
         pl.BlockSpec((per, span, span), lambda j, sc: (at(j, sc), 0, 0)),
         vec,
         vec,
     ]
-    args = [d_out, w, *saves, w_mix, gain, shift]
+    args = [d_out, w.reshape(steps, chunk, depth), *saves, w_mix, gain, shift]
     aliases = {}
     if carried is not None:
         for k, value in enumerate(carried):
@@ -276,7 +275,7 @@
     out = pl.BlockSpec((length, chunk), lambda j, sc: (0, at(j, sc)))
     shape = jax.ShapeDtypeStruct((length, width), bf16)
     return pl.pallas_call(
-        functools.partial(backward_kernel, (span, chans, per)),
+        functools.partial(backward_kernel, (span, chans, per, index * steps)),
         grid_spec=pltpu.PrefetchScalarGridSpec(
             num_scalar_prefetch=1,
             grid=(steps,),
@@ -284,7 +283,7 @@
             out_specs=[
                 out,
                 out,
-                pl.BlockSpec((1, span + 2 * LINES, span), lambda j, sc: (j, 0, 0)),
+                whole,
             ],
             scratch_shapes=[
                 pltpu.VMEM((length, chunk), bf16),
@@ -317,15 +316,13 @@
                 keep[i, j] = add(k[i, j, 0], r[i, j, 0])
 
 
-def join_kernel(k1, r1, k2, r2, out):
-    out[:, 0] = add(k1[...], r1[...])
-    out[:, 1] = add(k2[...], r2[...])
-
-
-def join_more_kernel(k1, r1, k2, r2, more, out):
-    for side, (k, r) in enumerate(((k1, r1), (k2, r2))):
-        total = k[...].astype(f32) + r[...].astype(f32)
-        out[:, side] = (total + more[:, side].astype(f32)).astype(bf16)
+def join_kernel(k, r, out):
+    out[...] = add(k[...], r[...])
+
+
+def join_more_kernel(k, r, more, out):
+    total = k[...].astype(f32) + r[...].astype(f32)
+    out[...] = (total + more[...].astype(f32)).astype(bf16)
 
 
 def merge_kernel(mine, got, out):
@@ -369,14 +366,9 @@
     )(sc, *blocks)
 
 
-def flip_kernel(step, value, got, *outs):
-    for side in range(value.shape[0]):
-        for j in range(value.shape[1]):
-            sums = add(value[side, j], got[side, j ^ step])
-            if len(outs) == 1:
-                outs[0][side, j] = sums
-            else:
-                outs[side][j] = sums
+def flip_kernel(step, value, got, out):
+    for j in range(value.shape[0]):
+        out[j] = add(value[j], got[j ^ step])
 
 
 def local(body, shapes, *args):
@@ -390,31 +382,33 @@
 
 
 def assemble_kernel(sc, *refs):
-    *parts, out = refs
-    half = parts[0].shape[-1]
-    piece = parts[0].shape[1]
-    for side in range(2):
-        for low in range(4):
-            at = jnp.bitwise_xor(low, jnp.bitwise_and(sc[1], 3)) * piece
-            rows = pl.ds(pl.multiple_of(at, piece), piece)
-            lanes = slice(side * half, (side + 1) * half)
-            out[rows, lanes] = parts[4 * side + low][0].astype(f32)
-
-
-def assemble(sc, parts):
+    parts, out = refs[:4], refs[-1]
+    rest, piece, _ = parts[0].shape
+    for low in range(4):
+        for high in range(rest):
+            at = jnp.bitwise_xor(4 * high + low, sc[1]) * piece
+            out[pl.ds(pl.multiple_of(at, piece), piece), :] = parts[low][high].astype(f32)
+
+
+def assemble(sc, side, parts, carried):
     rest, piece, half = parts[0].shape
-    spec = pl.BlockSpec((1, piece, half), lambda h, sc: (jnp.bitwise_xor(h, sc[1] // 4), 0, 0))
+    in_specs = [pl.BlockSpec(memory_space=pltpu.VMEM)] * 4
+    args = list(parts)
+    if carried is not None:
+        in_specs.append(pl.BlockSpec(memory_space=pl.ANY))
+        args.append(carried)
     return pl.pallas_call(
         assemble_kernel,
         grid_spec=pltpu.PrefetchScalarGridSpec(
             num_scalar_prefetch=1,
-            grid=(rest,),
-            in_specs=[spec] * 8,
-            out_specs=pl.BlockSpec((4 * piece, 2 * half), lambda h, sc: (h, 0)),
+            grid=(1,),
+            in_specs=in_specs,
+            out_specs=pl.BlockSpec((rest * 4 * piece, half), lambda p, sc: (0, side)),
         ),
         out_shape=jax.ShapeDtypeStruct((rest * 4 * piece, 2 * half), f32),
-        name="assemble",
-    )(sc, *parts)
+        input_output_aliases={} if carried is None else {5: 0},
+        compiler_params=pltpu.CompilerParams(vmem_limit_bytes=VMEM),
+    )(sc, *args)
 
 
 def bits_of(count):
@@ -430,7 +424,8 @@
             packed[rel ^ bit] = local(merge_kernel, [mine.shape], mine, got)[0]
     value = packed[0]
     for bit in sp_bits:
-        value = local(merge_kernel, [value.shape], value, swap(value, bit, 0))[0]
+        got = swap(value, bit, 0)
+        value = local(merge_kernel, [value.shape], value, got)[0]
     blocks = {0: value}
     for bit in dp_bits[1:] + [dp_bits[0]]:
         for rel in list(blocks):
@@ -447,8 +442,9 @@
     d = d_out.reshape(-1, d_out.shape[2])
     sc = jnp.stack([lax.axis_index("dp"), lax.axis_index("sp")]).astype(jnp.int32)
     bias, gain, shift = (a[:, None, :] for a in (mix_bias, norm_gain, norm_shift))
-    u, v, w_mix, bias, gain, shift = (
-        pltpu.with_memory_space_constraint(a, pltpu.HBM) for a in (u, v, w_mix, bias, gain, shift)
+    u_far, v_far, w_mix, bias, gain, shift = (
+        pltpu.with_memory_space_constraint(a, pltpu.HBM)
+        for a in (u, v, w_mix, bias, gain, shift)
     )
 
     sp_bits, dp_bits = bits_of(num_sp), bits_of(num_dp)
@@ -468,7 +464,11 @@
     saves, heads = {}, {}
 
     def front(rel, recv):
-        out = forward(sc, rel, count, u, v, d, w_mix, bias, gain, shift, recv)
+        if rel == num_dp - 1:
+            big = (False, u_far, v_far, d)
+        else:
+            big = (True, u, v, d)
+        out = forward(sc, rel, count, *big, w_mix, bias, gain, shift, recv)
         kept = out[-4:]
         for i in range(count):
             saves[rel - 2 * i] = (kept, i)
@@ -506,32 +506,33 @@
     carried = back(2, carried)
     t1b, k1b, t2b, k2b = split(k1b, r1b, k2b, r2b)
     r1b, r2b = swap(t1b, bit_b, 0), swap(t2b, bit_a, 0)
-    stacked = (count, 2, rest, piece, half)
-    send = local(join_kernel, [stacked], k1a, r1a, k2a, r2a)[0]
-    both_r = swap(send, 0, dp_bits[-1])
+    ends_a, ends_b = ((k1a, r1a), (k2a, r2a)), ((k1b, r1b), (k2b, r2b))
+    chip = []
+    for pair in ends_a:
+        send = local(join_kernel, [done], *pair)[0]
+        chip.append(swap(send, 0, dp_bits[-1]))
     carried = back(3, carried)
-    both = local(join_more_kernel, [stacked], k1b, r1b, k2b, r2b, both_r)[0]
+    sides = [local(join_more_kernel, [done], *pair, x)[0] for pair, x in zip(ends_b, chip)]
     for bit in reversed(dp_bits[1:-1]):
-        middle = both.shape[0] // 2
-        both = add(both[middle:], swap(both[:middle], 0, bit))
-    both = both[0]
+        middle = sides[0].shape[0] // 2
+        sides = [add(x[middle:], swap(x[:middle], 0, bit)) for x in sides]
+    sides = [x[0] for x in sides]
     for k, bit in enumerate(others):
-        got = swap(both, bit, 0)
+        got = [swap(x, bit, 0) for x in sides]
         if k == len(others) - 1:
-            shapes = [(rest, piece, half)] * 2
             for rel in list(range(4, num_dp)) + [0]:
                 carried = back(rel, carried)
-        else:
-            shapes = [both.shape]
-        out = local(functools.partial(flip_kernel, 1 << k), shapes, both, got)
-        both = out[0]
-    a, b = out
+        flip = functools.partial(flip_kernel, 1 << k)
+        sides = [local(flip, [x.shape], x, y)[0] for x, y in zip(sides, got)]
     grad_u, grad_v = carried
-    a1, b2 = swap(a, bit_a, 0), swap(b, bit_b, 0)
-    a2, b1 = swap(a, bit_b, 0), swap(b, bit_a, 0)
-    a3, b3 = swap(a1, bit_b, 0), swap(b2, bit_a, 0)
-    grad_w_out = assemble(sc, [a, a1, a2, a3, b, b1, b2, b3])
-    grads = unpack(sc, reduce_small(packed), groups)
+    grad_w_out = None
+    for side, (x, near, far) in enumerate(zip(sides, (bit_a, bit_b), (bit_b, bit_a))):
+        one, two = swap(x, near, 0), swap(x, far, 0)
+        three = swap(one, far, 0)
+        middle = (one, two) if near == bit_a else (two, one)
+        grad_w_out = assemble(sc, side, [x, *middle, three], grad_w_out)
+    small = reduce_small(packed)
+    grads = unpack(sc, small, groups)
     return (grad_u.reshape(shape), grad_v.reshape(shape), grad_w_out, *grads)
 
 

time: 185 us -> 173 us (0.935)
  waiting for transfers between devices: 79.8 us -> 63.9 us
  starting transfers between devices: 27.6 us -> 35.7 us
  Pallas kernels: 72.8 us -> 69.5 us
    ppermute x30 -> x32, waiting for transfers between devices: 79.8 us -> 63.9 us  [swap(): return lax.ppermute(value, AXES, pairs)]
    ppermute x30 -> x32, starting transfers between devices: 27.6 us -> 35.7 us  [swap(): return lax.ppermute(value, AXES, pairs)]
    pallas_call x4, Pallas kernels: 36.2 us -> 33.3 us  [forward(): pl.pallas_call(functools.partial(forward_kernel, (span, chans, per, piece...]
    pallas_call x1 -> x2, Pallas kernels: 4.16 us -> 4 us  [assemble(): pl.pallas_call(assemble_kernel, grid_spec=pltpu.PrefetchScalarGridSpec(nu...]
  transfers between devices with their start and end apart: 30 -> 32, of which waited for: 11 -> 11; matrix products, arithmetic and copies ran while one was open for 0% -> 0% of each run, Pallas kernels for 38% -> 39%
where the time goes in v3:
time: 173 us; the launch traced here: 172 us
  Pallas kernels  69.5 us (40%)
  waiting for transfers between devices  63.9 us (37%)
  starting transfers between devices  35.7 us (21%)
  local copies, waits for them, and re-layouts  2.21 us (1%)
    ppermute x32, waiting for transfers between devices, swap(): return lax.ppermute(value, AXES, pairs)  63.9 us
    ppermute x32, starting transfers between devices, swap(): return lax.ppermute(value, AXES, pairs)  35.7 us
    pallas_call x4, Pallas kernels, forward(): pl.pallas_call(functools.partial(forward_kernel, (span, chans, per, piece...  33.3 us
    pallas_call x4, Pallas kernels, backward(): pl.pallas_call(functools.partial(backward_kernel, (span, chans, per, inde...  29.4 us
    pallas_call x2, Pallas kernels, assemble(): pl.pallas_call(assemble_kernel, grid_spec=pltpu.PrefetchScalarGridSpec(nu...  4 us
  transfers between devices with their start and end apart: 32, of which 11 were waited for; matrix products, arithmetic and copies ran while one was open for 0% of the time, Pallas kernels for 39%

profile of v3, /device:TPU:0, one launch (start us, length us, event | category | flops | bytes accessed | tf_op | source)
XLA Modules:
  0.0 172.1 jit_solution(3111654770802264862)
XLA Ops:
  0.6 3.0 %collective-permute-start.1 = (bf16[512,2048]{1,0:T(8,128)(2,1)}, bf16[512,2048]{1,0:T(8,128)(2,1)S(1)}, u32[]{:S(2)}, u32[]{:S(2)}) collective-permute-start(bf16[512,2048]{1,0:T(8,128)(2,1)} %param.15), channel_id=1, source_target_pairs={{0,2},{1,3},{2,0},{3,1},{4,6},{5,7},{6,4},{7,5},{8,10},{9,11},{10,... | collective-permute-start | bytes 6291464 | tf_op jit(solution)/shard_map/ppermute | solution.py:27
  3.7 2.2 %copy-done = bf16[1,1024,2048]{2,1,0:T(8,128)(2,1)S(1)} copy-done((bf16[1,1024,2048]{2,1,0:T(8,128)(2,1)S(1)}, bf16[1,1024,2048]{2,1,0:T(8,128)(2,1)}, u32[]{:S(2)}) %copy-start) | copy-done | bytes 4194328
  5.9 8.3 %shard_map.137 = (bf16[2,256,2048]{2,1,0:T(8,128)(2,1)S(1)}, bf16[2,1024,256]{2,1,0:T(8,128)(2,1)S(1)}, bf16[2,1024,256]{2,1,0:T(8,128)(2,1)S(1)}, bf16[2,1024,2...) custom-call(s32[2]{0:T(128)S(1)} %pad_add_fusion.sc, bf16[1024,2048]{1,0:T(8,128)(2,1)} %bitcast.32, ...), custom_call_target="tpu_custom_call" | custom-call | flops 2147483648 | tf_op jit(solution)/shard_map/pallas_call | solution.py:150
  14.4 7.7 %shard_map.135 = (bf16[2,256,2048]{2,1,0:T(8,128)(2,1)S(1)}, bf16[2,1024,256]{2,1,0:T(8,128)(2,1)S(1)}, bf16[2,1024,256]{2,1,0:T(8,128)(2,1)S(1)}, bf16[2,1024,2...) custom-call(s32[2]{0:T(128)S(1)} %pad_add_fusion.sc, bf16[1024,2048]{1,0:T(8,128)(2,1)S(1)} %bitcast.33, ...), custom_call_target="tpu_custom_call" | custom-call | flops 2147483648 | tf_op jit(solution)/shard_map/pallas_call | solution.py:150
  22.1 0.5 collective-permute-start
  22.7 26.8 %collective-permute-done.1 = bf16[512,2048]{1,0:T(8,128)(2,1)S(1)} collective-permute-done((bf16[512,2048]{1,0:T(8,128)(2,1)}, bf16[512,2048]{1,0:T(8,128)(2,1)S(1)}, u32[]{:S(2)}, u32[]{:S(2)}) %collective-permute-start.1) | collective-permute-done | bytes 2097184 | tf_op jit(solution)/shard_map/ppermute | solution.py:27
  49.5 8.5 %shard_map.138 = (bf16[2,128,1024]{2,1,0:T(8,128)(2,1)S(1)}, bf16[2,128,1024]{2,1,0:T(8,128)(2,1)S(1)}, bf16[2,128,1024]{2,1,0:T(8,128)(2,1)S(1)}, bf16[2,128,10...) custom-call(s32[2]{0:T(128)S(1)} %pad_add_fusion.sc, ...), custom_call_target="tpu_custom_call" | custom-call | flops 2147483648 | tf_op jit(solution)/shard_map/pallas_call | solution.py:150
  58.1 1.8 %collective-permute-start.8 = (bf16[2,128,1024]{2,1,0:T(8,128)(2,1)S(1)}, bf16[2,128,1024]{2,1,0:T(8,128)(2,1)S(1)}, u32[]{:S(2)}, u32[]{:S(2)}) collective-permute-start(bf16[2,128,1024]{2,1,0:T(8,128)(2,1)S(1)} %get-tuple-element.90), channel_id=1, source_target_pairs={{0,4},{1,5},{2,6},{3,7},{4,0},{5,1},{6,2},{7,3},{8,12},{9,13},{10,... | collective-permute-start | bytes 1572872 | tf_op jit(solution)/shard_map/ppermute | solution.py:27
  59.9 1.6 collective-permute-start.9
  61.5 8.7 %shard_map.136 = (bf16[2,128,1024]{2,1,0:T(8,128)(2,1)S(1)}, bf16[2,128,1024]{2,1,0:T(8,128)(2,1)S(1)}, bf16[2,128,1024]{2,1,0:T(8,128)(2,1)S(1)}, bf16[2,128,10...) custom-call(s32[2]{0:T(128)S(1)} %pad_add_fusion.sc, ...), custom_call_target="tpu_custom_call" | custom-call | flops 2147483648 | tf_op jit(solution)/shard_map/pallas_call | solution.py:150
  70.2 0.6 collective-permute-start.5
  70.8 1.7 collective-permute-done.8
  72.5 2.3 %collective-permute-start.6 = (bf16[2,128,1024]{2,1,0:T(8,128)(2,1)S(1)}, bf16[2,128,1024]{2,1,0:T(8,128)(2,1)S(1)}, u32[]{:S(2)}, u32[]{:S(2)}) collective-permute-start(bf16[2,128,1024]{2,1,0:T(8,128)(2,1)S(1)} %get-tuple-element.86), channel_id=1, source_target_pairs={{0,8},{1,9},{2,10},{3,11},{4,12},{5,13},{6,14},{7,15},{8,0},{9,1},... | collective-permute-start | bytes 1572872 | tf_op jit(solution)/shard_map/ppermute | solution.py:27
  75.0 0.8 collective-permute-start.17
  75.8 8.2 %collective-permute-done.5 = bf16[2,128,1024]{2,1,0:T(8,128)(2,1)S(1)} collective-permute-done((bf16[2,128,1024]{2,1,0:T(8,128)(2,1)S(1)}, bf16[2,128,1024]{2,1,0:T(8,128)(2,1)S(1)}, u32[]{:S(2)}, u32[]{:S(2)}) %collective-permute-start.5) | collective-permute-done | bytes 524320 | tf_op jit(solution)/shard_map/ppermute | solution.py:27
  84.0 1.4 collective-permute-start.10
  85.4 2.1 %collective-permute-done.6 = bf16[2,128,1024]{2,1,0:T(8,128)(2,1)S(1)} collective-permute-done((bf16[2,128,1024]{2,1,0:T(8,128)(2,1)S(1)}, bf16[2,128,1024]{2,1,0:T(8,128)(2,1)S(1)}, u32[]{:S(2)}, u32[]{:S(2)}) %collective-permute-start.6) | collective-permute-done | bytes 524320 | tf_op jit(solution)/shard_map/ppermute | solution.py:27
  87.8 2.1 %collective-permute-start.16 = (bf16[1,2,64,1024]{3,2,1,0:T(8,128)(2,1)S(1)}, bf16[1,2,64,1024]{3,2,1,0:T(8,128)(2,1)S(1)}, u32[]{:S(2)}, u32[]{:S(2)}) collective-permute-start(bf16[1,2,64,1024]{3,2,1,0:T(8,128)(2,1)S(1)} %get-tuple-element.96), channel_id=1, source_target_pairs={{0,8},{1,9},{2,10},{3,11},{4,12},{5,13},{6,14},{7,15},{8,0},{9,1},... | collective-permute-start | bytes 786440 | tf_op jit(solution)/shard_map/ppermute | solution.py:27
  89.9 3.3 %collective-permute-done.17.r = bf16[1,2,64,1024]{3,2,1,0:T(8,128)(2,1)S(1)} collective-permute-done((bf16[1,2,64,1024]{3,2,1,0:T(8,128)(2,1)S(1)}, bf16[1,2,64,1024]{3,2,1,0:T(8,128)(2,1)S(1)}, u32[]{:S(2)}, u32[]{:S(2)}) %collective-permute-start.17) | collective-permute-done | bytes 262176 | tf_op jit(solution)/shard_map/ppermute | solution.py:27
  93.2 2.0 %collective-permute-start.7 = (bf16[1,2,64,1024]{3,2,1,0:T(8,128)(2,1)S(1)}, bf16[1,2,64,1024]{3,2,1,0:T(8,128)(2,1)S(1)}, u32[]{:S(2)}, u32[]{:S(2)}) collective-permute-start(bf16[1,2,64,1024]{3,2,1,0:T(8,128)(2,1)S(1)} %get-tuple-element.88), channel_id=1, source_target_pairs={{0,4},{1,5},{2,6},{3,7},{4,0},{5,1},{6,2},{7,3},{8,12},{9,13},{10,... | collective-permute-start | bytes 786440 | tf_op jit(solution)/shard_map/ppermute | solution.py:27
  95.2 1.6 collective-permute-start.18
  96.8 0.6 collective-permute-start.11
  97.4 7.2 %shard_map.139 = (bf16[1024,2048]{1,0:T(8,128)(2,1)}, bf16[1024,2048]{1,0:T(8,128)(2,1)}, bf16[2,160,128]{2,1,0:T(8,128)(2,1)S(1)}) custom-call(s32[2]{0:T(128)S(1)} %pad_add_fusion.sc, bf16[1024,2048]{1,0:T(8,128)(2,1)S(1)} %bitcast.28, bf16[2,256,2048]{2,1,0:T(8,128)(2,1)S(1)} %bitcast.43, bf16[2,1024,256]{2,1,0:T(8,128)(2,1)S(1)} %get-tuple-element.71.upper, ...), custom_call_target="tpu_custom_call" | custom-call | flops 2147483648 | tf_op jit(solution)/shard_map/pallas_call | solution.py:277
  104.7 7.3 %shard_map.140 = (bf16[1024,2048]{1,0:T(8,128)(2,1)}, bf16[1024,2048]{1,0:T(8,128)(2,1)}, bf16[2,160,128]{2,1,0:T(8,128)(2,1)S(1)}) custom-call(s32[2]{0:T(128)S(1)} %pad_add_fusion.sc, bf16[1024,2048]{1,0:T(8,128)(2,1)S(1)} %bitcast.29, bf16[2,256,2048]{2,1,0:T(8,128)(2,1)S(1)} %bitcast.41, ...), custom_call_target="tpu_custom_call", output_to_operand_aliasing={{0}: (10, {}), {1}: (11, {})} | custom-call | flops 2147483648 | tf_op jit(solution)/shard_map/pallas_call | solution.py:277
  112.1 2.7 %collective-permute-start.19 = (bf16[2,64,1024]{2,1,0:T(8,128)(2,1)S(1)}, bf16[2,64,1024]{2,1,0:T(8,128)(2,1)S(1)}, u32[]{:S(2)}, u32[]{:S(2)}) collective-permute-start(bf16[2,64,1024]{2,1,0:T(8,128)(2,1)S(1)} %bitcast.44), channel_id=1, source_target_pairs={{0,16},{1,17},{2,18},{3,19},{4,20},{5,21},{6,22},{7,23},{8,24},{9,... | collective-permute-start | bytes 786440 | tf_op jit(solution)/shard_map/ppermute | solution.py:27
  115.3 7.3 %shard_map.141 = (bf16[1024,2048]{1,0:T(8,128)(2,1)}, bf16[1024,2048]{1,0:T(8,128)(2,1)}, bf16[2,160,128]{2,1,0:T(8,128)(2,1)S(1)}) custom-call(s32[2]{0:T(128)S(1)} %pad_add_fusion.sc, bf16[1024,2048]{1,0:T(8,128)(2,1)S(1)} %bitcast.30, bf16[2,256,2048]{2,1,0:T(8,128)(2,1)S(1)} %bitcast.42, ...), custom_call_target="tpu_custom_call", output_to_operand_aliasing={{0}: (10, {}), {1}: (11, {})} | custom-call | flops 2147483648 | tf_op jit(solution)/shard_map/pallas_call | solution.py:277
  122.6 0.5 collective-permute-start.23
  123.1 6.1 %collective-permute-done.19.got = bf16[2,64,1024]{2,1,0:T(8,128)(2,1)S(1)} collective-permute-done((bf16[2,64,1024]{2,1,0:T(8,128)(2,1)S(1)}, bf16[2,64,1024]{2,1,0:T(8,128)(2,1)S(1)}, u32[]{:S(2)}, u32[]{:S(2)}) %collective-permute-start.19) | collective-permute-done | bytes 262176 | tf_op jit(solution)/shard_map/ppermute | solution.py:27
  129.3 0.7 collective-permute-start.20
  130.0 3.7 %collective-permute-done.12.got = bf16[2,64,1024]{2,1,0:T(8,128)(2,1)S(1)} collective-permute-done((bf16[2,64,1024]{2,1,0:T(8,128)(2,1)S(1)}, bf16[2,64,1024]{2,1,0:T(8,128)(2,1)S(1)}, u32[]{:S(2)}, u32[]{:S(2)}) %collective-permute-start.12) | collective-permute-done | bytes 262176 | tf_op jit(solution)/shard_map/ppermute | solution.py:27
  133.8 0.8 collective-permute-start.14
  134.6 1.5 collective-permute-start.25
  136.1 7.5 %shard_map.142 = (bf16[1024,2048]{1,0:T(8,128)(2,1)}, bf16[1024,2048]{1,0:T(8,128)(2,1)}, bf16[2,160,128]{2,1,0:T(8,128)(2,1)S(1)}) custom-call(s32[2]{0:T(128)S(1)} %pad_add_fusion.sc, bf16[1024,2048]{1,0:T(8,128)(2,1)S(1)} %bitcast.31, bf16[2,256,2048]{2,1,0:T(8,128)(2,1)S(1)} %bitcast.40, ...), custom_call_target="tpu_custom_call", output_to_operand_aliasing={{0}: (10, {}), {1}: (11, {})} | custom-call | flops 2147483648 | tf_op jit(solution)/shard_map/pallas_call | solution.py:277
  143.7 0.8 collective-permute-start.26
  144.5 1.7 collective-permute-start.21
  146.2 2.0 %collective-permute-done.26.got = bf16[2,160,128]{2,1,0:T(8,128)(2,1)S(1)} collective-permute-done((bf16[2,160,128]{2,1,0:T(8,128)(2,1)S(1)}, bf16[2,160,128]{2,1,0:T(8,128)(2,1)S(1)}, u32[]{:S(2)}, u32[]{:S(2)}) %collective-permute-start.26) | collective-permute-done | bytes 81952 | tf_op jit(solution)/shard_map/ppermute | solution.py:27
  148.2 1.5 collective-permute-start.27
  149.7 0.6 collective-permute-start.22
  150.3 0.8 collective-permute-start.13
  151.1 1.2 collective-permute-start.15
  152.3 3.1 %collective-permute-done.27.got = bf16[2,160,128]{2,1,0:T(8,128)(2,1)S(1)} collective-permute-done((bf16[2,160,128]{2,1,0:T(8,128)(2,1)S(1)}, bf16[2,160,128]{2,1,0:T(8,128)(2,1)S(1)}, u32[]{:S(2)}, u32[]{:S(2)}) %collective-permute-start.27) | collective-permute-done | bytes 81952 | tf_op jit(solution)/shard_map/ppermute | solution.py:27
  155.5 3.4 %collective-permute-start.28 = (bf16[2,160,128]{2,1,0:T(8,128)(2,1)S(1)}, bf16[2,160,128]{2,1,0:T(8,128)(2,1)S(1)}, u32[]{:S(2)}, u32[]{:S(2)}) collective-permute-start(bf16[2,160,128]{2,1,0:T(8,128)(2,1)S(1)} %shard_map.157.mine), channel_id=1, source_target_pairs={{0,16},{1,17},{2,18},{3,19},{4,20},{5,21},{6,22},{7,23},{8,24},{9,... | collective-permute-start | bytes 245768 | tf_op jit(solution)/shard_map/ppermute | solution.py:27
  158.9 3.0 %collective-permute-done.28.got = bf16[2,160,128]{2,1,0:T(8,128)(2,1)S(1)} collective-permute-done((bf16[2,160,128]{2,1,0:T(8,128)(2,1)S(1)}, bf16[2,160,128]{2,1,0:T(8,128)(2,1)S(1)}, u32[]{:S(2)}, u32[]{:S(2)}) %collective-permute-start.28) | collective-permute-done | bytes 81952 | tf_op jit(solution)/shard_map/ppermute | solution.py:27
  161.9 0.7 collective-permute-start.30
  162.6 3.8 %collective-permute-done.30.refs_2_ = bf16[2,160,128]{2,1,0:T(8,128)(2,1)S(1)} collective-permute-done((bf16[2,160,128]{2,1,0:T(8,128)(2,1)S(1)}, bf16[2,160,128]{2,1,0:T(8,128)(2,1)S(1)}, u32[]{:S(2)}, u32[]{:S(2)}) %collective-permute-start.30) | collective-permute-done | bytes 81952 | tf_op jit(solution)/shard_map/ppermute | solution.py:27
  166.4 2.0 %shard_map.151.refs_4_ = f32[512,2048]{1,0:T(8,128)} custom-call(s32[2]{0:T(128)S(1)} %pad_add_fusion.sc, bf16[2,64,1024]{2,1,0:T(8,128)(2,1)S(1)} %shard_map.150.refs_0_, bf16[2,64,1024]{2,1,0:T(8,128)(2,1)S(1)} %collective-permute-done.20.refs_1_, bf16[2,64,1024]{2,1,0:T(8,128)(2,1)S(1)} %collective-permute-done.21.refs_2_, ...), custom_call_target="tpu_custom_call" | custom-call | tf_op jit(solution)/shard_map/pallas_call | solution.py:400
  168.4 2.0 %shard_map.152 = f32[512,2048]{1,0:T(8,128)} custom-call(s32[2]{0:T(128)S(1)} %pad_add_fusion.sc, bf16[2,64,1024]{2,1,0:T(8,128)(2,1)S(1)} %shard_map.147.refs_0_, bf16[2,64,1024]{2,1,0:T(8,128)(2,1)S(1)} %collective-permute-done.13.refs_1_, bf16[2,64,1024]{2,1,0:T(8,128)(2,1)S(1)} %collective-permute-done.14.refs_2_, ...), custom_call_target="tpu_custom_call", output_to_operand_aliasing={{}: (5, {})} | custom-call | tf_op jit(solution)/shard_map/pallas_call | solution.py:400
  170.5 1.7 unpack.1
  (56 shorter events, 1.8 us)
Async XLA Ops:
  0.6 48.9 %collective-permute-start.1 = (bf16[512,2048]{1,0:T(8,128)(2,1)}, bf16[512,2048]{1,0:T(8,128)(2,1)S(1)}, u32[]{:S(2)}, u32[]{:S(2)}) collective-permute-start(bf16[512,2048]{1,0:T(8,128)(2,1)} %param.15), channel_id=1, source_target_pairs={{0,2},{1,3},{2,0},{3,1},{4,6},{5,7},{6,4},{7,5},{8,10},{9,11},{10,... | collective-permute-start | bytes 6291464 | tf_op jit(solution)/shard_map/ppermute | solution.py:27
  3.7 2.2 %copy-start = (bf16[1,1024,2048]{2,1,0:T(8,128)(2,1)S(1)}, bf16[1,1024,2048]{2,1,0:T(8,128)(2,1)}, u32[]{:S(2)}) copy-start(bf16[1,1024,2048]{2,1,0:T(8,128)(2,1)} %param.10) | copy-start | bytes 12582916
  5.9 8.4 %copy-start.1 = (bf16[1,1024,2048]{2,1,0:T(8,128)(2,1)S(1)}, bf16[1,1024,2048]{2,1,0:T(8,128)(2,1)}, u32[]{:S(2)}) copy-start(bf16[1,1024,2048]{2,1,0:T(8,128)(2,1)} %param.10) | copy-start | bytes 12582916
  5.9 8.4 %copy-start.2 = (bf16[1,1024,2048]{2,1,0:T(8,128)(2,1)S(1)}, bf16[1,1024,2048]{2,1,0:T(8,128)(2,1)}, u32[]{:S(2)}) copy-start(bf16[1,1024,2048]{2,1,0:T(8,128)(2,1)} %param.8) | copy-start | bytes 12582916
  5.9 8.4 %copy-start.3 = (bf16[1,1024,2048]{2,1,0:T(8,128)(2,1)S(1)}, bf16[1,1024,2048]{2,1,0:T(8,128)(2,1)}, u32[]{:S(2)}) copy-start(bf16[1,1024,2048]{2,1,0:T(8,128)(2,1)} %param.9) | copy-start | bytes 12582916
  14.3 8.3 %copy-start.4 = (bf16[512,2048]{1,0:T(8,128)(2,1)S(1)}, bf16[512,2048]{1,0:T(8,128)(2,1)}, u32[]{:S(2)}) copy-start(bf16[512,2048]{1,0:T(8,128)(2,1)} %param.15) | copy-start | bytes 6291460
  14.3 35.2 %collective-permute-start.3 = (bf16[2,256,2048]{2,1,0:T(8,128)(2,1)S(1)}, bf16[2,256,2048]{2,1,0:T(8,128)(2,1)S(1)}, u32[]{:S(2)}, u32[]{:S(2)}) collective-permute-start(bf16[2,256,2048]{2,1,0:T(8,128)(2,1)S(1)} %get-tuple-element.66), channel_id=1, source_target_pairs={{0,1},{1,0},{2,3},{3,2},{4,5},{5,4},{6,7},{7,6},{8,9},{9,8},{10,11... | collective-permute-start | bytes 6291464 | tf_op jit(solution)/shard_map/ppermute | solution.py:27
  22.1 39.4 %collective-permute-start = (bf16[2,256,2048]{2,1,0:T(8,128)(2,1)S(1)}, bf16[2,256,2048]{2,1,0:T(8,128)(2,1)S(1)}, u32[]{:S(2)}, u32[]{:S(2)}) collective-permute-start(bf16[2,256,2048]{2,1,0:T(8,128)(2,1)S(1)} %get-tuple-element.57), channel_id=1, source_target_pairs={{0,1},{1,0},{2,3},{3,2},{4,5},{5,4},{6,7},{7,6},{8,9},{9,8},{10,11... | collective-permute-start | bytes 6291464 | tf_op jit(solution)/shard_map/ppermute | solution.py:27
  22.6 74.2 %collective-permute-start.4 = (bf16[512,2048]{1,0:T(8,128)(2,1)S(1)}, bf16[512,2048]{1,0:T(8,128)(2,1)S(1)}, u32[]{:S(2)}, u32[]{:S(2)}) collective-permute-start(bf16[512,2048]{1,0:T(8,128)(2,1)S(1)} %copy-done.4), channel_id=1, source_target_pairs={{0,1},{1,0},{2,3},{3,2},{4,5},{5,4},{6,7},{7,6},{8,9},{9,8},{10,11... | collective-permute-start | bytes 6291464 | tf_op jit(solution)/shard_map/ppermute | solution.py:27
  49.5 65.8 %collective-permute-start.2 = (bf16[512,2048]{1,0:T(8,128)(2,1)S(1)}, bf16[512,2048]{1,0:T(8,128)(2,1)S(1)}, u32[]{:S(2)}, u32[]{:S(2)}) collective-permute-start(bf16[512,2048]{1,0:T(8,128)(2,1)S(1)} %collective-permute-done.1), channel_id=1, source_target_pairs={{0,1},{1,0},{2,3},{3,2},{4,5},{5,4},{6,7},{7,6},{8,9},{9,8},{10,11... | collective-permute-start | bytes 6291464 | tf_op jit(solution)/shard_map/ppermute | solution.py:27
  58.1 12.2 %copy-start.5 = (bf16[2,1024,256]{2,1,0:T(8,128)(2,1)}, bf16[2,1024,256]{2,1,0:T(8,128)(2,1)S(1)}, u32[]{:S(2)}) copy-start(bf16[2,1024,256]{2,1,0:T(8,128)(2,1)S(1)} %get-tuple-element.70.w1) | copy-start | bytes 3145732
  58.1 14.4 %collective-permute-start.8 = (bf16[2,128,1024]{2,1,0:T(8,128)(2,1)S(1)}, bf16[2,128,1024]{2,1,0:T(8,128)(2,1)S(1)}, u32[]{:S(2)}, u32[]{:S(2)}) collective-permute-start(bf16[2,128,1024]{2,1,0:T(8,128)(2,1)S(1)} %get-tuple-element.90), channel_id=1, source_target_pairs={{0,4},{1,5},{2,6},{3,7},{4,0},{5,1},{6,2},{7,3},{8,12},{9,13},{10,... | collective-permute-start | bytes 1572872 | tf_op jit(solution)/shard_map/ppermute | solution.py:27
  59.9 14.9 %collective-permute-start.9 = (bf16[2,128,1024]{2,1,0:T(8,128)(2,1)S(1)}, bf16[2,128,1024]{2,1,0:T(8,128)(2,1)S(1)}, u32[]{:S(2)}, u32[]{:S(2)}) collective-permute-start(bf16[2,128,1024]{2,1,0:T(8,128)(2,1)S(1)} %get-tuple-element.92), channel_id=1, source_target_pairs={{0,8},{1,9},{2,10},{3,11},{4,12},{5,13},{6,14},{7,15},{8,0},{9,1},... | collective-permute-start | bytes 1572872 | tf_op jit(solution)/shard_map/ppermute | solution.py:27
  70.2 13.8 %collective-permute-start.5 = (bf16[2,128,1024]{2,1,0:T(8,128)(2,1)S(1)}, bf16[2,128,1024]{2,1,0:T(8,128)(2,1)S(1)}, u32[]{:S(2)}, u32[]{:S(2)}) collective-permute-start(bf16[2,128,1024]{2,1,0:T(8,128)(2,1)S(1)} %get-tuple-element.84), channel_id=1, source_target_pairs={{0,4},{1,5},{2,6},{3,7},{4,0},{5,1},{6,2},{7,3},{8,12},{9,13},{10,... | collective-permute-start | bytes 1572872 | tf_op jit(solution)/shard_map/ppermute | solution.py:27
  72.5 15.1 %collective-permute-start.6 = (bf16[2,128,1024]{2,1,0:T(8,128)(2,1)S(1)}, bf16[2,128,1024]{2,1,0:T(8,128)(2,1)S(1)}, u32[]{:S(2)}, u32[]{:S(2)}) collective-permute-start(bf16[2,128,1024]{2,1,0:T(8,128)(2,1)S(1)} %get-tuple-element.86), channel_id=1, source_target_pairs={{0,8},{1,9},{2,10},{3,11},{4,12},{5,13},{6,14},{7,15},{8,0},{9,1},... | collective-permute-start | bytes 1572872 | tf_op jit(solution)/shard_map/ppermute | solution.py:27
  75.0 18.1 %collective-permute-start.17 = (bf16[1,2,64,1024]{3,2,1,0:T(8,128)(2,1)S(1)}, bf16[1,2,64,1024]{3,2,1,0:T(8,128)(2,1)S(1)}, u32[]{:S(2)}, u32[]{:S(2)}) collective-permute-start(bf16[1,2,64,1024]{3,2,1,0:T(8,128)(2,1)S(1)} %get-tuple-element.98), channel_id=1, source_target_pairs={{0,8},{1,9},{2,10},{3,11},{4,12},{5,13},{6,14},{7,15},{8,0},{9,1},... | collective-permute-start | bytes 786440 | tf_op jit(solution)/shard_map/ppermute | solution.py:27
  84.0 11.2 %collective-permute-start.10 = (bf16[1,2,64,1024]{3,2,1,0:T(8,128)(2,1)S(1)}, bf16[1,2,64,1024]{3,2,1,0:T(8,128)(2,1)S(1)}, u32[]{:S(2)}, u32[]{:S(2)}) collective-permute-start(bf16[1,2,64,1024]{3,2,1,0:T(8,128)(2,1)S(1)} %get-tuple-element.94), channel_id=1, source_target_pairs={{0,4},{1,5},{2,6},{3,7},{4,0},{5,1},{6,2},{7,3},{8,12},{9,13},{10,... | collective-permute-start | bytes 786440 | tf_op jit(solution)/shard_map/ppermute | solution.py:27
  87.8 24.2 %collective-permute-start.16 = (bf16[1,2,64,1024]{3,2,1,0:T(8,128)(2,1)S(1)}, bf16[1,2,64,1024]{3,2,1,0:T(8,128)(2,1)S(1)}, u32[]{:S(2)}, u32[]{:S(2)}) collective-permute-start(bf16[1,2,64,1024]{3,2,1,0:T(8,128)(2,1)S(1)} %get-tuple-element.96), channel_id=1, source_target_pairs={{0,8},{1,9},{2,10},{3,11},{4,12},{5,13},{6,14},{7,15},{8,0},{9,1},... | collective-permute-start | bytes 786440 | tf_op jit(solution)/shard_map/ppermute | solution.py:27
  93.2 21.6 %collective-permute-start.7 = (bf16[1,2,64,1024]{3,2,1,0:T(8,128)(2,1)S(1)}, bf16[1,2,64,1024]{3,2,1,0:T(8,128)(2,1)S(1)}, u32[]{:S(2)}, u32[]{:S(2)}) collective-permute-start(bf16[1,2,64,1024]{3,2,1,0:T(8,128)(2,1)S(1)} %get-tuple-element.88), channel_id=1, source_target_pairs={{0,4},{1,5},{2,6},{3,7},{4,0},{5,1},{6,2},{7,3},{8,12},{9,13},{10,... | collective-permute-start | bytes 786440 | tf_op jit(solution)/shard_map/ppermute | solution.py:27
  95.2 16.8 %collective-permute-start.18 = (bf16[1,2,64,1024]{3,2,1,0:T(8,128)(2,1)S(1)}, bf16[1,2,64,1024]{3,2,1,0:T(8,128)(2,1)S(1)}, u32[]{:S(2)}, u32[]{:S(2)}) collective-permute-start(bf16[1,2,64,1024]{3,2,1,0:T(8,128)(2,1)S(1)} %shard_map.148), channel_id=1, source_target_pairs={{0,2},{1,3},{2,0},{3,1},{4,6},{5,7},{6,4},{7,5},{8,10},{9,11},{10,... | collective-permute-start | bytes 786440 | tf_op jit(solution)/shard_map/ppermute | solution.py:27
  96.8 17.9 %collective-permute-start.11 = (bf16[1,2,64,1024]{3,2,1,0:T(8,128)(2,1)S(1)}, bf16[1,2,64,1024]{3,2,1,0:T(8,128)(2,1)S(1)}, u32[]{:S(2)}, u32[]{:S(2)}) collective-permute-start(bf16[1,2,64,1024]{3,2,1,0:T(8,128)(2,1)S(1)} %shard_map.145), channel_id=1, source_target_pairs={{0,2},{1,3},{2,0},{3,1},{4,6},{5,7},{6,4},{7,5},{8,10},{9,11},{10,... | collective-permute-start | bytes 786440 | tf_op jit(solution)/shard_map/ppermute | solution.py:27
  97.4 7.2 %copy-start.6 = (bf16[2,1024,256]{2,1,0:T(8,128)(2,1)S(1)}, bf16[2,1024,256]{2,1,0:T(8,128)(2,1)}, u32[]{:S(2)}) copy-start(bf16[2,1024,256]{2,1,0:T(8,128)(2,1)} %copy-done.5) | copy-start | bytes 3145732
  112.1 17.1 %collective-permute-start.19 = (bf16[2,64,1024]{2,1,0:T(8,128)(2,1)S(1)}, bf16[2,64,1024]{2,1,0:T(8,128)(2,1)S(1)}, u32[]{:S(2)}, u32[]{:S(2)}) collective-permute-start(bf16[2,64,1024]{2,1,0:T(8,128)(2,1)S(1)} %bitcast.44), channel_id=1, source_target_pairs={{0,16},{1,17},{2,18},{3,19},{4,20},{5,21},{6,22},{7,23},{8,24},{9,... | collective-permute-start | bytes 786440 | tf_op jit(solution)/shard_map/ppermute | solution.py:27
  114.9 18.8 %collective-permute-start.12 = (bf16[2,64,1024]{2,1,0:T(8,128)(2,1)S(1)}, bf16[2,64,1024]{2,1,0:T(8,128)(2,1)S(1)}, u32[]{:S(2)}, u32[]{:S(2)}) collective-permute-start(bf16[2,64,1024]{2,1,0:T(8,128)(2,1)S(1)} %bitcast.46), channel_id=1, source_target_pairs={{0,16},{1,17},{2,18},{3,19},{4,20},{5,21},{6,22},{7,23},{8,24},{9,... | collective-permute-start | bytes 786440 | tf_op jit(solution)/shard_map/ppermute | solution.py:27
  122.6 11.9 %collective-permute-start.24 = (bf16[2,160,128]{2,1,0:T(8,128)(2,1)S(1)}, bf16[2,160,128]{2,1,0:T(8,128)(2,1)S(1)}, u32[]{:S(2)}, u32[]{:S(2)}) collective-permute-start(bf16[2,160,128]{2,1,0:T(8,128)(2,1)S(1)} %get-tuple-element.102), channel_id=1, source_target_pairs={{0,1},{1,0},{2,3},{3,2},{4,5},{5,4},{6,7},{7,6},{8,9},{9,8},{10,11... | collective-permute-start | bytes 245768 | tf_op jit(solution)/shard_map/ppermute | solution.py:27
  122.6 21.0 %collective-permute-start.23 = (bf16[2,160,128]{2,1,0:T(8,128)(2,1)S(1)}, bf16[2,160,128]{2,1,0:T(8,128)(2,1)S(1)}, u32[]{:S(2)}, u32[]{:S(2)}) collective-permute-start(bf16[2,160,128]{2,1,0:T(8,128)(2,1)S(1)} %get-tuple-element.100), channel_id=1, source_target_pairs={{0,1},{1,0},{2,3},{3,2},{4,5},{5,4},{6,7},{7,6},{8,9},{9,8},{10,11... | collective-permute-start | bytes 245768 | tf_op jit(solution)/shard_map/ppermute | solution.py:27
  129.3 20.4 %collective-permute-start.20 = (bf16[2,64,1024]{2,1,0:T(8,128)(2,1)S(1)}, bf16[2,64,1024]{2,1,0:T(8,128)(2,1)S(1)}, u32[]{:S(2)}, u32[]{:S(2)}) collective-permute-start(bf16[2,64,1024]{2,1,0:T(8,128)(2,1)S(1)} %shard_map.150.refs_0_), channel_id=1, source_target_pairs={{0,4},{1,5},{2,6},{3,7},{4,0},{5,1},{6,2},{7,3},{8,12},{9,13},{10,... | collective-permute-start | bytes 786440 | tf_op jit(solution)/shard_map/ppermute | solution.py:27
  133.8 17.3 %collective-permute-start.14 = (bf16[2,64,1024]{2,1,0:T(8,128)(2,1)S(1)}, bf16[2,64,1024]{2,1,0:T(8,128)(2,1)S(1)}, u32[]{:S(2)}, u32[]{:S(2)}) collective-permute-start(bf16[2,64,1024]{2,1,0:T(8,128)(2,1)S(1)} %shard_map.147.refs_0_), channel_id=1, source_target_pairs={{0,8},{1,9},{2,10},{3,11},{4,12},{5,13},{6,14},{7,15},{8,0},{9,1},... | collective-permute-start | bytes 786440 | tf_op jit(solution)/shard_map/ppermute | solution.py:27
  134.6 9.1 %collective-permute-start.25 = (bf16[2,160,128]{2,1,0:T(8,128)(2,1)S(1)}, bf16[2,160,128]{2,1,0:T(8,128)(2,1)S(1)}, u32[]{:S(2)}, u32[]{:S(2)}) collective-permute-start(bf16[2,160,128]{2,1,0:T(8,128)(2,1)S(1)} %shard_map.154), channel_id=1, source_target_pairs={{0,2},{1,3},{2,0},{3,1},{4,6},{5,7},{6,4},{7,5},{8,10},{9,11},{10,... | collective-permute-start | bytes 245768 | tf_op jit(solution)/shard_map/ppermute | solution.py:27
  143.7 4.5 %collective-permute-start.26 = (bf16[2,160,128]{2,1,0:T(8,128)(2,1)S(1)}, bf16[2,160,128]{2,1,0:T(8,128)(2,1)S(1)}, u32[]{:S(2)}, u32[]{:S(2)}) collective-permute-start(bf16[2,160,128]{2,1,0:T(8,128)(2,1)S(1)} %shard_map.155.mine), channel_id=1, source_target_pairs={{0,4},{1,5},{2,6},{3,7},{4,0},{5,1},{6,2},{7,3},{8,12},{9,13},{10,... | collective-permute-start | bytes 245768 | tf_op jit(solution)/shard_map/ppermute | solution.py:27
  144.5 18.1 %collective-permute-start.21 = (bf16[2,64,1024]{2,1,0:T(8,128)(2,1)S(1)}, bf16[2,64,1024]{2,1,0:T(8,128)(2,1)S(1)}, u32[]{:S(2)}, u32[]{:S(2)}) collective-permute-start(bf16[2,64,1024]{2,1,0:T(8,128)(2,1)S(1)} %shard_map.150.refs_0_), channel_id=1, source_target_pairs={{0,8},{1,9},{2,10},{3,11},{4,12},{5,13},{6,14},{7,15},{8,0},{9,1},... | collective-permute-start | bytes 786440 | tf_op jit(solution)/shard_map/ppermute | solution.py:27
  148.2 7.2 %collective-permute-start.27 = (bf16[2,160,128]{2,1,0:T(8,128)(2,1)S(1)}, bf16[2,160,128]{2,1,0:T(8,128)(2,1)S(1)}, u32[]{:S(2)}, u32[]{:S(2)}) collective-permute-start(bf16[2,160,128]{2,1,0:T(8,128)(2,1)S(1)} %shard_map.156.mine), channel_id=1, source_target_pairs={{0,8},{1,9},{2,10},{3,11},{4,12},{5,13},{6,14},{7,15},{8,0},{9,1},... | collective-permute-start | bytes 245768 | tf_op jit(solution)/shard_map/ppermute | solution.py:27
  149.7 16.7 %collective-permute-start.22 = (bf16[2,64,1024]{2,1,0:T(8,128)(2,1)S(1)}, bf16[2,64,1024]{2,1,0:T(8,128)(2,1)S(1)}, u32[]{:S(2)}, u32[]{:S(2)}) collective-permute-start(bf16[2,64,1024]{2,1,0:T(8,128)(2,1)S(1)} %collective-permute-done.20.refs_1_), channel_id=1, source_target_pairs={{0,8},{1,9},{2,10},{3,11},{4,12},{5,13},{6,14},{7,15},{8,0},{9,1},... | collective-permute-start | bytes 786440 | tf_op jit(solution)/shard_map/ppermute | solution.py:27
  150.3 18.1 %collective-permute-start.13 = (bf16[2,64,1024]{2,1,0:T(8,128)(2,1)S(1)}, bf16[2,64,1024]{2,1,0:T(8,128)(2,1)S(1)}, u32[]{:S(2)}, u32[]{:S(2)}) collective-permute-start(bf16[2,64,1024]{2,1,0:T(8,128)(2,1)S(1)} %shard_map.147.refs_0_), channel_id=1, source_target_pairs={{0,4},{1,5},{2,6},{3,7},{4,0},{5,1},{6,2},{7,3},{8,12},{9,13},{10,... | collective-permute-start | bytes 786440 | tf_op jit(solution)/shard_map/ppermute | solution.py:27
  151.1 17.4 %collective-permute-start.15 = (bf16[2,64,1024]{2,1,0:T(8,128)(2,1)S(1)}, bf16[2,64,1024]{2,1,0:T(8,128)(2,1)S(1)}, u32[]{:S(2)}, u32[]{:S(2)}) collective-permute-start(bf16[2,64,1024]{2,1,0:T(8,128)(2,1)S(1)} %collective-permute-done.14.refs_2_), channel_id=1, source_target_pairs={{0,4},{1,5},{2,6},{3,7},{4,0},{5,1},{6,2},{7,3},{8,12},{9,13},{10,... | collective-permute-start | bytes 786440 | tf_op jit(solution)/shard_map/ppermute | solution.py:27
  155.5 6.4 %collective-permute-start.28 = (bf16[2,160,128]{2,1,0:T(8,128)(2,1)S(1)}, bf16[2,160,128]{2,1,0:T(8,128)(2,1)S(1)}, u32[]{:S(2)}, u32[]{:S(2)}) collective-permute-start(bf16[2,160,128]{2,1,0:T(8,128)(2,1)S(1)} %shard_map.157.mine), channel_id=1, source_target_pairs={{0,16},{1,17},{2,18},{3,19},{4,20},{5,21},{6,22},{7,23},{8,24},{9,... | collective-permute-start | bytes 245768 | tf_op jit(solution)/shard_map/ppermute | solution.py:27
  161.9 4.5 %collective-permute-start.30 = (bf16[2,160,128]{2,1,0:T(8,128)(2,1)S(1)}, bf16[2,160,128]{2,1,0:T(8,128)(2,1)S(1)}, u32[]{:S(2)}, u32[]{:S(2)}) collective-permute-start(bf16[2,160,128]{2,1,0:T(8,128)(2,1)S(1)} %shard_map.158.refs_0_), channel_id=1, source_target_pairs={{0,2},{1,3},{2,0},{3,1},{4,6},{5,7},{6,4},{7,5},{8,10},{9,11},{10,... | collective-permute-start | bytes 245768 | tf_op jit(solution)/shard_map/ppermute | solution.py:27
  162.6 7.8 %collective-permute-start.29 = (bf16[2,160,128]{2,1,0:T(8,128)(2,1)S(1)}, bf16[2,160,128]{2,1,0:T(8,128)(2,1)S(1)}, u32[]{:S(2)}, u32[]{:S(2)}) collective-permute-start(bf16[2,160,128]{2,1,0:T(8,128)(2,1)S(1)} %shard_map.158.refs_0_), channel_id=1, source_target_pairs={{0,1},{1,0},{2,3},{3,2},{4,5},{5,4},{6,7},{7,6},{8,9},{9,8},{10,11... | collective-permute-start | bytes 245768 | tf_op jit(solution)/shard_map/ppermute | solution.py:27
  166.4 4.0 %collective-permute-start.31 = (bf16[2,160,128]{2,1,0:T(8,128)(2,1)S(1)}, bf16[2,160,128]{2,1,0:T(8,128)(2,1)S(1)}, u32[]{:S(2)}, u32[]{:S(2)}) collective-permute-start(bf16[2,160,128]{2,1,0:T(8,128)(2,1)S(1)} %collective-permute-done.30.refs_2_), channel_id=1, source_target_pairs={{0,1},{1,0},{2,3},{3,2},{4,5},{5,4},{6,7},{7,6},{8,9},{9,8},{10,11... | collective-permute-start | bytes 245768 | tf_op jit(solution)/shard_map/ppermute | solution.py:27

commit v4 on v3

--- a/solution.py
+++ b/solution.py
@@ -39,6 +39,8 @@
     else:
         part, upper_o, m1_o, scaled_o, w1_o, gated, wide = rest
     blocks = u.shape[0] // span
+    first = place(pl.program_id(0), pl.program_id(1), sc) * per
+    base = first if resident else 0
 
     row = lax.broadcasted_iota(jnp.int32, (span, span), 0)
     col = lax.broadcasted_iota(jnp.int32, (span, span), 1)
@@ -46,8 +48,7 @@
         lanes = slice(g * chans, (g + 1) * chans)
         source = lanes
         if resident:
-            start = (place(pl.program_id(0), pl.program_id(1), sc) * per + g) * chans
-            source = pl.ds(pl.multiple_of(start, chans), chans)
+            source = pl.ds(pl.multiple_of((first + g) * chans, chans), chans)
         for b in range(blocks):
             rows = slice(b * span, (b + 1) * span)
             c = v[rows, source].astype(f32)
@@ -60,12 +61,13 @@
             var = jnp.mean(centre * centre, axis=1, keepdims=True)
             inv = lax.rsqrt(var + EPS)
             scaled = centre * inv
-            wide[:, b * chans : (b + 1) * chans] = (scaled * gain[g] + shift[g]).astype(bf16)
+            wide[:, b * chans : (b + 1) * chans] = (scaled * gain[base + g] + shift[base + g]).astype(bf16)
             scaled_o[here, rows, lanes] = scaled.astype(bf16)
             w1_o[here, rows, lanes] = (dv * inv).astype(bf16)
-        w_low = jnp.where(row >= col, w_mix[g], jnp.zeros_like(w_mix[g]))
+        w_low = w_mix[base + g]
+        w_low = jnp.where(row >= col, w_low, jnp.zeros_like(w_low))
         mixed_all = dot(w_low, wide[...], ((1,), (0,)))
-        offset = jnp.transpose(jnp.broadcast_to(bias[g], (chans, span)))
+        offset = jnp.transpose(jnp.broadcast_to(bias[base + g], (chans, span)))
         for b in range(blocks):
             rows = slice(b * span, (b + 1) * span)
             a = u[rows, source].astype(f32)
@@ -82,29 +84,24 @@
         part[here] = dot(gated[...], d_out[...], ((0,), (0,))).astype(bf16)
         return
     half = d_out.shape[1] // 2
-    count = per * chans // piece
+    own = sc[1] % inner
     there = pl.program_id(0) * pl.num_programs(1) + jnp.bitwise_xor(pl.program_id(1), sc[1] // inner)
     for side, (send, keep) in enumerate(((s1, k1), (s2, k2))):
         lanes = slice(side * half, (side + 1) * half)
         total = dot(gated[...], d_out[:, lanes], ((0,), (0,)))
-        for p in range(count):
-            rows = slice(p * piece, (p + 1) * piece)
-            value = (total[rows] + recv[here, rows, lanes].astype(f32)).astype(bf16)
-            rel = jnp.bitwise_xor(p, sc[1] % inner)
-            low, high = rel % 2, rel // 2
-            if side == 0:
-                flag, at = low, high
-            else:
-                flag, at = high % 2, (high // 2) * 2 + low
+        total = (total + recv[here, :, lanes].astype(f32)).astype(bf16)
+        swapped = jnp.bitwise_and(own // (1 << side), 1) == 1
+        for p in range(per * chans // piece):
+            if p & (1 << side):
+                continue
+            q = p + (1 << side)
+            low = total[p * piece : (p + 1) * piece]
+            high = total[q * piece : (q + 1) * piece]
+            rel = jnp.bitwise_xor(p, own)
+            at = rel // 2 if side == 0 else rel // 4 * 2 + rel % 2
             where = pl.ds(pl.multiple_of(at * piece, piece), piece)
-
-            @pl.when(flag == 1)
-            def _():
-                send[there, where, :] = value
-
-            @pl.when(flag == 0)
-            def _():
-                keep[there, where, :] = value
+            send[there, where, :] = jnp.where(swapped, low, high)
+            keep[there, where, :] = jnp.where(swapped, high, low)
 
 
 def forward(sc, first, count, resident, u, v, d_out, w_mix, bias, gain, shift, recv):
@@ -124,17 +121,17 @@
         return jnp.bitwise_xor(first - 2 * i, sc[0]) * steps + j
 
     wide = pl.BlockSpec((length, chunk), lambda i, j, sc: (0, at(i, j, sc)))
-    vec = pl.BlockSpec((per, 1, span), lambda i, j, sc: (at(i, j, sc), 0, 0))
     whole = pl.BlockSpec(memory_space=pltpu.VMEM)
     in_specs = [
         whole if resident else wide,
         whole if resident else wide,
         whole,
-        pl.BlockSpec((per, span, span), lambda i, j, sc: (at(i, j, sc), 0, 0)),
-        vec,
-        vec,
-        vec,
     ]
+    if resident:
+        in_specs += [whole] * 4
+    else:
+        in_specs.append(pl.BlockSpec((per, span, span), lambda i, j, sc: (at(i, j, sc), 0, 0)))
+        in_specs += [pl.BlockSpec((per, 1, span), lambda i, j, sc: (at(i, j, sc), 0, 0))] * 3
     args = [u, v, d_out, w_mix, bias, gain, shift]
     blocks = count * steps
     save_shape = jax.ShapeDtypeStruct((blocks, length, chunk), bf16)
@@ -185,14 +182,16 @@
 
 
 def backward_kernel(cfg, sc, d_out, w, upper, m1, scaled_i, w1, w_mix, gain, shift, *rest):
-    span, chans, per, base = cfg
+    span, chans, per, base, place = cfg
     here = pl.program_id(0)
+    first = place(here, sc) * per
     save = base + here
     gu, gv, small, grad, dm_all, nm_all = rest[-6:]
     blocks = upper.shape[1] // span
     row = lax.broadcasted_iota(jnp.int32, (span, span), 0)
     col = lax.broadcasted_iota(jnp.int32, (span, span), 1)
-    w_low = [jnp.where(row >= col, w_mix[g], jnp.zeros_like(w_mix[g])) for g in range(per)]
+    w_low = [w_mix[first + g] for g in range(per)]
+    w_low = [jnp.where(row >= col, m, jnp.zeros_like(m)) for m in w_low]
     nm_all[:, span:, :] = jnp.ones((per, span, nm_all.shape[2]), bf16)
     parts = 2
     acc = [None] * per
@@ -212,7 +211,7 @@
                 gu[rows, lanes] = (cot * m1[save, rows, lanes].astype(f32)).astype(bf16)
                 dm_all[g, :, at] = (cot * upper[save, rows, lanes].astype(f32)).astype(bf16)
                 scaled = scaled_i[save, rows, lanes].astype(f32)
-                nm_all[g, :span, at] = (scaled * gain[g] + shift[g]).astype(bf16)
+                nm_all[g, :span, at] = (scaled * gain[first + g] + shift[first + g]).astype(bf16)
             both = dot(dm_all[g, :, wide], nm_all[g, :, wide], ((1,), (1,)))
             acc[g] = both if h == 0 else acc[g] + both
             dn_all = dot(w_low[g], dm_all[g, :, wide], ((0,), (0,)))
@@ -224,9 +223,9 @@
                 prod = dn * scaled
                 acc_g[g] = acc_g[g] + jnp.sum(prod.reshape(-1, 8, chans), axis=0)
                 acc_s[g] = acc_s[g] + jnp.sum(dn.reshape(-1, 8, chans), axis=0)
-                e = dn * gain[g]
+                e = dn * gain[first + g]
                 mean_e = jnp.mean(e, axis=1, keepdims=True)
-                mean_s = jnp.mean(prod * gain[g], axis=1, keepdims=True)
+                mean_s = jnp.mean(prod * gain[first + g], axis=1, keepdims=True)
                 gv[rows, lanes] = (
                     w1[save, rows, lanes].astype(f32) * (e - mean_e - scaled * mean_s)
                 ).astype(bf16)
@@ -259,12 +258,7 @@
         return jnp.bitwise_xor(rel, sc[0]) * steps + j
 
     whole = pl.BlockSpec(memory_space=pltpu.VMEM)
-    vec = pl.BlockSpec((per, 1, span), lambda j, sc: (at(j, sc), 0, 0))
-    in_specs = [whole] * 6 + [
-        pl.BlockSpec((per, span, span), lambda j, sc: (at(j, sc), 0, 0)),
-        vec,
-        vec,
-    ]
+    in_specs = [whole] * 9
     args = [d_out, w.reshape(steps, chunk, depth), *saves, w_mix, gain, shift]
     aliases = {}
     if carried is not None:
@@ -275,7 +269,7 @@
     out = pl.BlockSpec((length, chunk), lambda j, sc: (0, at(j, sc)))
     shape = jax.ShapeDtypeStruct((length, width), bf16)
     return pl.pallas_call(
-        functools.partial(backward_kernel, (span, chans, per, index * steps)),
+        functools.partial(backward_kernel, (span, chans, per, index * steps, at)),
         grid_spec=pltpu.PrefetchScalarGridSpec(
             num_scalar_prefetch=1,
             grid=(steps,),
@@ -442,9 +436,9 @@
     d = d_out.reshape(-1, d_out.shape[2])
     sc = jnp.stack([lax.axis_index("dp"), lax.axis_index("sp")]).astype(jnp.int32)
     bias, gain, shift = (a[:, None, :] for a in (mix_bias, norm_gain, norm_shift))
-    u_far, v_far, w_mix, bias, gain, shift = (
-        pltpu.with_memory_space_constraint(a, pltpu.HBM)
-        for a in (u, v, w_mix, bias, gain, shift)
+    small = (w_mix, bias, gain, shift)
+    u_far, v_far, *small_far = (
+        pltpu.with_memory_space_constraint(a, pltpu.HBM) for a in (u, v, *small)
     )
 
     sp_bits, dp_bits = bits_of(num_sp), bits_of(num_dp)
@@ -465,10 +459,9 @@
 
     def front(rel, recv):
         if rel == num_dp - 1:
-            big = (False, u_far, v_far, d)
+            out = forward(sc, rel, count, False, u_far, v_far, d, *small_far, recv)
         else:
-            big = (True, u, v, d)
-        out = forward(sc, rel, count, *big, w_mix, bias, gain, shift, recv)
+            out = forward(sc, rel, count, True, u, v, d, *small, recv)
         kept = out[-4:]
         for i in range(count):
             saves[rel - 2 * i] = (kept, i)
@@ -503,7 +496,7 @@
     carried = back(1, None)
     t1a, k1a, t2a, k2a = split(k1a, r1a, k2a, r2a)
     r1a, r2a = swap(t1a, bit_b, 0), swap(t2a, bit_a, 0)
-    carried = back(2, carried)
+    carried = back(0, carried)
     t1b, k1b, t2b, k2b = split(k1b, r1b, k2b, r2b)
     r1b, r2b = swap(t1b, bit_b, 0), swap(t2b, bit_a, 0)
     ends_a, ends_b = ((k1a, r1a), (k2a, r2a)), ((k1b, r1b), (k2b, r2b))
@@ -511,7 +504,7 @@
     for pair in ends_a:
         send = local(join_kernel, [done], *pair)[0]
         chip.append(swap(send, 0, dp_bits[-1]))
-    carried = back(3, carried)
+    carried = back(2, carried)
     sides = [local(join_more_kernel, [done], *pair, x)[0] for pair, x in zip(ends_b, chip)]
     for bit in reversed(dp_bits[1:-1]):
         middle = sides[0].shape[0] // 2
@@ -520,19 +513,22 @@
     for k, bit in enumerate(others):
         got = [swap(x, bit, 0) for x in sides]
         if k == len(others) - 1:
-            for rel in list(range(4, num_dp)) + [0]:
+            for rel in range(3, num_dp):
                 carried = back(rel, carried)
         flip = functools.partial(flip_kernel, 1 << k)
         sides = [local(flip, [x.shape], x, y)[0] for x, y in zip(sides, got)]
     grad_u, grad_v = carried
-    grad_w_out = None
-    for side, (x, near, far) in enumerate(zip(sides, (bit_a, bit_b), (bit_b, bit_a))):
+    pieces = []
+    for x, near, far in zip(sides, (bit_a, bit_b), (bit_b, bit_a)):
         one, two = swap(x, near, 0), swap(x, far, 0)
         three = swap(one, far, 0)
         middle = (one, two) if near == bit_a else (two, one)
-        grad_w_out = assemble(sc, side, [x, *middle, three], grad_w_out)
-    small = reduce_small(packed)
-    grads = unpack(sc, small, groups)
+        pieces.append([x, *middle, three])
+    grad_w_out = None
+    for side in (1, 0):
+        grad_w_out = assemble(sc, side, pieces[side], grad_w_out)
+    sums = reduce_small(packed)
+    grads = unpack(sc, sums, groups)
     return (grad_u.reshape(shape), grad_v.reshape(shape), grad_w_out, *grads)
 
 

time: 173 us -> 168 us (0.971)
  Pallas kernels: 69.5 us -> 61.7 us
  waiting for transfers between devices: 63.9 us -> 68.2 us
  starting transfers between devices: 35.7 us -> 32.5 us
    ppermute x32, waiting for transfers between devices: 63.9 us -> 68.2 us  [swap(): return lax.ppermute(value, AXES, pairs)]
    pallas_call x4, Pallas kernels: 33.3 us -> 29.3 us  [forward(): pl.pallas_call(functools.partial(forward_kernel, (span, chans, per, piece...]
    pallas_call x4, Pallas kernels: 29.4 us -> 25.6 us  [backward(): pl.pallas_call(functools.partial(backward_kernel, (span, chans, per, inde...]
    ppermute x32, starting transfers between devices: 35.7 us -> 32.5 us  [swap(): return lax.ppermute(value, AXES, pairs)]
  transfers between devices with their start and end apart: 32 -> 32, of which waited for: 11 -> 12; matrix products, arithmetic and copies ran while one was open for 0% -> 0% of each run, Pallas kernels for 39% -> 36%
where the time goes in v4:
time: 168 us; the launch traced here: 166 us
  waiting for transfers between devices  68.2 us (41%)
  Pallas kernels  61.7 us (37%)
  starting transfers between devices  32.5 us (19%)
  local copies, waits for them, and re-layouts  3.03 us (2%)
    ppermute x32, waiting for transfers between devices, swap(): return lax.ppermute(value, AXES, pairs)  68.2 us
    ppermute x32, starting transfers between devices, swap(): return lax.ppermute(value, AXES, pairs)  32.5 us
    pallas_call x4, Pallas kernels, forward(): pl.pallas_call(functools.partial(forward_kernel, (span, chans, per, piece...  29.3 us
    pallas_call x4, Pallas kernels, backward(): pl.pallas_call(functools.partial(backward_kernel, (span, chans, per, inde...  25.6 us
    pallas_call x2, Pallas kernels, assemble(): pl.pallas_call(assemble_kernel, grid_spec=pltpu.PrefetchScalarGridSpec(nu...  4 us
  transfers between devices with their start and end apart: 32, of which 12 were waited for; matrix products, arithmetic and copies ran while one was open for 0% of the time, Pallas kernels for 36%

profile of v4, /device:TPU:0, one launch (start us, length us, event | category | flops | bytes accessed | tf_op | source)
XLA Modules:
  0.0 166.4 jit_solution(12756333810990872613)
XLA Ops:
  0.6 3.0 %collective-permute-start = (bf16[512,2048]{1,0:T(8,128)(2,1)}, bf16[512,2048]{1,0:T(8,128)(2,1)S(1)}, u32[]{:S(2)}, u32[]{:S(2)}) collective-permute-start(bf16[512,2048]{1,0:T(8,128)(2,1)} %param.15), channel_id=1, source_target_pairs={{0,2},{1,3},{2,0},{3,1},{4,6},{5,7},{6,4},{7,5},{8,10},{9,11},{10,... | collective-permute-start | bytes 6291464 | tf_op jit(solution)/shard_map/ppermute | solution.py:27
  3.7 2.2 %copy-done = bf16[1,1024,2048]{2,1,0:T(8,128)(2,1)S(1)} copy-done((bf16[1,1024,2048]{2,1,0:T(8,128)(2,1)S(1)}, bf16[1,1024,2048]{2,1,0:T(8,128)(2,1)}, u32[]{:S(2)}) %copy-start) | copy-done | bytes 4194328
  6.0 8.3 %shard_map.135 = (bf16[2,256,2048]{2,1,0:T(8,128)(2,1)S(1)}, bf16[2,1024,256]{2,1,0:T(8,128)(2,1)S(1)}, bf16[2,1024,256]{2,1,0:T(8,128)(2,1)S(1)}, bf16[2,1024,2...) custom-call(s32[2]{0:T(128)S(1)} %pad_add_fusion.sc, bf16[1024,2048]{1,0:T(8,128)(2,1)} %bitcast.32, ...), custom_call_target="tpu_custom_call" | custom-call | flops 2147483648 | tf_op jit(solution)/shard_map/pallas_call | solution.py:147
  14.5 6.7 %shard_map.137 = (bf16[2,256,2048]{2,1,0:T(8,128)(2,1)S(1)}, bf16[2,1024,256]{2,1,0:T(8,128)(2,1)S(1)}, bf16[2,1024,256]{2,1,0:T(8,128)(2,1)S(1)}, bf16[2,1024,2...) custom-call(s32[2]{0:T(128)S(1)} %pad_add_fusion.sc, bf16[1024,2048]{1,0:T(8,128)(2,1)S(1)} %bitcast.33, ...), custom_call_target="tpu_custom_call" | custom-call | flops 2147483648 | tf_op jit(solution)/shard_map/pallas_call | solution.py:147
  21.2 0.5 collective-permute-start.3
  21.8 27.7 %collective-permute-done = bf16[512,2048]{1,0:T(8,128)(2,1)S(1)} collective-permute-done((bf16[512,2048]{1,0:T(8,128)(2,1)}, bf16[512,2048]{1,0:T(8,128)(2,1)S(1)}, u32[]{:S(2)}, u32[]{:S(2)}) %collective-permute-start) | collective-permute-done | bytes 2097184 | tf_op jit(solution)/shard_map/ppermute | solution.py:27
  49.5 6.9 %shard_map.136 = (bf16[2,128,1024]{2,1,0:T(8,128)(2,1)S(1)}, bf16[2,128,1024]{2,1,0:T(8,128)(2,1)S(1)}, bf16[2,128,1024]{2,1,0:T(8,128)(2,1)S(1)}, bf16[2,128,10...) custom-call(s32[2]{0:T(128)S(1)} %pad_add_fusion.sc, ...), custom_call_target="tpu_custom_call" | custom-call | flops 2147483648 | tf_op jit(solution)/shard_map/pallas_call | solution.py:147
  56.5 0.8 copy-done.10
  57.2 1.8 %collective-permute-start.8 = (bf16[2,128,1024]{2,1,0:T(8,128)(2,1)S(1)}, bf16[2,128,1024]{2,1,0:T(8,128)(2,1)S(1)}, u32[]{:S(2)}, u32[]{:S(2)}) collective-permute-start(bf16[2,128,1024]{2,1,0:T(8,128)(2,1)S(1)} %get-tuple-element.90), channel_id=1, source_target_pairs={{0,4},{1,5},{2,6},{3,7},{4,0},{5,1},{6,2},{7,3},{8,12},{9,13},{10,... | collective-permute-start | bytes 1572872 | tf_op jit(solution)/shard_map/ppermute | solution.py:27
  59.0 1.6 collective-permute-start.9
  60.6 7.3 %shard_map.138 = (bf16[2,128,1024]{2,1,0:T(8,128)(2,1)}, bf16[2,128,1024]{2,1,0:T(8,128)(2,1)S(1)}, bf16[2,128,1024]{2,1,0:T(8,128)(2,1)S(1)}, bf16[2,128,1024]{...) custom-call(s32[2]{0:T(128)S(1)} %pad_add_fusion.sc, ...), custom_call_target="tpu_custom_call" | custom-call | flops 2147483648 | tf_op jit(solution)/shard_map/pallas_call | solution.py:147
  67.9 0.5 collective-permute-start.5
  68.4 3.6 %collective-permute-done.8 = bf16[2,128,1024]{2,1,0:T(8,128)(2,1)S(1)} collective-permute-done((bf16[2,128,1024]{2,1,0:T(8,128)(2,1)S(1)}, bf16[2,128,1024]{2,1,0:T(8,128)(2,1)S(1)}, u32[]{:S(2)}, u32[]{:S(2)}) %collective-permute-start.8) | collective-permute-done | bytes 524320 | tf_op jit(solution)/shard_map/ppermute | solution.py:27
  72.0 1.8 %collective-permute-start.6 = (bf16[2,128,1024]{2,1,0:T(8,128)(2,1)S(1)}, bf16[2,128,1024]{2,1,0:T(8,128)(2,1)S(1)}, u32[]{:S(2)}, u32[]{:S(2)}) collective-permute-start(bf16[2,128,1024]{2,1,0:T(8,128)(2,1)S(1)} %get-tuple-element.86), channel_id=1, source_target_pairs={{0,8},{1,9},{2,10},{3,11},{4,12},{5,13},{6,14},{7,15},{8,0},{9,1},... | collective-permute-start | bytes 1572872 | tf_op jit(solution)/shard_map/ppermute | solution.py:27
  73.9 0.2 shard_map.144
  74.1 1.6 collective-permute-start.17
  75.7 7.6 %collective-permute-done.5 = bf16[2,128,1024]{2,1,0:T(8,128)(2,1)S(1)} collective-permute-done((bf16[2,128,1024]{2,1,0:T(8,128)(2,1)}, bf16[2,128,1024]{2,1,0:T(8,128)(2,1)S(1)}, u32[]{:S(2)}, u32[]{:S(2)}) %collective-permute-start.5) | collective-permute-done | bytes 524320 | tf_op jit(solution)/shard_map/ppermute | solution.py:27
  83.3 1.8 %collective-permute-start.10 = (bf16[1,2,64,1024]{3,2,1,0:T(8,128)(2,1)S(1)}, bf16[1,2,64,1024]{3,2,1,0:T(8,128)(2,1)S(1)}, u32[]{:S(2)}, u32[]{:S(2)}) collective-permute-start(bf16[1,2,64,1024]{3,2,1,0:T(8,128)(2,1)S(1)} %get-tuple-element.94), channel_id=1, source_target_pairs={{0,8},{1,9},{2,10},{3,11},{4,12},{5,13},{6,14},{7,15},{8,0},{9,1},... | collective-permute-start | bytes 786440 | tf_op jit(solution)/shard_map/ppermute | solution.py:27
  85.4 1.7 %collective-permute-start.16 = (bf16[1,2,64,1024]{3,2,1,0:T(8,128)(2,1)S(1)}, bf16[1,2,64,1024]{3,2,1,0:T(8,128)(2,1)S(1)}, u32[]{:S(2)}, u32[]{:S(2)}) collective-permute-start(bf16[1,2,64,1024]{3,2,1,0:T(8,128)(2,1)S(1)} %get-tuple-element.96), channel_id=1, source_target_pairs={{0,4},{1,5},{2,6},{3,7},{4,0},{5,1},{6,2},{7,3},{8,12},{9,13},{10,... | collective-permute-start | bytes 786440 | tf_op jit(solution)/shard_map/ppermute | solution.py:27
  87.2 1.7 %collective-permute-done.17.r = bf16[1,2,64,1024]{3,2,1,0:T(8,128)(2,1)S(1)} collective-permute-done((bf16[1,2,64,1024]{3,2,1,0:T(8,128)(2,1)S(1)}, bf16[1,2,64,1024]{3,2,1,0:T(8,128)(2,1)S(1)}, u32[]{:S(2)}, u32[]{:S(2)}) %collective-permute-start.17) | collective-permute-done | bytes 262176 | tf_op jit(solution)/shard_map/ppermute | solution.py:27
  88.9 1.8 %collective-permute-start.7 = (bf16[1,2,64,1024]{3,2,1,0:T(8,128)(2,1)S(1)}, bf16[1,2,64,1024]{3,2,1,0:T(8,128)(2,1)S(1)}, u32[]{:S(2)}, u32[]{:S(2)}) collective-permute-start(bf16[1,2,64,1024]{3,2,1,0:T(8,128)(2,1)S(1)} %get-tuple-element.88), channel_id=1, source_target_pairs={{0,8},{1,9},{2,10},{3,11},{4,12},{5,13},{6,14},{7,15},{8,0},{9,1},... | collective-permute-start | bytes 786440 | tf_op jit(solution)/shard_map/ppermute | solution.py:27
  90.8 1.6 collective-permute-start.18
  92.5 0.5 collective-permute-start.11
  93.0 6.4 %shard_map.139 = (bf16[1024,2048]{1,0:T(8,128)(2,1)}, bf16[1024,2048]{1,0:T(8,128)(2,1)}, bf16[2,160,128]{2,1,0:T(8,128)(2,1)S(1)}) custom-call(s32[2]{0:T(128)S(1)} %pad_add_fusion.sc, bf16[1024,2048]{1,0:T(8,128)(2,1)S(1)} %bitcast.28, bf16[2,256,2048]{2,1,0:T(8,128)(2,1)S(1)} %bitcast.43, bf16[2,1024,256]{2,1,0:T(8,128)(2,1)S(1)} %get-tuple-element.71.upper, ...), custom_call_target="tpu_custom_call" | custom-call | flops 2147483648 | tf_op jit(solution)/shard_map/pallas_call | solution.py:271
  99.5 6.4 %shard_map.140 = (bf16[1024,2048]{1,0:T(8,128)(2,1)}, bf16[1024,2048]{1,0:T(8,128)(2,1)}, bf16[2,160,128]{2,1,0:T(8,128)(2,1)S(1)}) custom-call(s32[2]{0:T(128)S(1)} %pad_add_fusion.sc, bf16[1024,2048]{1,0:T(8,128)(2,1)S(1)} %bitcast.29, bf16[2,256,2048]{2,1,0:T(8,128)(2,1)S(1)} %bitcast.40, ...), custom_call_target="tpu_custom_call", output_to_operand_aliasing={{0}: (10, {}), {1}: (11, {})} | custom-call | flops 2147483648 | tf_op jit(solution)/shard_map/pallas_call | solution.py:271
  106.0 2.7 %collective-permute-start.19 = (bf16[2,64,1024]{2,1,0:T(8,128)(2,1)S(1)}, bf16[2,64,1024]{2,1,0:T(8,128)(2,1)S(1)}, u32[]{:S(2)}, u32[]{:S(2)}) collective-permute-start(bf16[2,64,1024]{2,1,0:T(8,128)(2,1)S(1)} %bitcast.44), channel_id=1, source_target_pairs={{0,16},{1,17},{2,18},{3,19},{4,20},{5,21},{6,22},{7,23},{8,24},{9,... | collective-permute-start | bytes 786440 | tf_op jit(solution)/shard_map/ppermute | solution.py:27
  108.8 0.3 collective-permute-start.12
  109.2 6.3 %shard_map.141 = (bf16[1024,2048]{1,0:T(8,128)(2,1)}, bf16[1024,2048]{1,0:T(8,128)(2,1)}, bf16[2,160,128]{2,1,0:T(8,128)(2,1)S(1)}) custom-call(s32[2]{0:T(128)S(1)} %pad_add_fusion.sc, bf16[1024,2048]{1,0:T(8,128)(2,1)S(1)} %bitcast.30, bf16[2,256,2048]{2,1,0:T(8,128)(2,1)S(1)} %bitcast.41, ...), custom_call_target="tpu_custom_call", output_to_operand_aliasing={{0}: (10, {}), {1}: (11, {})} | custom-call | flops 2147483648 | tf_op jit(solution)/shard_map/pallas_call | solution.py:271
  115.5 6.4 %shard_map.142 = (bf16[1024,2048]{1,0:T(8,128)(2,1)}, bf16[1024,2048]{1,0:T(8,128)(2,1)}, bf16[2,160,128]{2,1,0:T(8,128)(2,1)S(1)}) custom-call(s32[2]{0:T(128)S(1)} %pad_add_fusion.sc, bf16[1024,2048]{1,0:T(8,128)(2,1)S(1)} %bitcast.31, bf16[2,256,2048]{2,1,0:T(8,128)(2,1)S(1)} %bitcast.42, ...), custom_call_target="tpu_custom_call", output_to_operand_aliasing={{0}: (10, {}), {1}: (11, {})} | custom-call | flops 2147483648 | tf_op jit(solution)/shard_map/pallas_call | solution.py:271
  122.0 3.4 %collective-permute-done.19.got = bf16[2,64,1024]{2,1,0:T(8,128)(2,1)S(1)} collective-permute-done((bf16[2,64,1024]{2,1,0:T(8,128)(2,1)S(1)}, bf16[2,64,1024]{2,1,0:T(8,128)(2,1)S(1)}, u32[]{:S(2)}, u32[]{:S(2)}) %collective-permute-start.19) | collective-permute-done | bytes 262176 | tf_op jit(solution)/shard_map/ppermute | solution.py:27
  125.7 4.8 %collective-permute-done.12.got = bf16[2,64,1024]{2,1,0:T(8,128)(2,1)S(1)} collective-permute-done((bf16[2,64,1024]{2,1,0:T(8,128)(2,1)S(1)}, bf16[2,64,1024]{2,1,0:T(8,128)(2,1)S(1)}, u32[]{:S(2)}, u32[]{:S(2)}) %collective-permute-start.12) | collective-permute-done | bytes 262176 | tf_op jit(solution)/shard_map/ppermute | solution.py:27
  130.5 1.6 collective-permute-start.13
  132.2 1.5 collective-permute-start.25
  133.7 3.3 %collective-permute-done.25.got = bf16[2,160,128]{2,1,0:T(8,128)(2,1)S(1)} collective-permute-done((bf16[2,160,128]{2,1,0:T(8,128)(2,1)S(1)}, bf16[2,160,128]{2,1,0:T(8,128)(2,1)S(1)}, u32[]{:S(2)}, u32[]{:S(2)}) %collective-permute-start.25) | collective-permute-done | bytes 81952 | tf_op jit(solution)/shard_map/ppermute | solution.py:27
  137.1 0.6 collective-permute-start.26
  137.7 1.5 collective-permute-start.20
  139.2 3.3 %collective-permute-done.26.got = bf16[2,160,128]{2,1,0:T(8,128)(2,1)S(1)} collective-permute-done((bf16[2,160,128]{2,1,0:T(8,128)(2,1)S(1)}, bf16[2,160,128]{2,1,0:T(8,128)(2,1)S(1)}, u32[]{:S(2)}, u32[]{:S(2)}) %collective-permute-start.26) | collective-permute-done | bytes 81952 | tf_op jit(solution)/shard_map/ppermute | solution.py:27
  142.5 0.3 collective-permute-start.27
  142.8 0.5 collective-permute-start.22
  143.3 1.8 %collective-permute-start.14 = (bf16[2,64,1024]{2,1,0:T(8,128)(2,1)S(1)}, bf16[2,64,1024]{2,1,0:T(8,128)(2,1)S(1)}, u32[]{:S(2)}, u32[]{:S(2)}) collective-permute-start(bf16[2,64,1024]{2,1,0:T(8,128)(2,1)S(1)} %shard_map.147.refs_0_), channel_id=1, source_target_pairs={{0,8},{1,9},{2,10},{3,11},{4,12},{5,13},{6,14},{7,15},{8,0},{9,1},... | collective-permute-start | bytes 786440 | tf_op jit(solution)/shard_map/ppermute | solution.py:27
  145.4 3.4 %collective-permute-done.27.got = bf16[2,160,128]{2,1,0:T(8,128)(2,1)S(1)} collective-permute-done((bf16[2,160,128]{2,1,0:T(8,128)(2,1)S(1)}, bf16[2,160,128]{2,1,0:T(8,128)(2,1)S(1)}, u32[]{:S(2)}, u32[]{:S(2)}) %collective-permute-start.27) | collective-permute-done | bytes 81952 | tf_op jit(solution)/shard_map/ppermute | solution.py:27
  148.8 1.1 collective-permute-start.28
  149.9 6.3 %collective-permute-done.28.got = bf16[2,160,128]{2,1,0:T(8,128)(2,1)S(1)} collective-permute-done((bf16[2,160,128]{2,1,0:T(8,128)(2,1)S(1)}, bf16[2,160,128]{2,1,0:T(8,128)(2,1)S(1)}, u32[]{:S(2)}, u32[]{:S(2)}) %collective-permute-start.28) | collective-permute-done | bytes 81952 | tf_op jit(solution)/shard_map/ppermute | solution.py:27
  156.2 1.5 collective-permute-start.30
  157.8 3.0 %collective-permute-done.30.refs_2_ = bf16[2,160,128]{2,1,0:T(8,128)(2,1)S(1)} collective-permute-done((bf16[2,160,128]{2,1,0:T(8,128)(2,1)S(1)}, bf16[2,160,128]{2,1,0:T(8,128)(2,1)S(1)}, u32[]{:S(2)}, u32[]{:S(2)}) %collective-permute-start.30) | collective-permute-done | bytes 81952 | tf_op jit(solution)/shard_map/ppermute | solution.py:27
  160.7 2.0 %shard_map.151.refs_4_ = f32[512,2048]{1,0:T(8,128)} custom-call(s32[2]{0:T(128)S(1)} %pad_add_fusion.sc, bf16[2,64,1024]{2,1,0:T(8,128)(2,1)S(1)} %shard_map.150.refs_0_, bf16[2,64,1024]{2,1,0:T(8,128)(2,1)S(1)} %collective-permute-done.20.refs_1_, bf16[2,64,1024]{2,1,0:T(8,128)(2,1)S(1)} %collective-permute-done.21.refs_2_, ...), custom_call_target="tpu_custom_call" | custom-call | tf_op jit(solution)/shard_map/pallas_call | solution.py:394
  162.7 2.0 %shard_map.152 = f32[512,2048]{1,0:T(8,128)} custom-call(s32[2]{0:T(128)S(1)} %pad_add_fusion.sc, bf16[2,64,1024]{2,1,0:T(8,128)(2,1)S(1)} %shard_map.147.refs_0_, bf16[2,64,1024]{2,1,0:T(8,128)(2,1)S(1)} %collective-permute-done.13.refs_1_, bf16[2,64,1024]{2,1,0:T(8,128)(2,1)S(1)} %collective-permute-done.14.refs_2_, ...), custom_call_target="tpu_custom_call", output_to_operand_aliasing={{}: (5, {})} | custom-call | tf_op jit(solution)/shard_map/pallas_call | solution.py:394
  164.7 1.7 %unpack.1 = (f32[16,128,128]{2,1,0:T(8,128)}, f32[16,128]{1,0:T(8,128)}, f32[16,128]{1,0:T(8,128)}, f32[16,128]{1,0:T(8,128)}) custom-call(s32[2]{0:T(128)S(1)} %pad_add_fusion.sc, bf16[2,160,128]{2,1,0:T(8,128)(2,1)S(1)} %shard_map.158.refs_0_, bf16[2,160,128]{2,1,0:T(8,128)(2,1)S(1)} %collective-permute-done.29.refs_1_, ...), custom_call_target="tpu_custom_call" | custom-call | tf_op jit(solution)/shard_map/unpack/pallas_call | solution.py:353
  (68 shorter events, 1.7 us)
Async XLA Ops:
  0.6 48.9 %collective-permute-start = (bf16[512,2048]{1,0:T(8,128)(2,1)}, bf16[512,2048]{1,0:T(8,128)(2,1)S(1)}, u32[]{:S(2)}, u32[]{:S(2)}) collective-permute-start(bf16[512,2048]{1,0:T(8,128)(2,1)} %param.15), channel_id=1, source_target_pairs={{0,2},{1,3},{2,0},{3,1},{4,6},{5,7},{6,4},{7,5},{8,10},{9,11},{10,... | collective-permute-start | bytes 6291464 | tf_op jit(solution)/shard_map/ppermute | solution.py:27
  3.7 2.2 %copy-start = (bf16[1,1024,2048]{2,1,0:T(8,128)(2,1)S(1)}, bf16[1,1024,2048]{2,1,0:T(8,128)(2,1)}, u32[]{:S(2)}) copy-start(bf16[1,1024,2048]{2,1,0:T(8,128)(2,1)} %param.10) | copy-start | bytes 12582916
  5.9 8.5 %copy-start.1 = (bf16[1,1024,2048]{2,1,0:T(8,128)(2,1)S(1)}, bf16[1,1024,2048]{2,1,0:T(8,128)(2,1)}, u32[]{:S(2)}) copy-start(bf16[1,1024,2048]{2,1,0:T(8,128)(2,1)} %param.10) | copy-start | bytes 12582916
  5.9 8.5 %copy-start.2 = (bf16[1,1024,2048]{2,1,0:T(8,128)(2,1)S(1)}, bf16[1,1024,2048]{2,1,0:T(8,128)(2,1)}, u32[]{:S(2)}) copy-start(bf16[1,1024,2048]{2,1,0:T(8,128)(2,1)} %param.8) | copy-start | bytes 12582916
  5.9 8.5 %copy-start.3 = (bf16[1,1024,2048]{2,1,0:T(8,128)(2,1)S(1)}, bf16[1,1024,2048]{2,1,0:T(8,128)(2,1)}, u32[]{:S(2)}) copy-start(bf16[1,1024,2048]{2,1,0:T(8,128)(2,1)} %param.9) | copy-start | bytes 12582916
  5.9 8.5 %copy-start.4 = (bf16[16,128,128]{2,1,0:T(8,128)(2,1)S(1)}, bf16[16,128,128]{2,1,0:T(8,128)(2,1)}, u32[]{:S(2)}) copy-start(bf16[16,128,128]{2,1,0:T(8,128)(2,1)} %w_mix.15) | copy-start | bytes 1572868
  5.9 8.5 %copy-start.8 = (f32[16,128]{1,0:T(8,128)S(1)}, f32[16,128]{1,0:T(8,128)}, u32[]{:S(2)}) copy-start(f32[16,128]{1,0:T(8,128)} %param.13) | copy-start | bytes 24580
  6.0 8.5 %copy-start.9 = (f32[16,128]{1,0:T(8,128)S(1)}, f32[16,128]{1,0:T(8,128)}, u32[]{:S(2)}) copy-start(f32[16,128]{1,0:T(8,128)} %param.14) | copy-start | bytes 24580
  6.0 8.5 %copy-start.12 = (f32[16,128]{1,0:T(8,128)S(1)}, f32[16,128]{1,0:T(8,128)}, u32[]{:S(2)}) copy-start(f32[16,128]{1,0:T(8,128)} %param.12) | copy-start | bytes 24580
  14.3 7.4 %copy-start.5 = (bf16[512,2048]{1,0:T(8,128)(2,1)S(1)}, bf16[512,2048]{1,0:T(8,128)(2,1)}, u32[]{:S(2)}) copy-start(bf16[512,2048]{1,0:T(8,128)(2,1)} %param.15) | copy-start | bytes 6291460
  14.3 35.2 %collective-permute-start.2 = (bf16[2,256,2048]{2,1,0:T(8,128)(2,1)S(1)}, bf16[2,256,2048]{2,1,0:T(8,128)(2,1)S(1)}, u32[]{:S(2)}, u32[]{:S(2)}) collective-permute-start(bf16[2,256,2048]{2,1,0:T(8,128)(2,1)S(1)} %get-tuple-element.61), channel_id=1, source_target_pairs={{0,1},{1,0},{2,3},{3,2},{4,5},{5,4},{6,7},{7,6},{8,9},{9,8},{10,11... | collective-permute-start | bytes 6291464 | tf_op jit(solution)/shard_map/ppermute | solution.py:27
  21.2 39.4 %collective-permute-start.3 = (bf16[2,256,2048]{2,1,0:T(8,128)(2,1)S(1)}, bf16[2,256,2048]{2,1,0:T(8,128)(2,1)S(1)}, u32[]{:S(2)}, u32[]{:S(2)}) collective-permute-start(bf16[2,256,2048]{2,1,0:T(8,128)(2,1)S(1)} %get-tuple-element.66), channel_id=1, source_target_pairs={{0,1},{1,0},{2,3},{3,2},{4,5},{5,4},{6,7},{7,6},{8,9},{9,8},{10,11... | collective-permute-start | bytes 6291464 | tf_op jit(solution)/shard_map/ppermute | solution.py:27
  21.7 70.7 %collective-permute-start.4 = (bf16[512,2048]{1,0:T(8,128)(2,1)S(1)}, bf16[512,2048]{1,0:T(8,128)(2,1)S(1)}, u32[]{:S(2)}, u32[]{:S(2)}) collective-permute-start(bf16[512,2048]{1,0:T(8,128)(2,1)S(1)} %copy-done.5), channel_id=1, source_target_pairs={{0,1},{1,0},{2,3},{3,2},{4,5},{5,4},{6,7},{7,6},{8,9},{9,8},{10,11... | collective-permute-start | bytes 6291464 | tf_op jit(solution)/shard_map/ppermute | solution.py:27
  49.5 66.0 %collective-permute-start.1 = (bf16[512,2048]{1,0:T(8,128)(2,1)S(1)}, bf16[512,2048]{1,0:T(8,128)(2,1)S(1)}, u32[]{:S(2)}, u32[]{:S(2)}) collective-permute-start(bf16[512,2048]{1,0:T(8,128)(2,1)S(1)} %collective-permute-done), channel_id=1, source_target_pairs={{0,1},{1,0},{2,3},{3,2},{4,5},{5,4},{6,7},{7,6},{8,9},{9,8},{10,11... | collective-permute-start | bytes 6291464 | tf_op jit(solution)/shard_map/ppermute | solution.py:27
  56.4 0.8 copy-start.10
  57.2 10.7 %copy-start.6 = (bf16[2,1024,256]{2,1,0:T(8,128)(2,1)}, bf16[2,1024,256]{2,1,0:T(8,128)(2,1)S(1)}, u32[]{:S(2)}) copy-start(bf16[2,1024,256]{2,1,0:T(8,128)(2,1)S(1)} %get-tuple-element.65.w1) | copy-start | bytes 3145732
  57.2 14.8 %collective-permute-start.8 = (bf16[2,128,1024]{2,1,0:T(8,128)(2,1)S(1)}, bf16[2,128,1024]{2,1,0:T(8,128)(2,1)S(1)}, u32[]{:S(2)}, u32[]{:S(2)}) collective-permute-start(bf16[2,128,1024]{2,1,0:T(8,128)(2,1)S(1)} %get-tuple-element.90), channel_id=1, source_target_pairs={{0,4},{1,5},{2,6},{3,7},{4,0},{5,1},{6,2},{7,3},{8,12},{9,13},{10,... | collective-permute-start | bytes 1572872 | tf_op jit(solution)/shard_map/ppermute | solution.py:27
  59.0 14.9 %copy-start.11 = (bf16[2,128,1024]{2,1,0:T(8,128)(2,1)S(1)}, bf16[2,128,1024]{2,1,0:T(8,128)(2,1)}, u32[]{:S(2)}) copy-start(bf16[2,128,1024]{2,1,0:T(8,128)(2,1)} %copy-done.10) | copy-start | bytes 1572868
  59.0 14.9 %collective-permute-start.9 = (bf16[2,128,1024]{2,1,0:T(8,128)(2,1)S(1)}, bf16[2,128,1024]{2,1,0:T(8,128)(2,1)S(1)}, u32[]{:S(2)}, u32[]{:S(2)}) collective-permute-start(bf16[2,128,1024]{2,1,0:T(8,128)(2,1)S(1)} %get-tuple-element.92), channel_id=1, source_target_pairs={{0,8},{1,9},{2,10},{3,11},{4,12},{5,13},{6,14},{7,15},{8,0},{9,1},... | collective-permute-start | bytes 1572872 | tf_op jit(solution)/shard_map/ppermute | solution.py:27
  67.9 15.4 %collective-permute-start.5 = (bf16[2,128,1024]{2,1,0:T(8,128)(2,1)}, bf16[2,128,1024]{2,1,0:T(8,128)(2,1)S(1)}, u32[]{:S(2)}, u32[]{:S(2)}) collective-permute-start(bf16[2,128,1024]{2,1,0:T(8,128)(2,1)} %get-tuple-element.84), channel_id=1, source_target_pairs={{0,4},{1,5},{2,6},{3,7},{4,0},{5,1},{6,2},{7,3},{8,12},{9,13},{10,... | collective-permute-start | bytes 1572872 | tf_op jit(solution)/shard_map/ppermute | solution.py:27
  72.0 13.1 %collective-permute-start.6 = (bf16[2,128,1024]{2,1,0:T(8,128)(2,1)S(1)}, bf16[2,128,1024]{2,1,0:T(8,128)(2,1)S(1)}, u32[]{:S(2)}, u32[]{:S(2)}) collective-permute-start(bf16[2,128,1024]{2,1,0:T(8,128)(2,1)S(1)} %get-tuple-element.86), channel_id=1, source_target_pairs={{0,8},{1,9},{2,10},{3,11},{4,12},{5,13},{6,14},{7,15},{8,0},{9,1},... | collective-permute-start | bytes 1572872 | tf_op jit(solution)/shard_map/ppermute | solution.py:27
  74.1 14.8 %collective-permute-start.17 = (bf16[1,2,64,1024]{3,2,1,0:T(8,128)(2,1)S(1)}, bf16[1,2,64,1024]{3,2,1,0:T(8,128)(2,1)S(1)}, u32[]{:S(2)}, u32[]{:S(2)}) collective-permute-start(bf16[1,2,64,1024]{3,2,1,0:T(8,128)(2,1)S(1)} %get-tuple-element.98), channel_id=1, source_target_pairs={{0,4},{1,5},{2,6},{3,7},{4,0},{5,1},{6,2},{7,3},{8,12},{9,13},{10,... | collective-permute-start | bytes 786440 | tf_op jit(solution)/shard_map/ppermute | solution.py:27
  83.3 7.5 %collective-permute-start.10 = (bf16[1,2,64,1024]{3,2,1,0:T(8,128)(2,1)S(1)}, bf16[1,2,64,1024]{3,2,1,0:T(8,128)(2,1)S(1)}, u32[]{:S(2)}, u32[]{:S(2)}) collective-permute-start(bf16[1,2,64,1024]{3,2,1,0:T(8,128)(2,1)S(1)} %get-tuple-element.94), channel_id=1, source_target_pairs={{0,8},{1,9},{2,10},{3,11},{4,12},{5,13},{6,14},{7,15},{8,0},{9,1},... | collective-permute-start | bytes 786440 | tf_op jit(solution)/shard_map/ppermute | solution.py:27
  85.4 20.5 %collective-permute-start.16 = (bf16[1,2,64,1024]{3,2,1,0:T(8,128)(2,1)S(1)}, bf16[1,2,64,1024]{3,2,1,0:T(8,128)(2,1)S(1)}, u32[]{:S(2)}, u32[]{:S(2)}) collective-permute-start(bf16[1,2,64,1024]{3,2,1,0:T(8,128)(2,1)S(1)} %get-tuple-element.96), channel_id=1, source_target_pairs={{0,4},{1,5},{2,6},{3,7},{4,0},{5,1},{6,2},{7,3},{8,12},{9,13},{10,... | collective-permute-start | bytes 786440 | tf_op jit(solution)/shard_map/ppermute | solution.py:27
  88.9 19.8 %collective-permute-start.7 = (bf16[1,2,64,1024]{3,2,1,0:T(8,128)(2,1)S(1)}, bf16[1,2,64,1024]{3,2,1,0:T(8,128)(2,1)S(1)}, u32[]{:S(2)}, u32[]{:S(2)}) collective-permute-start(bf16[1,2,64,1024]{3,2,1,0:T(8,128)(2,1)S(1)} %get-tuple-element.88), channel_id=1, source_target_pairs={{0,8},{1,9},{2,10},{3,11},{4,12},{5,13},{6,14},{7,15},{8,0},{9,1},... | collective-permute-start | bytes 786440 | tf_op jit(solution)/shard_map/ppermute | solution.py:27
  90.8 15.1 %collective-permute-start.18 = (bf16[1,2,64,1024]{3,2,1,0:T(8,128)(2,1)S(1)}, bf16[1,2,64,1024]{3,2,1,0:T(8,128)(2,1)S(1)}, u32[]{:S(2)}, u32[]{:S(2)}) collective-permute-start(bf16[1,2,64,1024]{3,2,1,0:T(8,128)(2,1)S(1)} %shard_map.148), channel_id=1, source_target_pairs={{0,2},{1,3},{2,0},{3,1},{4,6},{5,7},{6,4},{7,5},{8,10},{9,11},{10,... | collective-permute-start | bytes 786440 | tf_op jit(solution)/shard_map/ppermute | solution.py:27
  92.5 16.2 %collective-permute-start.11 = (bf16[1,2,64,1024]{3,2,1,0:T(8,128)(2,1)S(1)}, bf16[1,2,64,1024]{3,2,1,0:T(8,128)(2,1)S(1)}, u32[]{:S(2)}, u32[]{:S(2)}) collective-permute-start(bf16[1,2,64,1024]{3,2,1,0:T(8,128)(2,1)S(1)} %shard_map.145), channel_id=1, source_target_pairs={{0,2},{1,3},{2,0},{3,1},{4,6},{5,7},{6,4},{7,5},{8,10},{9,11},{10,... | collective-permute-start | bytes 786440 | tf_op jit(solution)/shard_map/ppermute | solution.py:27
  99.5 9.7 %copy-start.7 = (bf16[2,1024,256]{2,1,0:T(8,128)(2,1)S(1)}, bf16[2,1024,256]{2,1,0:T(8,128)(2,1)}, u32[]{:S(2)}) copy-start(bf16[2,1024,256]{2,1,0:T(8,128)(2,1)} %copy-done.6) | copy-start | bytes 3145732
  106.0 19.4 %collective-permute-start.19 = (bf16[2,64,1024]{2,1,0:T(8,128)(2,1)S(1)}, bf16[2,64,1024]{2,1,0:T(8,128)(2,1)S(1)}, u32[]{:S(2)}, u32[]{:S(2)}) collective-permute-start(bf16[2,64,1024]{2,1,0:T(8,128)(2,1)S(1)} %bitcast.44), channel_id=1, source_target_pairs={{0,16},{1,17},{2,18},{3,19},{4,20},{5,21},{6,22},{7,23},{8,24},{9,... | collective-permute-start | bytes 786440 | tf_op jit(solution)/shard_map/ppermute | solution.py:27
  108.8 21.7 %collective-permute-start.12 = (bf16[2,64,1024]{2,1,0:T(8,128)(2,1)S(1)}, bf16[2,64,1024]{2,1,0:T(8,128)(2,1)S(1)}, u32[]{:S(2)}, u32[]{:S(2)}) collective-permute-start(bf16[2,64,1024]{2,1,0:T(8,128)(2,1)S(1)} %bitcast.46), channel_id=1, source_target_pairs={{0,16},{1,17},{2,18},{3,19},{4,20},{5,21},{6,22},{7,23},{8,24},{9,... | collective-permute-start | bytes 786440 | tf_op jit(solution)/shard_map/ppermute | solution.py:27
  121.9 10.2 %collective-permute-start.24 = (bf16[2,160,128]{2,1,0:T(8,128)(2,1)S(1)}, bf16[2,160,128]{2,1,0:T(8,128)(2,1)S(1)}, u32[]{:S(2)}, u32[]{:S(2)}) collective-permute-start(bf16[2,160,128]{2,1,0:T(8,128)(2,1)S(1)} %get-tuple-element.102), channel_id=1, source_target_pairs={{0,1},{1,0},{2,3},{3,2},{4,5},{5,4},{6,7},{7,6},{8,9},{9,8},{10,11... | collective-permute-start | bytes 245768 | tf_op jit(solution)/shard_map/ppermute | solution.py:27
  125.5 17.4 %collective-permute-start.21 = (bf16[2,64,1024]{2,1,0:T(8,128)(2,1)S(1)}, bf16[2,64,1024]{2,1,0:T(8,128)(2,1)S(1)}, u32[]{:S(2)}, u32[]{:S(2)}) collective-permute-start(bf16[2,64,1024]{2,1,0:T(8,128)(2,1)S(1)} %shard_map.150.refs_0_), channel_id=1, source_target_pairs={{0,8},{1,9},{2,10},{3,11},{4,12},{5,13},{6,14},{7,15},{8,0},{9,1},... | collective-permute-start | bytes 786440 | tf_op jit(solution)/shard_map/ppermute | solution.py:27
  130.5 14.6 %collective-permute-start.13 = (bf16[2,64,1024]{2,1,0:T(8,128)(2,1)S(1)}, bf16[2,64,1024]{2,1,0:T(8,128)(2,1)S(1)}, u32[]{:S(2)}, u32[]{:S(2)}) collective-permute-start(bf16[2,64,1024]{2,1,0:T(8,128)(2,1)S(1)} %shard_map.147.refs_0_), channel_id=1, source_target_pairs={{0,4},{1,5},{2,6},{3,7},{4,0},{5,1},{6,2},{7,3},{8,12},{9,13},{10,... | collective-permute-start | bytes 786440 | tf_op jit(solution)/shard_map/ppermute | solution.py:27
  132.1 1.6 collective-permute-start.23
  132.2 4.9 %collective-permute-start.25 = (bf16[2,160,128]{2,1,0:T(8,128)(2,1)S(1)}, bf16[2,160,128]{2,1,0:T(8,128)(2,1)S(1)}, u32[]{:S(2)}, u32[]{:S(2)}) collective-permute-start(bf16[2,160,128]{2,1,0:T(8,128)(2,1)S(1)} %shard_map.154), channel_id=1, source_target_pairs={{0,2},{1,3},{2,0},{3,1},{4,6},{5,7},{6,4},{7,5},{8,10},{9,11},{10,... | collective-permute-start | bytes 245768 | tf_op jit(solution)/shard_map/ppermute | solution.py:27
  137.1 5.4 %collective-permute-start.26 = (bf16[2,160,128]{2,1,0:T(8,128)(2,1)S(1)}, bf16[2,160,128]{2,1,0:T(8,128)(2,1)S(1)}, u32[]{:S(2)}, u32[]{:S(2)}) collective-permute-start(bf16[2,160,128]{2,1,0:T(8,128)(2,1)S(1)} %shard_map.155.mine), channel_id=1, source_target_pairs={{0,4},{1,5},{2,6},{3,7},{4,0},{5,1},{6,2},{7,3},{8,12},{9,13},{10,... | collective-permute-start | bytes 245768 | tf_op jit(solution)/shard_map/ppermute | solution.py:27
  137.7 20.1 %collective-permute-start.20 = (bf16[2,64,1024]{2,1,0:T(8,128)(2,1)S(1)}, bf16[2,64,1024]{2,1,0:T(8,128)(2,1)S(1)}, u32[]{:S(2)}, u32[]{:S(2)}) collective-permute-start(bf16[2,64,1024]{2,1,0:T(8,128)(2,1)S(1)} %shard_map.150.refs_0_), channel_id=1, source_target_pairs={{0,4},{1,5},{2,6},{3,7},{4,0},{5,1},{6,2},{7,3},{8,12},{9,13},{10,... | collective-permute-start | bytes 786440 | tf_op jit(solution)/shard_map/ppermute | solution.py:27
  142.5 6.3 %collective-permute-start.27 = (bf16[2,160,128]{2,1,0:T(8,128)(2,1)S(1)}, bf16[2,160,128]{2,1,0:T(8,128)(2,1)S(1)}, u32[]{:S(2)}, u32[]{:S(2)}) collective-permute-start(bf16[2,160,128]{2,1,0:T(8,128)(2,1)S(1)} %shard_map.156.mine), channel_id=1, source_target_pairs={{0,8},{1,9},{2,10},{3,11},{4,12},{5,13},{6,14},{7,15},{8,0},{9,1},... | collective-permute-start | bytes 245768 | tf_op jit(solution)/shard_map/ppermute | solution.py:27
  142.8 17.9 %collective-permute-start.22 = (bf16[2,64,1024]{2,1,0:T(8,128)(2,1)S(1)}, bf16[2,64,1024]{2,1,0:T(8,128)(2,1)S(1)}, u32[]{:S(2)}, u32[]{:S(2)}) collective-permute-start(bf16[2,64,1024]{2,1,0:T(8,128)(2,1)S(1)} %collective-permute-done.21.refs_2_), channel_id=1, source_target_pairs={{0,4},{1,5},{2,6},{3,7},{4,0},{5,1},{6,2},{7,3},{8,12},{9,13},{10,... | collective-permute-start | bytes 786440 | tf_op jit(solution)/shard_map/ppermute | solution.py:27
  143.3 19.4 %collective-permute-start.14 = (bf16[2,64,1024]{2,1,0:T(8,128)(2,1)S(1)}, bf16[2,64,1024]{2,1,0:T(8,128)(2,1)S(1)}, u32[]{:S(2)}, u32[]{:S(2)}) collective-permute-start(bf16[2,64,1024]{2,1,0:T(8,128)(2,1)S(1)} %shard_map.147.refs_0_), channel_id=1, source_target_pairs={{0,8},{1,9},{2,10},{3,11},{4,12},{5,13},{6,14},{7,15},{8,0},{9,1},... | collective-permute-start | bytes 786440 | tf_op jit(solution)/shard_map/ppermute | solution.py:27
  145.1 17.6 %collective-permute-start.15 = (bf16[2,64,1024]{2,1,0:T(8,128)(2,1)S(1)}, bf16[2,64,1024]{2,1,0:T(8,128)(2,1)S(1)}, u32[]{:S(2)}, u32[]{:S(2)}) collective-permute-start(bf16[2,64,1024]{2,1,0:T(8,128)(2,1)S(1)} %collective-permute-done.13.refs_1_), channel_id=1, source_target_pairs={{0,8},{1,9},{2,10},{3,11},{4,12},{5,13},{6,14},{7,15},{8,0},{9,1},... | collective-permute-start | bytes 786440 | tf_op jit(solution)/shard_map/ppermute | solution.py:27
  148.8 7.4 %collective-permute-start.28 = (bf16[2,160,128]{2,1,0:T(8,128)(2,1)S(1)}, bf16[2,160,128]{2,1,0:T(8,128)(2,1)S(1)}, u32[]{:S(2)}, u32[]{:S(2)}) collective-permute-start(bf16[2,160,128]{2,1,0:T(8,128)(2,1)S(1)} %shard_map.157.mine), channel_id=1, source_target_pairs={{0,16},{1,17},{2,18},{3,19},{4,20},{5,21},{6,22},{7,23},{8,24},{9,... | collective-permute-start | bytes 245768 | tf_op jit(solution)/shard_map/ppermute | solution.py:27
  156.2 4.5 %collective-permute-start.30 = (bf16[2,160,128]{2,1,0:T(8,128)(2,1)S(1)}, bf16[2,160,128]{2,1,0:T(8,128)(2,1)S(1)}, u32[]{:S(2)}, u32[]{:S(2)}) collective-permute-start(bf16[2,160,128]{2,1,0:T(8,128)(2,1)S(1)} %shard_map.158.refs_0_), channel_id=1, source_target_pairs={{0,2},{1,3},{2,0},{3,1},{4,6},{5,7},{6,4},{7,5},{8,10},{9,11},{10,... | collective-permute-start | bytes 245768 | tf_op jit(solution)/shard_map/ppermute | solution.py:27
  157.8 7.0 %collective-permute-start.29 = (bf16[2,160,128]{2,1,0:T(8,128)(2,1)S(1)}, bf16[2,160,128]{2,1,0:T(8,128)(2,1)S(1)}, u32[]{:S(2)}, u32[]{:S(2)}) collective-permute-start(bf16[2,160,128]{2,1,0:T(8,128)(2,1)S(1)} %shard_map.158.refs_0_), channel_id=1, source_target_pairs={{0,1},{1,0},{2,3},{3,2},{4,5},{5,4},{6,7},{7,6},{8,9},{9,8},{10,11... | collective-permute-start | bytes 245768 | tf_op jit(solution)/shard_map/ppermute | solution.py:27
  160.7 4.0 %collective-permute-start.31 = (bf16[2,160,128]{2,1,0:T(8,128)(2,1)S(1)}, bf16[2,160,128]{2,1,0:T(8,128)(2,1)S(1)}, u32[]{:S(2)}, u32[]{:S(2)}) collective-permute-start(bf16[2,160,128]{2,1,0:T(8,128)(2,1)S(1)} %collective-permute-done.30.refs_2_), channel_id=1, source_target_pairs={{0,1},{1,0},{2,3},{3,2},{4,5},{5,4},{6,7},{7,6},{8,9},{9,8},{10,11... | collective-permute-start | bytes 245768 | tf_op jit(solution)/shard_map/ppermute | solution.py:27

commit v5 on v4

--- a/solution.py
+++ b/solution.py
@@ -375,32 +375,44 @@
     )(*args)
 
 
-def assemble_kernel(sc, *refs):
-    parts, out = refs[:4], refs[-1]
+def assemble_kernel(base, sc, *refs):
+    *parts, out = refs
     rest, piece, _ = parts[0].shape
-    for low in range(4):
-        for high in range(rest):
-            at = jnp.bitwise_xor(4 * high + low, sc[1]) * piece
-            out[pl.ds(pl.multiple_of(at, piece), piece), :] = parts[low][high].astype(f32)
-
-
-def assemble(sc, side, parts, carried):
+    if base == 0:
+        for low in range(4):
+            for high in range(rest):
+                at = jnp.bitwise_xor(4 * high + low, sc[1]) * piece
+                out[pl.ds(pl.multiple_of(at, piece), piece), :] = parts[low][high].astype(f32)
+    else:
+        out[...] = parts[0][pl.program_id(0)].astype(f32)
+
+
+def assemble(sc, side, base, parts, carried):
     rest, piece, half = parts[0].shape
-    in_specs = [pl.BlockSpec(memory_space=pltpu.VMEM)] * 4
-    args = list(parts)
+    in_specs = [pl.BlockSpec(memory_space=pltpu.VMEM)] * len(parts)
+    args, aliases = list(parts), {}
     if carried is not None:
+        aliases = {1 + len(args): 0}
         in_specs.append(pl.BlockSpec(memory_space=pl.ANY))
         args.append(carried)
+
+    def body(sc, *refs):
+        assemble_kernel(base, sc, *refs[: len(parts)], refs[-1])
+
+    if base == 0:
+        out = pl.BlockSpec((rest * 4 * piece, half), lambda p, sc: (0, side))
+    else:
+        out = pl.BlockSpec((piece, half), lambda p, sc: (jnp.bitwise_xor(4 * p + base, sc[1]), side))
     return pl.pallas_call(
-        assemble_kernel,
+        body,
         grid_spec=pltpu.PrefetchScalarGridSpec(
             num_scalar_prefetch=1,
-            grid=(1,),
+            grid=(1 if base == 0 else rest,),
             in_specs=in_specs,
-            out_specs=pl.BlockSpec((rest * 4 * piece, half), lambda p, sc: (0, side)),
+            out_specs=out,
         ),
         out_shape=jax.ShapeDtypeStruct((rest * 4 * piece, 2 * half), f32),
-        input_output_aliases={} if carried is None else {5: 0},
+        input_output_aliases=aliases,
         compiler_params=pltpu.CompilerParams(vmem_limit_bytes=VMEM),
     )(sc, *args)
 
@@ -526,7 +538,10 @@
         pieces.append([x, *middle, three])
     grad_w_out = None
     for side in (1, 0):
-        grad_w_out = assemble(sc, side, pieces[side], grad_w_out)
+        x, one, two, three = pieces[side]
+        grad_w_out = assemble(sc, side, 0, [x, one, two, x], grad_w_out)
+    for side in (1, 0):
+        grad_w_out = assemble(sc, side, 3, [pieces[side][3]], grad_w_out)
     sums = reduce_small(packed)
     grads = unpack(sc, sums, groups)
     return (grad_u.reshape(shape), grad_v.reshape(shape), grad_w_out, *grads)

time: 168 us -> 171 us (1.018)
  Pallas kernels: 61.7 us -> 64.5 us
    pallas_call x2 -> x4, Pallas kernels: 4 us -> 6.75 us  [assemble(): pl.pallas_call(body, grid_spec=pltpu.PrefetchScalarGridSpec(num_scalar_pr...]
  transfers between devices with their start and end apart: 32 -> 32, of which waited for: 12 -> 12; matrix products, arithmetic and copies ran while one was open for 0% -> 0% of each run, Pallas kernels for 36% -> 37%
where the time goes in v5:
time: 171 us; the launch traced here: 169 us
  waiting for transfers between devices  68 us (40%)
  Pallas kernels  64.5 us (38%)
  starting transfers between devices  32.5 us (19%)
  local copies, waits for them, and re-layouts  3.03 us (2%)
    ppermute x32, waiting for transfers between devices, swap(): return lax.ppermute(value, AXES, pairs)  68 us
    ppermute x32, starting transfers between devices, swap(): return lax.ppermute(value, AXES, pairs)  32.5 us
    pallas_call x4, Pallas kernels, forward(): pl.pallas_call(functools.partial(forward_kernel, (span, chans, per, piece...  29.3 us
    pallas_call x4, Pallas kernels, backward(): pl.pallas_call(functools.partial(backward_kernel, (span, chans, per, inde...  25.6 us
    pallas_call x4, Pallas kernels, assemble(): pl.pallas_call(body, grid_spec=pltpu.PrefetchScalarGridSpec(num_scalar_pr...  6.75 us
  transfers between devices with their start and end apart: 32, of which 12 were waited for; matrix products, arithmetic and copies ran while one was open for 0% of the time, Pallas kernels for 37%

profile of v5, /device:TPU:0, one launch (start us, length us, event | category | flops | bytes accessed | tf_op | source)
XLA Modules:
  0.0 168.9 jit_solution(5508530012879404381)
XLA Ops:
  0.6 3.0 %collective-permute-start = (bf16[512,2048]{1,0:T(8,128)(2,1)}, bf16[512,2048]{1,0:T(8,128)(2,1)S(1)}, u32[]{:S(2)}, u32[]{:S(2)}) collective-permute-start(bf16[512,2048]{1,0:T(8,128)(2,1)} %param.15), channel_id=1, source_target_pairs={{0,2},{1,3},{2,0},{3,1},{4,6},{5,7},{6,4},{7,5},{8,10},{9,11},{10,... | collective-permute-start | bytes 6291464 | tf_op jit(solution)/shard_map/ppermute | solution.py:27
  3.7 2.2 %copy-done = bf16[1,1024,2048]{2,1,0:T(8,128)(2,1)S(1)} copy-done((bf16[1,1024,2048]{2,1,0:T(8,128)(2,1)S(1)}, bf16[1,1024,2048]{2,1,0:T(8,128)(2,1)}, u32[]{:S(2)}) %copy-start) | copy-done | bytes 4194328
  6.0 8.3 %shard_map.135 = (bf16[2,256,2048]{2,1,0:T(8,128)(2,1)S(1)}, bf16[2,1024,256]{2,1,0:T(8,128)(2,1)S(1)}, bf16[2,1024,256]{2,1,0:T(8,128)(2,1)S(1)}, bf16[2,1024,2...) custom-call(s32[2]{0:T(128)S(1)} %pad_add_fusion.sc, bf16[1024,2048]{1,0:T(8,128)(2,1)} %bitcast.32, ...), custom_call_target="tpu_custom_call" | custom-call | flops 2147483648 | tf_op jit(solution)/shard_map/pallas_call | solution.py:147
  14.5 6.7 %shard_map.137 = (bf16[2,256,2048]{2,1,0:T(8,128)(2,1)S(1)}, bf16[2,1024,256]{2,1,0:T(8,128)(2,1)S(1)}, bf16[2,1024,256]{2,1,0:T(8,128)(2,1)S(1)}, bf16[2,1024,2...) custom-call(s32[2]{0:T(128)S(1)} %pad_add_fusion.sc, bf16[1024,2048]{1,0:T(8,128)(2,1)S(1)} %bitcast.33, ...), custom_call_target="tpu_custom_call" | custom-call | flops 2147483648 | tf_op jit(solution)/shard_map/pallas_call | solution.py:147
  21.2 0.5 collective-permute-start.3
  21.8 27.7 %collective-permute-done = bf16[512,2048]{1,0:T(8,128)(2,1)S(1)} collective-permute-done((bf16[512,2048]{1,0:T(8,128)(2,1)}, bf16[512,2048]{1,0:T(8,128)(2,1)S(1)}, u32[]{:S(2)}, u32[]{:S(2)}) %collective-permute-start) | collective-permute-done | bytes 2097184 | tf_op jit(solution)/shard_map/ppermute | solution.py:27
  49.5 6.9 %shard_map.136 = (bf16[2,128,1024]{2,1,0:T(8,128)(2,1)S(1)}, bf16[2,128,1024]{2,1,0:T(8,128)(2,1)S(1)}, bf16[2,128,1024]{2,1,0:T(8,128)(2,1)S(1)}, bf16[2,128,10...) custom-call(s32[2]{0:T(128)S(1)} %pad_add_fusion.sc, ...), custom_call_target="tpu_custom_call" | custom-call | flops 2147483648 | tf_op jit(solution)/shard_map/pallas_call | solution.py:147
  56.5 0.8 copy-done.10
  57.2 1.8 %collective-permute-start.8 = (bf16[2,128,1024]{2,1,0:T(8,128)(2,1)S(1)}, bf16[2,128,1024]{2,1,0:T(8,128)(2,1)S(1)}, u32[]{:S(2)}, u32[]{:S(2)}) collective-permute-start(bf16[2,128,1024]{2,1,0:T(8,128)(2,1)S(1)} %get-tuple-element.90), channel_id=1, source_target_pairs={{0,4},{1,5},{2,6},{3,7},{4,0},{5,1},{6,2},{7,3},{8,12},{9,13},{10,... | collective-permute-start | bytes 1572872 | tf_op jit(solution)/shard_map/ppermute | solution.py:27
  59.0 1.6 collective-permute-start.9
  60.6 7.3 %shard_map.138 = (bf16[2,128,1024]{2,1,0:T(8,128)(2,1)}, bf16[2,128,1024]{2,1,0:T(8,128)(2,1)S(1)}, bf16[2,128,1024]{2,1,0:T(8,128)(2,1)S(1)}, bf16[2,128,1024]{...) custom-call(s32[2]{0:T(128)S(1)} %pad_add_fusion.sc, ...), custom_call_target="tpu_custom_call" | custom-call | flops 2147483648 | tf_op jit(solution)/shard_map/pallas_call | solution.py:147
  67.9 0.5 collective-permute-start.5
  68.4 3.6 %collective-permute-done.8 = bf16[2,128,1024]{2,1,0:T(8,128)(2,1)S(1)} collective-permute-done((bf16[2,128,1024]{2,1,0:T(8,128)(2,1)S(1)}, bf16[2,128,1024]{2,1,0:T(8,128)(2,1)S(1)}, u32[]{:S(2)}, u32[]{:S(2)}) %collective-permute-start.8) | collective-permute-done | bytes 524320 | tf_op jit(solution)/shard_map/ppermute | solution.py:27
  72.0 1.8 %collective-permute-start.6 = (bf16[2,128,1024]{2,1,0:T(8,128)(2,1)S(1)}, bf16[2,128,1024]{2,1,0:T(8,128)(2,1)S(1)}, u32[]{:S(2)}, u32[]{:S(2)}) collective-permute-start(bf16[2,128,1024]{2,1,0:T(8,128)(2,1)S(1)} %get-tuple-element.86), channel_id=1, source_target_pairs={{0,8},{1,9},{2,10},{3,11},{4,12},{5,13},{6,14},{7,15},{8,0},{9,1},... | collective-permute-start | bytes 1572872 | tf_op jit(solution)/shard_map/ppermute | solution.py:27
  74.1 1.6 collective-permute-start.16
  75.7 7.6 %collective-permute-done.5 = bf16[2,128,1024]{2,1,0:T(8,128)(2,1)S(1)} collective-permute-done((bf16[2,128,1024]{2,1,0:T(8,128)(2,1)}, bf16[2,128,1024]{2,1,0:T(8,128)(2,1)S(1)}, u32[]{:S(2)}, u32[]{:S(2)}) %collective-permute-start.5) | collective-permute-done | bytes 524320 | tf_op jit(solution)/shard_map/ppermute | solution.py:27
  83.3 1.8 %collective-permute-start.10 = (bf16[1,2,64,1024]{3,2,1,0:T(8,128)(2,1)S(1)}, bf16[1,2,64,1024]{3,2,1,0:T(8,128)(2,1)S(1)}, u32[]{:S(2)}, u32[]{:S(2)}) collective-permute-start(bf16[1,2,64,1024]{3,2,1,0:T(8,128)(2,1)S(1)} %get-tuple-element.94), channel_id=1, source_target_pairs={{0,8},{1,9},{2,10},{3,11},{4,12},{5,13},{6,14},{7,15},{8,0},{9,1},... | collective-permute-start | bytes 786440 | tf_op jit(solution)/shard_map/ppermute | solution.py:27
  85.4 1.7 %collective-permute-start.15 = (bf16[1,2,64,1024]{3,2,1,0:T(8,128)(2,1)S(1)}, bf16[1,2,64,1024]{3,2,1,0:T(8,128)(2,1)S(1)}, u32[]{:S(2)}, u32[]{:S(2)}) collective-permute-start(bf16[1,2,64,1024]{3,2,1,0:T(8,128)(2,1)S(1)} %get-tuple-element.96), channel_id=1, source_target_pairs={{0,4},{1,5},{2,6},{3,7},{4,0},{5,1},{6,2},{7,3},{8,12},{9,13},{10,... | collective-permute-start | bytes 786440 | tf_op jit(solution)/shard_map/ppermute | solution.py:27
  87.2 1.7 %collective-permute-done.16.r = bf16[1,2,64,1024]{3,2,1,0:T(8,128)(2,1)S(1)} collective-permute-done((bf16[1,2,64,1024]{3,2,1,0:T(8,128)(2,1)S(1)}, bf16[1,2,64,1024]{3,2,1,0:T(8,128)(2,1)S(1)}, u32[]{:S(2)}, u32[]{:S(2)}) %collective-permute-start.16) | collective-permute-done | bytes 262176 | tf_op jit(solution)/shard_map/ppermute | solution.py:27
  88.9 1.8 %collective-permute-start.7 = (bf16[1,2,64,1024]{3,2,1,0:T(8,128)(2,1)S(1)}, bf16[1,2,64,1024]{3,2,1,0:T(8,128)(2,1)S(1)}, u32[]{:S(2)}, u32[]{:S(2)}) collective-permute-start(bf16[1,2,64,1024]{3,2,1,0:T(8,128)(2,1)S(1)} %get-tuple-element.88), channel_id=1, source_target_pairs={{0,8},{1,9},{2,10},{3,11},{4,12},{5,13},{6,14},{7,15},{8,0},{9,1},... | collective-permute-start | bytes 786440 | tf_op jit(solution)/shard_map/ppermute | solution.py:27
  90.8 1.6 collective-permute-start.17
  92.5 0.5 collective-permute-start.11
  93.0 6.4 %shard_map.139 = (bf16[1024,2048]{1,0:T(8,128)(2,1)}, bf16[1024,2048]{1,0:T(8,128)(2,1)}, bf16[2,160,128]{2,1,0:T(8,128)(2,1)S(1)}) custom-call(s32[2]{0:T(128)S(1)} %pad_add_fusion.sc, bf16[1024,2048]{1,0:T(8,128)(2,1)S(1)} %bitcast.28, bf16[2,256,2048]{2,1,0:T(8,128)(2,1)S(1)} %bitcast.43, bf16[2,1024,256]{2,1,0:T(8,128)(2,1)S(1)} %get-tuple-element.71.upper, ...), custom_call_target="tpu_custom_call" | custom-call | flops 2147483648 | tf_op jit(solution)/shard_map/pallas_call | solution.py:271
  99.5 6.4 %shard_map.140 = (bf16[1024,2048]{1,0:T(8,128)(2,1)}, bf16[1024,2048]{1,0:T(8,128)(2,1)}, bf16[2,160,128]{2,1,0:T(8,128)(2,1)S(1)}) custom-call(s32[2]{0:T(128)S(1)} %pad_add_fusion.sc, bf16[1024,2048]{1,0:T(8,128)(2,1)S(1)} %bitcast.29, bf16[2,256,2048]{2,1,0:T(8,128)(2,1)S(1)} %bitcast.40, ...), custom_call_target="tpu_custom_call", output_to_operand_aliasing={{0}: (10, {}), {1}: (11, {})} | custom-call | flops 2147483648 | tf_op jit(solution)/shard_map/pallas_call | solution.py:271
  106.0 2.7 %collective-permute-start.18 = (bf16[2,64,1024]{2,1,0:T(8,128)(2,1)S(1)}, bf16[2,64,1024]{2,1,0:T(8,128)(2,1)S(1)}, u32[]{:S(2)}, u32[]{:S(2)}) collective-permute-start(bf16[2,64,1024]{2,1,0:T(8,128)(2,1)S(1)} %bitcast.44), channel_id=1, source_target_pairs={{0,16},{1,17},{2,18},{3,19},{4,20},{5,21},{6,22},{7,23},{8,24},{9,... | collective-permute-start | bytes 786440 | tf_op jit(solution)/shard_map/ppermute | solution.py:27
  108.8 0.3 collective-permute-start.12
  109.2 6.3 %shard_map.141 = (bf16[1024,2048]{1,0:T(8,128)(2,1)}, bf16[1024,2048]{1,0:T(8,128)(2,1)}, bf16[2,160,128]{2,1,0:T(8,128)(2,1)S(1)}) custom-call(s32[2]{0:T(128)S(1)} %pad_add_fusion.sc, bf16[1024,2048]{1,0:T(8,128)(2,1)S(1)} %bitcast.30, bf16[2,256,2048]{2,1,0:T(8,128)(2,1)S(1)} %bitcast.41, ...), custom_call_target="tpu_custom_call", output_to_operand_aliasing={{0}: (10, {}), {1}: (11, {})} | custom-call | flops 2147483648 | tf_op jit(solution)/shard_map/pallas_call | solution.py:271
  115.5 6.4 %shard_map.142 = (bf16[1024,2048]{1,0:T(8,128)(2,1)}, bf16[1024,2048]{1,0:T(8,128)(2,1)}, bf16[2,160,128]{2,1,0:T(8,128)(2,1)S(1)}) custom-call(s32[2]{0:T(128)S(1)} %pad_add_fusion.sc, bf16[1024,2048]{1,0:T(8,128)(2,1)S(1)} %bitcast.31, bf16[2,256,2048]{2,1,0:T(8,128)(2,1)S(1)} %bitcast.42, ...), custom_call_target="tpu_custom_call", output_to_operand_aliasing={{0}: (10, {}), {1}: (11, {})} | custom-call | flops 2147483648 | tf_op jit(solution)/shard_map/pallas_call | solution.py:271
  122.0 3.4 %collective-permute-done.18.got = bf16[2,64,1024]{2,1,0:T(8,128)(2,1)S(1)} collective-permute-done((bf16[2,64,1024]{2,1,0:T(8,128)(2,1)S(1)}, bf16[2,64,1024]{2,1,0:T(8,128)(2,1)S(1)}, u32[]{:S(2)}, u32[]{:S(2)}) %collective-permute-start.18) | collective-permute-done | bytes 262176 | tf_op jit(solution)/shard_map/ppermute | solution.py:27
  125.7 4.8 %collective-permute-done.12.got = bf16[2,64,1024]{2,1,0:T(8,128)(2,1)S(1)} collective-permute-done((bf16[2,64,1024]{2,1,0:T(8,128)(2,1)S(1)}, bf16[2,64,1024]{2,1,0:T(8,128)(2,1)S(1)}, u32[]{:S(2)}, u32[]{:S(2)}) %collective-permute-start.12) | collective-permute-done | bytes 262176 | tf_op jit(solution)/shard_map/ppermute | solution.py:27
  130.5 1.6 collective-permute-start.13
  132.2 1.5 collective-permute-start.25
  133.7 3.3 %collective-permute-done.25.got = bf16[2,160,128]{2,1,0:T(8,128)(2,1)S(1)} collective-permute-done((bf16[2,160,128]{2,1,0:T(8,128)(2,1)S(1)}, bf16[2,160,128]{2,1,0:T(8,128)(2,1)S(1)}, u32[]{:S(2)}, u32[]{:S(2)}) %collective-permute-start.25) | collective-permute-done | bytes 81952 | tf_op jit(solution)/shard_map/ppermute | solution.py:27
  137.1 0.6 collective-permute-start.26
  137.7 1.5 collective-permute-start.22
  139.2 3.3 %collective-permute-done.26.got = bf16[2,160,128]{2,1,0:T(8,128)(2,1)S(1)} collective-permute-done((bf16[2,160,128]{2,1,0:T(8,128)(2,1)S(1)}, bf16[2,160,128]{2,1,0:T(8,128)(2,1)S(1)}, u32[]{:S(2)}, u32[]{:S(2)}) %collective-permute-start.26) | collective-permute-done | bytes 81952 | tf_op jit(solution)/shard_map/ppermute | solution.py:27
  142.8 1.8 %collective-permute-start.21 = (bf16[2,64,1024]{2,1,0:T(8,128)(2,1)S(1)}, bf16[2,64,1024]{2,1,0:T(8,128)(2,1)S(1)}, u32[]{:S(2)}, u32[]{:S(2)}) collective-permute-start(bf16[2,64,1024]{2,1,0:T(8,128)(2,1)S(1)} %shard_map.147.refs_0_.refs_3_), channel_id=1, source_target_pairs={{0,8},{1,9},{2,10},{3,11},{4,12},{5,13},{6,14},{7,15},{8,0},{9,1},... | collective-permute-start | bytes 786440 | tf_op jit(solution)/shard_map/ppermute | solution.py:27
  144.6 0.5 collective-permute-start.20
  145.4 3.4 %collective-permute-done.27.got = bf16[2,160,128]{2,1,0:T(8,128)(2,1)S(1)} collective-permute-done((bf16[2,160,128]{2,1,0:T(8,128)(2,1)S(1)}, bf16[2,160,128]{2,1,0:T(8,128)(2,1)S(1)}, u32[]{:S(2)}, u32[]{:S(2)}) %collective-permute-start.27) | collective-permute-done | bytes 81952 | tf_op jit(solution)/shard_map/ppermute | solution.py:27
  148.8 1.1 collective-permute-start.28
  149.9 6.0 %collective-permute-done.28.got = bf16[2,160,128]{2,1,0:T(8,128)(2,1)S(1)} collective-permute-done((bf16[2,160,128]{2,1,0:T(8,128)(2,1)S(1)}, bf16[2,160,128]{2,1,0:T(8,128)(2,1)S(1)}, u32[]{:S(2)}, u32[]{:S(2)}) %collective-permute-start.28) | collective-permute-done | bytes 81952 | tf_op jit(solution)/shard_map/ppermute | solution.py:27
  156.0 1.5 collective-permute-start.30
  157.5 3.0 %collective-permute-done.30.refs_2_ = bf16[2,160,128]{2,1,0:T(8,128)(2,1)S(1)} collective-permute-done((bf16[2,160,128]{2,1,0:T(8,128)(2,1)S(1)}, bf16[2,160,128]{2,1,0:T(8,128)(2,1)S(1)}, u32[]{:S(2)}, u32[]{:S(2)}) %collective-permute-start.30) | collective-permute-done | bytes 81952 | tf_op jit(solution)/shard_map/ppermute | solution.py:27
  160.5 2.0 %shard_map.151.refs_4_ = f32[512,2048]{1,0:T(8,128)} custom-call(s32[2]{0:T(128)S(1)} %pad_add_fusion.sc, bf16[2,64,1024]{2,1,0:T(8,128)(2,1)S(1)} %shard_map.150.refs_0_.refs_3_, bf16[2,64,1024]{2,1,0:T(8,128)(2,1)S(1)} %collective-permute-done.22.refs_1_, bf16[2,64,1024]{2,1,0:T(8,128)(2,1)S(1)} %collective-permute-done.19.refs_2_, ...), custom_call_target="tpu_custom_call" | custom-call | tf_op jit(solution)/shard_map/pallas_call | solution.py:406
  162.5 2.0 %shard_map.152.refs_1_ = f32[512,2048]{1,0:T(8,128)} custom-call(s32[2]{0:T(128)S(1)} %pad_add_fusion.sc, bf16[2,64,1024]{2,1,0:T(8,128)(2,1)S(1)} %shard_map.147.refs_0_.refs_3_, bf16[2,64,1024]{2,1,0:T(8,128)(2,1)S(1)} %collective-permute-done.13.refs_1_, bf16[2,64,1024]{2,1,0:T(8,128)(2,1)S(1)} %collective-permute-done.21.refs_2_, ...), custom_call_target="tpu_custom_call", output_to_operand_aliasing={{}: (5, {})} | custom-call | tf_op jit(solution)/shard_map/pallas_call | solution.py:406
  164.5 1.4 shard_map.153.refs_1_
  165.9 1.4 shard_map.154
  167.2 1.7 %unpack.1 = (f32[16,128,128]{2,1,0:T(8,128)}, f32[16,128]{1,0:T(8,128)}, f32[16,128]{1,0:T(8,128)}, f32[16,128]{1,0:T(8,128)}) custom-call(s32[2]{0:T(128)S(1)} %pad_add_fusion.sc, bf16[2,160,128]{2,1,0:T(8,128)(2,1)S(1)} %shard_map.160.refs_0_, bf16[2,160,128]{2,1,0:T(8,128)(2,1)S(1)} %collective-permute-done.29.refs_1_, ...), custom_call_target="tpu_custom_call" | custom-call | tf_op jit(solution)/shard_map/unpack/pallas_call | solution.py:353
  (70 shorter events, 2.2 us)
Async XLA Ops:
  0.6 48.9 %collective-permute-start = (bf16[512,2048]{1,0:T(8,128)(2,1)}, bf16[512,2048]{1,0:T(8,128)(2,1)S(1)}, u32[]{:S(2)}, u32[]{:S(2)}) collective-permute-start(bf16[512,2048]{1,0:T(8,128)(2,1)} %param.15), channel_id=1, source_target_pairs={{0,2},{1,3},{2,0},{3,1},{4,6},{5,7},{6,4},{7,5},{8,10},{9,11},{10,... | collective-permute-start | bytes 6291464 | tf_op jit(solution)/shard_map/ppermute | solution.py:27
  3.7 2.2 %copy-start = (bf16[1,1024,2048]{2,1,0:T(8,128)(2,1)S(1)}, bf16[1,1024,2048]{2,1,0:T(8,128)(2,1)}, u32[]{:S(2)}) copy-start(bf16[1,1024,2048]{2,1,0:T(8,128)(2,1)} %param.10) | copy-start | bytes 12582916
  5.9 8.5 %copy-start.1 = (bf16[1,1024,2048]{2,1,0:T(8,128)(2,1)S(1)}, bf16[1,1024,2048]{2,1,0:T(8,128)(2,1)}, u32[]{:S(2)}) copy-start(bf16[1,1024,2048]{2,1,0:T(8,128)(2,1)} %param.10) | copy-start | bytes 12582916
  5.9 8.5 %copy-start.2 = (bf16[1,1024,2048]{2,1,0:T(8,128)(2,1)S(1)}, bf16[1,1024,2048]{2,1,0:T(8,128)(2,1)}, u32[]{:S(2)}) copy-start(bf16[1,1024,2048]{2,1,0:T(8,128)(2,1)} %param.8) | copy-start | bytes 12582916
  5.9 8.5 %copy-start.3 = (bf16[1,1024,2048]{2,1,0:T(8,128)(2,1)S(1)}, bf16[1,1024,2048]{2,1,0:T(8,128)(2,1)}, u32[]{:S(2)}) copy-start(bf16[1,1024,2048]{2,1,0:T(8,128)(2,1)} %param.9) | copy-start | bytes 12582916
  5.9 8.5 %copy-start.4 = (bf16[16,128,128]{2,1,0:T(8,128)(2,1)S(1)}, bf16[16,128,128]{2,1,0:T(8,128)(2,1)}, u32[]{:S(2)}) copy-start(bf16[16,128,128]{2,1,0:T(8,128)(2,1)} %w_mix.15) | copy-start | bytes 1572868
  5.9 8.5 %copy-start.8 = (f32[16,128]{1,0:T(8,128)S(1)}, f32[16,128]{1,0:T(8,128)}, u32[]{:S(2)}) copy-start(f32[16,128]{1,0:T(8,128)} %param.13) | copy-start | bytes 24580
  6.0 8.5 %copy-start.9 = (f32[16,128]{1,0:T(8,128)S(1)}, f32[16,128]{1,0:T(8,128)}, u32[]{:S(2)}) copy-start(f32[16,128]{1,0:T(8,128)} %param.14) | copy-start | bytes 24580
  6.0 8.5 %copy-start.12 = (f32[16,128]{1,0:T(8,128)S(1)}, f32[16,128]{1,0:T(8,128)}, u32[]{:S(2)}) copy-start(f32[16,128]{1,0:T(8,128)} %param.12) | copy-start | bytes 24580
  14.3 7.4 %copy-start.5 = (bf16[512,2048]{1,0:T(8,128)(2,1)S(1)}, bf16[512,2048]{1,0:T(8,128)(2,1)}, u32[]{:S(2)}) copy-start(bf16[512,2048]{1,0:T(8,128)(2,1)} %param.15) | copy-start | bytes 6291460
  14.3 35.2 %collective-permute-start.2 = (bf16[2,256,2048]{2,1,0:T(8,128)(2,1)S(1)}, bf16[2,256,2048]{2,1,0:T(8,128)(2,1)S(1)}, u32[]{:S(2)}, u32[]{:S(2)}) collective-permute-start(bf16[2,256,2048]{2,1,0:T(8,128)(2,1)S(1)} %get-tuple-element.61), channel_id=1, source_target_pairs={{0,1},{1,0},{2,3},{3,2},{4,5},{5,4},{6,7},{7,6},{8,9},{9,8},{10,11... | collective-permute-start | bytes 6291464 | tf_op jit(solution)/shard_map/ppermute | solution.py:27
  21.2 39.4 %collective-permute-start.3 = (bf16[2,256,2048]{2,1,0:T(8,128)(2,1)S(1)}, bf16[2,256,2048]{2,1,0:T(8,128)(2,1)S(1)}, u32[]{:S(2)}, u32[]{:S(2)}) collective-permute-start(bf16[2,256,2048]{2,1,0:T(8,128)(2,1)S(1)} %get-tuple-element.66), channel_id=1, source_target_pairs={{0,1},{1,0},{2,3},{3,2},{4,5},{5,4},{6,7},{7,6},{8,9},{9,8},{10,11... | collective-permute-start | bytes 6291464 | tf_op jit(solution)/shard_map/ppermute | solution.py:27
  21.7 70.7 %collective-permute-start.4 = (bf16[512,2048]{1,0:T(8,128)(2,1)S(1)}, bf16[512,2048]{1,0:T(8,128)(2,1)S(1)}, u32[]{:S(2)}, u32[]{:S(2)}) collective-permute-start(bf16[512,2048]{1,0:T(8,128)(2,1)S(1)} %copy-done.5), channel_id=1, source_target_pairs={{0,1},{1,0},{2,3},{3,2},{4,5},{5,4},{6,7},{7,6},{8,9},{9,8},{10,11... | collective-permute-start | bytes 6291464 | tf_op jit(solution)/shard_map/ppermute | solution.py:27
  49.5 66.0 %collective-permute-start.1 = (bf16[512,2048]{1,0:T(8,128)(2,1)S(1)}, bf16[512,2048]{1,0:T(8,128)(2,1)S(1)}, u32[]{:S(2)}, u32[]{:S(2)}) collective-permute-start(bf16[512,2048]{1,0:T(8,128)(2,1)S(1)} %collective-permute-done), channel_id=1, source_target_pairs={{0,1},{1,0},{2,3},{3,2},{4,5},{5,4},{6,7},{7,6},{8,9},{9,8},{10,11... | collective-permute-start | bytes 6291464 | tf_op jit(solution)/shard_map/ppermute | solution.py:27
  56.4 0.8 copy-start.10
  57.2 10.7 %copy-start.6 = (bf16[2,1024,256]{2,1,0:T(8,128)(2,1)}, bf16[2,1024,256]{2,1,0:T(8,128)(2,1)S(1)}, u32[]{:S(2)}) copy-start(bf16[2,1024,256]{2,1,0:T(8,128)(2,1)S(1)} %get-tuple-element.65.w1) | copy-start | bytes 3145732
  57.2 14.8 %collective-permute-start.8 = (bf16[2,128,1024]{2,1,0:T(8,128)(2,1)S(1)}, bf16[2,128,1024]{2,1,0:T(8,128)(2,1)S(1)}, u32[]{:S(2)}, u32[]{:S(2)}) collective-permute-start(bf16[2,128,1024]{2,1,0:T(8,128)(2,1)S(1)} %get-tuple-element.90), channel_id=1, source_target_pairs={{0,4},{1,5},{2,6},{3,7},{4,0},{5,1},{6,2},{7,3},{8,12},{9,13},{10,... | collective-permute-start | bytes 1572872 | tf_op jit(solution)/shard_map/ppermute | solution.py:27
  59.0 14.9 %copy-start.11 = (bf16[2,128,1024]{2,1,0:T(8,128)(2,1)S(1)}, bf16[2,128,1024]{2,1,0:T(8,128)(2,1)}, u32[]{:S(2)}) copy-start(bf16[2,128,1024]{2,1,0:T(8,128)(2,1)} %copy-done.10) | copy-start | bytes 1572868
  59.0 14.9 %collective-permute-start.9 = (bf16[2,128,1024]{2,1,0:T(8,128)(2,1)S(1)}, bf16[2,128,1024]{2,1,0:T(8,128)(2,1)S(1)}, u32[]{:S(2)}, u32[]{:S(2)}) collective-permute-start(bf16[2,128,1024]{2,1,0:T(8,128)(2,1)S(1)} %get-tuple-element.92), channel_id=1, source_target_pairs={{0,8},{1,9},{2,10},{3,11},{4,12},{5,13},{6,14},{7,15},{8,0},{9,1},... | collective-permute-start | bytes 1572872 | tf_op jit(solution)/shard_map/ppermute | solution.py:27
  67.9 15.4 %collective-permute-start.5 = (bf16[2,128,1024]{2,1,0:T(8,128)(2,1)}, bf16[2,128,1024]{2,1,0:T(8,128)(2,1)S(1)}, u32[]{:S(2)}, u32[]{:S(2)}) collective-permute-start(bf16[2,128,1024]{2,1,0:T(8,128)(2,1)} %get-tuple-element.84), channel_id=1, source_target_pairs={{0,4},{1,5},{2,6},{3,7},{4,0},{5,1},{6,2},{7,3},{8,12},{9,13},{10,... | collective-permute-start | bytes 1572872 | tf_op jit(solution)/shard_map/ppermute | solution.py:27
  72.0 13.1 %collective-permute-start.6 = (bf16[2,128,1024]{2,1,0:T(8,128)(2,1)S(1)}, bf16[2,128,1024]{2,1,0:T(8,128)(2,1)S(1)}, u32[]{:S(2)}, u32[]{:S(2)}) collective-permute-start(bf16[2,128,1024]{2,1,0:T(8,128)(2,1)S(1)} %get-tuple-element.86), channel_id=1, source_target_pairs={{0,8},{1,9},{2,10},{3,11},{4,12},{5,13},{6,14},{7,15},{8,0},{9,1},... | collective-permute-start | bytes 1572872 | tf_op jit(solution)/shard_map/ppermute | solution.py:27
  74.1 14.8 %collective-permute-start.16 = (bf16[1,2,64,1024]{3,2,1,0:T(8,128)(2,1)S(1)}, bf16[1,2,64,1024]{3,2,1,0:T(8,128)(2,1)S(1)}, u32[]{:S(2)}, u32[]{:S(2)}) collective-permute-start(bf16[1,2,64,1024]{3,2,1,0:T(8,128)(2,1)S(1)} %get-tuple-element.98), channel_id=1, source_target_pairs={{0,4},{1,5},{2,6},{3,7},{4,0},{5,1},{6,2},{7,3},{8,12},{9,13},{10,... | collective-permute-start | bytes 786440 | tf_op jit(solution)/shard_map/ppermute | solution.py:27
  83.3 7.5 %collective-permute-start.10 = (bf16[1,2,64,1024]{3,2,1,0:T(8,128)(2,1)S(1)}, bf16[1,2,64,1024]{3,2,1,0:T(8,128)(2,1)S(1)}, u32[]{:S(2)}, u32[]{:S(2)}) collective-permute-start(bf16[1,2,64,1024]{3,2,1,0:T(8,128)(2,1)S(1)} %get-tuple-element.94), channel_id=1, source_target_pairs={{0,8},{1,9},{2,10},{3,11},{4,12},{5,13},{6,14},{7,15},{8,0},{9,1},... | collective-permute-start | bytes 786440 | tf_op jit(solution)/shard_map/ppermute | solution.py:27
  85.4 20.5 %collective-permute-start.15 = (bf16[1,2,64,1024]{3,2,1,0:T(8,128)(2,1)S(1)}, bf16[1,2,64,1024]{3,2,1,0:T(8,128)(2,1)S(1)}, u32[]{:S(2)}, u32[]{:S(2)}) collective-permute-start(bf16[1,2,64,1024]{3,2,1,0:T(8,128)(2,1)S(1)} %get-tuple-element.96), channel_id=1, source_target_pairs={{0,4},{1,5},{2,6},{3,7},{4,0},{5,1},{6,2},{7,3},{8,12},{9,13},{10,... | collective-permute-start | bytes 786440 | tf_op jit(solution)/shard_map/ppermute | solution.py:27
  88.9 19.8 %collective-permute-start.7 = (bf16[1,2,64,1024]{3,2,1,0:T(8,128)(2,1)S(1)}, bf16[1,2,64,1024]{3,2,1,0:T(8,128)(2,1)S(1)}, u32[]{:S(2)}, u32[]{:S(2)}) collective-permute-start(bf16[1,2,64,1024]{3,2,1,0:T(8,128)(2,1)S(1)} %get-tuple-element.88), channel_id=1, source_target_pairs={{0,8},{1,9},{2,10},{3,11},{4,12},{5,13},{6,14},{7,15},{8,0},{9,1},... | collective-permute-start | bytes 786440 | tf_op jit(solution)/shard_map/ppermute | solution.py:27
  90.8 15.1 %collective-permute-start.17 = (bf16[1,2,64,1024]{3,2,1,0:T(8,128)(2,1)S(1)}, bf16[1,2,64,1024]{3,2,1,0:T(8,128)(2,1)S(1)}, u32[]{:S(2)}, u32[]{:S(2)}) collective-permute-start(bf16[1,2,64,1024]{3,2,1,0:T(8,128)(2,1)S(1)} %shard_map.148), channel_id=1, source_target_pairs={{0,2},{1,3},{2,0},{3,1},{4,6},{5,7},{6,4},{7,5},{8,10},{9,11},{10,... | collective-permute-start | bytes 786440 | tf_op jit(solution)/shard_map/ppermute | solution.py:27
  92.5 16.2 %collective-permute-start.11 = (bf16[1,2,64,1024]{3,2,1,0:T(8,128)(2,1)S(1)}, bf16[1,2,64,1024]{3,2,1,0:T(8,128)(2,1)S(1)}, u32[]{:S(2)}, u32[]{:S(2)}) collective-permute-start(bf16[1,2,64,1024]{3,2,1,0:T(8,128)(2,1)S(1)} %shard_map.145), channel_id=1, source_target_pairs={{0,2},{1,3},{2,0},{3,1},{4,6},{5,7},{6,4},{7,5},{8,10},{9,11},{10,... | collective-permute-start | bytes 786440 | tf_op jit(solution)/shard_map/ppermute | solution.py:27
  99.5 9.7 %copy-start.7 = (bf16[2,1024,256]{2,1,0:T(8,128)(2,1)S(1)}, bf16[2,1024,256]{2,1,0:T(8,128)(2,1)}, u32[]{:S(2)}) copy-start(bf16[2,1024,256]{2,1,0:T(8,128)(2,1)} %copy-done.6) | copy-start | bytes 3145732
  106.0 19.4 %collective-permute-start.18 = (bf16[2,64,1024]{2,1,0:T(8,128)(2,1)S(1)}, bf16[2,64,1024]{2,1,0:T(8,128)(2,1)S(1)}, u32[]{:S(2)}, u32[]{:S(2)}) collective-permute-start(bf16[2,64,1024]{2,1,0:T(8,128)(2,1)S(1)} %bitcast.44), channel_id=1, source_target_pairs={{0,16},{1,17},{2,18},{3,19},{4,20},{5,21},{6,22},{7,23},{8,24},{9,... | collective-permute-start | bytes 786440 | tf_op jit(solution)/shard_map/ppermute | solution.py:27
  108.8 21.7 %collective-permute-start.12 = (bf16[2,64,1024]{2,1,0:T(8,128)(2,1)S(1)}, bf16[2,64,1024]{2,1,0:T(8,128)(2,1)S(1)}, u32[]{:S(2)}, u32[]{:S(2)}) collective-permute-start(bf16[2,64,1024]{2,1,0:T(8,128)(2,1)S(1)} %bitcast.46), channel_id=1, source_target_pairs={{0,16},{1,17},{2,18},{3,19},{4,20},{5,21},{6,22},{7,23},{8,24},{9,... | collective-permute-start | bytes 786440 | tf_op jit(solution)/shard_map/ppermute | solution.py:27
  121.9 10.2 %collective-permute-start.24 = (bf16[2,160,128]{2,1,0:T(8,128)(2,1)S(1)}, bf16[2,160,128]{2,1,0:T(8,128)(2,1)S(1)}, u32[]{:S(2)}, u32[]{:S(2)}) collective-permute-start(bf16[2,160,128]{2,1,0:T(8,128)(2,1)S(1)} %get-tuple-element.102), channel_id=1, source_target_pairs={{0,1},{1,0},{2,3},{3,2},{4,5},{5,4},{6,7},{7,6},{8,9},{9,8},{10,11... | collective-permute-start | bytes 245768 | tf_op jit(solution)/shard_map/ppermute | solution.py:27
  125.5 19.2 %collective-permute-start.19 = (bf16[2,64,1024]{2,1,0:T(8,128)(2,1)S(1)}, bf16[2,64,1024]{2,1,0:T(8,128)(2,1)S(1)}, u32[]{:S(2)}, u32[]{:S(2)}) collective-permute-start(bf16[2,64,1024]{2,1,0:T(8,128)(2,1)S(1)} %shard_map.150.refs_0_.refs_3_), channel_id=1, source_target_pairs={{0,8},{1,9},{2,10},{3,11},{4,12},{5,13},{6,14},{7,15},{8,0},{9,1},... | collective-permute-start | bytes 786440 | tf_op jit(solution)/shard_map/ppermute | solution.py:27
  130.5 14.6 %collective-permute-start.13 = (bf16[2,64,1024]{2,1,0:T(8,128)(2,1)S(1)}, bf16[2,64,1024]{2,1,0:T(8,128)(2,1)S(1)}, u32[]{:S(2)}, u32[]{:S(2)}) collective-permute-start(bf16[2,64,1024]{2,1,0:T(8,128)(2,1)S(1)} %shard_map.147.refs_0_.refs_3_), channel_id=1, source_target_pairs={{0,4},{1,5},{2,6},{3,7},{4,0},{5,1},{6,2},{7,3},{8,12},{9,13},{10,... | collective-permute-start | bytes 786440 | tf_op jit(solution)/shard_map/ppermute | solution.py:27
  132.1 1.6 collective-permute-start.23
  132.2 4.9 %collective-permute-start.25 = (bf16[2,160,128]{2,1,0:T(8,128)(2,1)S(1)}, bf16[2,160,128]{2,1,0:T(8,128)(2,1)S(1)}, u32[]{:S(2)}, u32[]{:S(2)}) collective-permute-start(bf16[2,160,128]{2,1,0:T(8,128)(2,1)S(1)} %shard_map.156), channel_id=1, source_target_pairs={{0,2},{1,3},{2,0},{3,1},{4,6},{5,7},{6,4},{7,5},{8,10},{9,11},{10,... | collective-permute-start | bytes 245768 | tf_op jit(solution)/shard_map/ppermute | solution.py:27
  137.1 5.4 %collective-permute-start.26 = (bf16[2,160,128]{2,1,0:T(8,128)(2,1)S(1)}, bf16[2,160,128]{2,1,0:T(8,128)(2,1)S(1)}, u32[]{:S(2)}, u32[]{:S(2)}) collective-permute-start(bf16[2,160,128]{2,1,0:T(8,128)(2,1)S(1)} %shard_map.157.mine), channel_id=1, source_target_pairs={{0,4},{1,5},{2,6},{3,7},{4,0},{5,1},{6,2},{7,3},{8,12},{9,13},{10,... | collective-permute-start | bytes 245768 | tf_op jit(solution)/shard_map/ppermute | solution.py:27
  137.7 19.8 %collective-permute-start.22 = (bf16[2,64,1024]{2,1,0:T(8,128)(2,1)S(1)}, bf16[2,64,1024]{2,1,0:T(8,128)(2,1)S(1)}, u32[]{:S(2)}, u32[]{:S(2)}) collective-permute-start(bf16[2,64,1024]{2,1,0:T(8,128)(2,1)S(1)} %shard_map.150.refs_0_.refs_3_), channel_id=1, source_target_pairs={{0,4},{1,5},{2,6},{3,7},{4,0},{5,1},{6,2},{7,3},{8,12},{9,13},{10,... | collective-permute-start | bytes 786440 | tf_op jit(solution)/shard_map/ppermute | solution.py:27
  142.5 6.3 %collective-permute-start.27 = (bf16[2,160,128]{2,1,0:T(8,128)(2,1)S(1)}, bf16[2,160,128]{2,1,0:T(8,128)(2,1)S(1)}, u32[]{:S(2)}, u32[]{:S(2)}) collective-permute-start(bf16[2,160,128]{2,1,0:T(8,128)(2,1)S(1)} %shard_map.158.mine), channel_id=1, source_target_pairs={{0,8},{1,9},{2,10},{3,11},{4,12},{5,13},{6,14},{7,15},{8,0},{9,1},... | collective-permute-start | bytes 245768 | tf_op jit(solution)/shard_map/ppermute | solution.py:27
  142.8 19.7 %collective-permute-start.21 = (bf16[2,64,1024]{2,1,0:T(8,128)(2,1)S(1)}, bf16[2,64,1024]{2,1,0:T(8,128)(2,1)S(1)}, u32[]{:S(2)}, u32[]{:S(2)}) collective-permute-start(bf16[2,64,1024]{2,1,0:T(8,128)(2,1)S(1)} %shard_map.147.refs_0_.refs_3_), channel_id=1, source_target_pairs={{0,8},{1,9},{2,10},{3,11},{4,12},{5,13},{6,14},{7,15},{8,0},{9,1},... | collective-permute-start | bytes 786440 | tf_op jit(solution)/shard_map/ppermute | solution.py:27
  144.6 19.9 %collective-permute-start.20 = (bf16[2,64,1024]{2,1,0:T(8,128)(2,1)S(1)}, bf16[2,64,1024]{2,1,0:T(8,128)(2,1)S(1)}, u32[]{:S(2)}, u32[]{:S(2)}) collective-permute-start(bf16[2,64,1024]{2,1,0:T(8,128)(2,1)S(1)} %collective-permute-done.19.refs_2_), channel_id=1, source_target_pairs={{0,4},{1,5},{2,6},{3,7},{4,0},{5,1},{6,2},{7,3},{8,12},{9,13},{10,... | collective-permute-start | bytes 786440 | tf_op jit(solution)/shard_map/ppermute | solution.py:27
  145.1 20.7 %collective-permute-start.14 = (bf16[2,64,1024]{2,1,0:T(8,128)(2,1)S(1)}, bf16[2,64,1024]{2,1,0:T(8,128)(2,1)S(1)}, u32[]{:S(2)}, u32[]{:S(2)}) collective-permute-start(bf16[2,64,1024]{2,1,0:T(8,128)(2,1)S(1)} %collective-permute-done.13.refs_1_), channel_id=1, source_target_pairs={{0,8},{1,9},{2,10},{3,11},{4,12},{5,13},{6,14},{7,15},{8,0},{9,1},... | collective-permute-start | bytes 786440 | tf_op jit(solution)/shard_map/ppermute | solution.py:27
  148.8 7.1 %collective-permute-start.28 = (bf16[2,160,128]{2,1,0:T(8,128)(2,1)S(1)}, bf16[2,160,128]{2,1,0:T(8,128)(2,1)S(1)}, u32[]{:S(2)}, u32[]{:S(2)}) collective-permute-start(bf16[2,160,128]{2,1,0:T(8,128)(2,1)S(1)} %shard_map.159.mine), channel_id=1, source_target_pairs={{0,16},{1,17},{2,18},{3,19},{4,20},{5,21},{6,22},{7,23},{8,24},{9,... | collective-permute-start | bytes 245768 | tf_op jit(solution)/shard_map/ppermute | solution.py:27
  156.0 4.5 %collective-permute-start.30 = (bf16[2,160,128]{2,1,0:T(8,128)(2,1)S(1)}, bf16[2,160,128]{2,1,0:T(8,128)(2,1)S(1)}, u32[]{:S(2)}, u32[]{:S(2)}) collective-permute-start(bf16[2,160,128]{2,1,0:T(8,128)(2,1)S(1)} %shard_map.160.refs_0_), channel_id=1, source_target_pairs={{0,2},{1,3},{2,0},{3,1},{4,6},{5,7},{6,4},{7,5},{8,10},{9,11},{10,... | collective-permute-start | bytes 245768 | tf_op jit(solution)/shard_map/ppermute | solution.py:27
  157.5 9.7 %collective-permute-start.29 = (bf16[2,160,128]{2,1,0:T(8,128)(2,1)S(1)}, bf16[2,160,128]{2,1,0:T(8,128)(2,1)S(1)}, u32[]{:S(2)}, u32[]{:S(2)}) collective-permute-start(bf16[2,160,128]{2,1,0:T(8,128)(2,1)S(1)} %shard_map.160.refs_0_), channel_id=1, source_target_pairs={{0,1},{1,0},{2,3},{3,2},{4,5},{5,4},{6,7},{7,6},{8,9},{9,8},{10,11... | collective-permute-start | bytes 245768 | tf_op jit(solution)/shard_map/ppermute | solution.py:27
  160.5 6.8 %collective-permute-start.31 = (bf16[2,160,128]{2,1,0:T(8,128)(2,1)S(1)}, bf16[2,160,128]{2,1,0:T(8,128)(2,1)S(1)}, u32[]{:S(2)}, u32[]{:S(2)}) collective-permute-start(bf16[2,160,128]{2,1,0:T(8,128)(2,1)S(1)} %collective-permute-done.30.refs_2_), channel_id=1, source_target_pairs={{0,1},{1,0},{2,3},{3,2},{4,5},{5,4},{6,7},{7,6},{8,9},{9,8},{10,11... | collective-permute-start | bytes 245768 | tf_op jit(solution)/shard_map/ppermute | solution.py:27
